TPU v7x, 128 devices: a whole 4x4x4 slice. The times are simulated.
128 devices in a mesh: kv: 16 (over z, y), tp: 8 (over x, core).
Axes of the slice: x: 4, y: 4, z: 4, core: 2. Of those that a mesh axis runs over, the one named last changes fastest.
Arguments:
- tokens: bfloat16 [16, 4096], P(None, 'kv'), may hold values from -6 to 6
- norm_gain: float32 [4096], P('kv'), may hold values from 0.1 to 1.9
- query_weight: bfloat16 [4096, 2048], P('kv', 'tp'), may hold values from -1 to 1
- key_weight: bfloat16 [4096, 2048], P('kv', 'tp'), may hold values from -0.09375 to 0.09375
- value_weight: bfloat16 [4096, 2048], P('kv', 'tp'), may hold values from -0.09375 to 0.09375
- out_weight: bfloat16 [2048, 4096], P('tp', 'kv'), may hold values from -0.125 to 0.125
- lambdas: float32 [16], P('tp'), may hold values from 0.3 to 0.8
- head_gain: float32 [128], replicated, may hold values from 0.1 to 1.9
- lengths: int32 [16], replicated, may hold values from 1 to 16383, as said below
- key_cache: bfloat16 [16, 16384, 16, 128], P(None, 'kv', 'tp'), may hold values from -48 to 48, as said below
- value_cache: bfloat16 [16, 16384, 16, 128], P(None, 'kv', 'tp'), may hold values from -6 to 6
Outputs:
- attended: bfloat16 [16, 4096], P(None, 'kv')
Inputs may be any that keep to these rules, and one draw needn't show every extreme that they name: `lengths`: each sequence has 1 to 16383 cached tokens. `key_cache`: cached keys lie between -48 and 48.
All inputs are finite; a program needn't handle non-finite values.
Results may differ from a plain program's by a relative error of at most 0.012.
The roundings to bfloat16 on the way count: a program that leaves them out, or rounds other values in their place, can miss the bound.
Values may be sent and summed in bfloat16 or wider, within the bound.
No kernel may reach another device: no remote copies, remote signals or barrier semaphores. Data moves between devices by JAX's collectives and lax.ppermute only.
A program may use at most 64 MiB of HBM per device.

v0:
```python
import jax
import jax.numpy as jnp
from jax import lax
from jax.sharding import PartitionSpec as P

D = 4096
DH = 64


epsilon = 1e-05
theta_base = 500000.0
floor_value = -1e30


def from_everyone(array, axis):
    copies = jnp.broadcast_to(array, (lax.axis_size(axis), *array.shape))
    return lax.all_to_all(copies, axis, split_axis=0, concat_axis=0, tiled=True)


def of_everyone(array, axis):
    return from_everyone(array, axis).sum(axis=0)


def together(arrays, axis):
    ends = [0]
    for a in arrays:
        ends.append(ends[-1] + a.size)
    so_far = of_everyone(jnp.concatenate([a.ravel() for a in arrays]), axis)
    return tuple((so_far[b:e].reshape(a.shape) for a, b, e in zip(arrays, ends, ends[1:])))


def collected_together(array, axis):
    leaves = jax.tree.leaves(array)
    turns = sorted(range(len(leaves)), key=lambda k: -leaves[k].size)
    width = (1, *leaves[turns[0]].shape)[-1]
    lines = [
        jnp.pad(leaves[k].reshape(-1), (0, -leaves[k].size % width)).reshape(-1, width)
        for k in turns
    ]
    both, at, found = (from_everyone(jnp.concatenate(lines), axis), 0, {})
    for k, line in zip(turns, lines):
        section = both[:, at : at + len(line)].reshape(len(both), -1)
        found[k] = section[:, : leaves[k].size].reshape(-1, *leaves[k].shape)
        at += len(line)
    numbers = iter(range(len(leaves)))
    return jax.tree.map(lambda _: found[next(numbers)], array)


def joined_by_halves(pieces, combine):
    while len(jax.tree.leaves(pieces)[0]) > 1:
        pieces = jax.vmap(combine)(
            *(jax.tree.map(lambda part: part[side::2], pieces) for side in (0, 1))
        )
    return jax.tree.map(lambda part: part[0], pieces)


def combined_all(array, axis, combine):
    pieces = collected_together(array, axis)
    return joined_by_halves(pieces, combine)


def angles_for(positions, width):
    halfway = width // 2
    frequency = theta_base ** (-jnp.arange(halfway, dtype=jnp.float32) / halfway)
    return positions.astype(jnp.float32)[:, None] * frequency[None, :]


def rotate(values_in, angles):
    halfway = values_in.shape[-1] // 2
    cosine = jnp.cos(angles)[:, None, None, :]
    sine_part = jnp.sin(angles)[:, None, None, :]
    former = values_in[..., :halfway]
    latter = values_in[..., halfway:]
    return jnp.concatenate(
        [former * cosine - latter * sine_part, latter * cosine + former * sine_part], axis=-1
    )


def finish(query_sum, key_sum, value_sum, square_sum, positions, heads_here):
    scaling = lax.rsqrt(square_sum / D + epsilon)[:, None]
    own_count = query_sum.shape[0]
    angles = angles_for(positions, DH)
    query = rotate((query_sum * scaling).reshape(own_count, heads_here, 2, DH), angles).astype(
        jnp.bfloat16
    )
    fresh_key = rotate((key_sum * scaling).reshape(own_count, heads_here, 2, DH), angles).astype(
        jnp.bfloat16
    )
    fresh_value = (value_sum * scaling).reshape(own_count, heads_here, 2 * DH).astype(jnp.bfloat16)
    return (query, fresh_key, fresh_value)


def combine(former, latter):
    highest = jnp.maximum(former[0], latter[0])
    former_scale = jnp.exp(former[0] - highest)
    latter_scale = jnp.exp(latter[0] - highest)
    return (
        highest,
        former[1] * former_scale + latter[1] * latter_scale,
        former[2] * former_scale[..., None] + latter[2] * latter_scale[..., None],
    )


def local(
    tokens,
    norm_gain,
    query_weight,
    key_weight,
    value_weight,
    out_weight,
    lambdas,
    head_gain,
    lengths,
    key_cache,
    value_cache,
):
    seq_count = tokens.shape[0]
    heads_here = query_weight.shape[1] // (2 * DH)
    widened = tokens.astype(jnp.float32)
    squares = jnp.sum(widened * widened, axis=1)
    normed = (widened * norm_gain[None, :]).astype(jnp.bfloat16)
    query_part = jnp.dot(normed, query_weight, preferred_element_type=jnp.float32)
    key_part = jnp.dot(normed, key_weight, preferred_element_type=jnp.float32)
    value_part = jnp.dot(normed, value_weight, preferred_element_type=jnp.float32)
    query_sum, key_sum, value_sum, square_sum = together(
        (query_part, key_part, value_part, squares), "kv"
    )
    query, fresh_key, fresh_value = finish(
        query_sum, key_sum, value_sum, square_sum, lengths, heads_here
    )
    pos_count = key_cache.shape[1]
    positions = lax.axis_index("kv") * pos_count + jnp.arange(pos_count, dtype=jnp.int32)
    key_blocks = key_cache.reshape(seq_count, pos_count, heads_here, 2, DH)
    scores = jnp.einsum(
        "shjd,sphjd->shjp", query, key_blocks, preferred_element_type=jnp.float32
    ) * DH ** (-0.5)
    fresh_score = jnp.einsum(
        "shjd,shjd->shj", query, fresh_key, preferred_element_type=jnp.float32
    ) * DH ** (-0.5)
    at_length = (positions[None, :] == lengths[:, None])[:, None, None, :]
    visible = (positions[None, :] <= lengths[:, None])[:, None, None, :]
    scores = jnp.where(at_length, fresh_score[..., None], scores)
    masked = jnp.where(visible, scores, floor_value)
    block_max = jnp.max(masked, axis=-1)
    weights = jnp.where(visible, jnp.exp(masked - block_max[..., None]), 0.0).astype(jnp.bfloat16)
    totals = jnp.sum(weights.astype(jnp.float32), axis=-1)
    cached_weights = jnp.where(at_length, jnp.zeros_like(weights), weights)
    weighted = jnp.einsum(
        "shjp,sphe->shje", cached_weights, value_cache, preferred_element_type=jnp.float32
    )
    fresh_weight = jnp.sum(
        jnp.where(at_length, weights, jnp.zeros_like(weights)).astype(jnp.float32), axis=-1
    )
    weighted = weighted + fresh_weight[..., None] * fresh_value[:, :, None, :].astype(jnp.float32)
    highest, totals, weighted = combined_all((block_max, totals, weighted), "kv", combine)
    mixed_heads = (
        weighted[:, :, 0] / totals[:, :, 0, None]
        - lambdas[None, :, None] * weighted[:, :, 1] / totals[:, :, 1, None]
    )
    head_out = (
        mixed_heads
        * lax.rsqrt(jnp.mean(mixed_heads * mixed_heads, axis=-1, keepdims=True) + epsilon)
        * head_gain
    )
    head_out = head_out.astype(jnp.bfloat16).reshape(seq_count, heads_here * 2 * DH)
    partial_value = jnp.dot(head_out, out_weight, preferred_element_type=jnp.float32)
    return of_everyone(partial_value, "tp").astype(jnp.bfloat16)


def solution(mesh):
    return jax.shard_map(
        local,
        mesh=mesh,
        in_specs=(
            P(None, "kv"),
            P("kv"),
            P("kv", "tp"),
            P("kv", "tp"),
            P("kv", "tp"),
            P("tp", "kv"),
            P("tp"),
            P(),
            P(),
            P(None, "kv", "tp", None),
            P(None, "kv", "tp", None),
        ),
        out_specs=P(None, "kv"),
        check_vma=False,
    )
```

profile of v0, /device:TPU:1, one launch (start us, length us, event | category | flops | bytes accessed | tf_op | source)
XLA Modules:
  0.0 93.3 jit_solution(3220499189359782565)
XLA Ops:
  0.0 0.8 fusion.13
  0.9 0.8 convolution_bitcast_fusion.2
  1.8 1.1 %convolution_bitcast_fusion.1 = f32[2,2,8,128]{3,2,1,0:T(8,128)S(1)} fusion(bf16[256,256]{1,0:T(8,128)(2,1)} %param.14, bf16[16,256]{1,0:T(8,128)(2,1)} %param.11, f32[256]{0:T(256)} %param.12), kind=kOutput, calls=%fused_computation.4 | convolution fusion | flops 2109440 | bytes 156672 | tf_op jit(solution)/shard_map/dot_general | solution.py:123
  2.9 1.1 %convolution_bitcast_fusion = f32[2,2,8,128]{3,2,1,0:T(8,128)S(1)} fusion(bf16[256,256]{1,0:T(8,128)(2,1)} %param.15, bf16[16,256]{1,0:T(8,128)(2,1)} %param.11, f32[256]{0:T(256)} %param.12), kind=kOutput, calls=%fused_computation.3 | convolution fusion | flops 2109440 | bytes 156672 | tf_op jit(solution)/shard_map/dot_general | solution.py:124
  4.0 1.3 %broadcast_in_dim.51 = f32[16,1,12304]{2,1,0:T(1,128)} broadcast(f32[12304]{0:T(1024)S(1)} %pad_maximum_fusion), dimensions={2} | broadcast | bytes 836672 | tf_op jit(solution)/shard_map/broadcast_in_dim | solution.py:16
  5.3 8.6 %all-to-all-start = ((f32[16,1,12304]{2,1,0:T(1,128)}), f32[16,1,12304]{2,1,0:T(1,128)S(1)}, u32[]{:S(2)}, u32[]{:S(2)}) async-start(f32[16,1,12304]{2,1,0:T(1,128)} %broadcast_in_dim.51), calls=%async_computation | async-start | bytes 1589248 | tf_op jit(solution)/shard_map/all_to_all | solution.py:17
  13.9 0.7 convert_element_type.47
  14.6 21.2 %copy.138 = bf16[16,1024,2,128]{1,3,2,0:T(8,128)(2,1)} copy(bf16[16,1024,2,128]{3,2,1,0:T(2,128)(2,1)} %param.20) | data formatting | bytes 16777216 | tf_op args[9]
  35.8 0.1 multiply_cosine_fusion
  36.0 0.5 reduce_sum.55
  36.8 0.2 subtract_convert_fusion
  37.0 0.1 fusion.39
  37.1 0.2 fusion.9
  37.3 4.6 %fusion.10 = f32[16,2,2,1,1024]{4,3,2,1,0:T(1,128)S(1)} fusion(bf16[16,1024,2,2,64]{1,4,3,2,0:T(8,128)(2,1)} %bitcast.109, bf16[16,2,2,64,1]{3,2,1,0,4:T(2,128)(2,1)S(1)} %fusion.39), kind=kOutput, calls=%fused_computation.26 | convolution fusion | flops 8388608 | bytes 8658944 | tf_op jit(solution)/shard_map/shjd,sphjd->shjp/dot_general | solution.py:134
  41.9 0.5 fusion.38
  42.4 0.9 convert_reduce_fusion.1
  43.3 0.1 reshape.223
  43.5 0.1 reshape.225
  43.6 4.8 %fusion.2 = f32[16,2,2,128]{3,2,1,0:T(2,128)S(1)} fusion(bf16[16,1024,2,128]{3,2,1,0:T(2,128)(2,1)} %param.21, bf16[16,2,2,1024]{3,2,1,0:T(2,128)(2,1)S(1)} %get-tuple-element.19, pred[16,1024]{1,0:T(8,128)(4,1)S(1)} %get-tuple-element.32, f32[16,2,128]{2,1,0:T(2,128)S(1)} %fusion.25, f32[16,2,2]{2,1,0:T(2,128)S(1)} %get-tuple-element.5), kind=kOutput, calls=%fused_computation.2 | convolution fusion | flops 16859136 | bytes 8585472 | tf_op jit(solution)/shard_map/shjp,sphe->shje/dot_general | solution.py:148
  48.5 0.8 broadcast_in_dim.55
  49.4 6.7 %all-to-all-start.1 = ((f32[16,66,128]{2,1,0:T(8,128)}), f32[16,66,128]{2,1,0:T(8,128)S(1)}, u32[]{:S(2)}, u32[]{:S(2)}) async-start(f32[16,66,128]{2,1,0:T(8,128)} %broadcast_in_dim.55), calls=%async_computation.1 | async-start | bytes 1179648 | tf_op jit(solution)/shard_map/all_to_all | solution.py:17
  56.1 10.8 %all-to-all-done.1 = f32[16,66,128]{2,1,0:T(8,128)S(1)} async-done(((f32[16,66,128]{2,1,0:T(8,128)}), f32[16,66,128]{2,1,0:T(8,128)S(1)}, u32[]{:S(2)}, u32[]{:S(2)}) %all-to-all-start.1) | async-done | bytes 540704 | tf_op jit(solution)/shard_map/all_to_all | solution.py:17
  66.9 0.3 copy.175
  67.2 0.6 slice.138
  67.9 0.6 slice.143
  68.5 0.1 copy.176
  68.6 1.5 %slice.141 = f32[8,16,2,2]{0,3,2,1:T(2,128)S(1)} slice(f32[16,16,2,2]{0,3,2,1:T(2,128)S(1)} %bitcast.112), slice={[0:16:2], [0:16:1], [0:2:1], [0:2:1]} | slice | bytes 4096 | tf_op jit(solution)/shard_map/slice | solution.py:52
  70.2 1.5 %slice.142 = f32[8,16,2,2]{0,3,2,1:T(2,128)S(1)} slice(f32[16,16,2,2]{0,3,2,1:T(2,128)S(1)} %bitcast.113), slice={[1:16:2], [0:16:1], [0:2:1], [0:2:1]} | slice | bytes 4096 | tf_op jit(solution)/shard_map/slice | solution.py:52
  71.7 0.1 copy.179
  71.8 1.5 %slice.159 = f32[8,16,2,2]{0,3,2,1:T(2,128)S(1)} slice(f32[16,16,2,2]{0,3,2,1:T(2,128)S(1)} %bitcast.114), slice={[0:16:2], [0:16:1], [0:2:1], [0:2:1]} | slice | bytes 4096 | tf_op jit(solution)/shard_map/slice | solution.py:52
  73.3 1.5 %slice.160 = f32[8,16,2,2]{0,3,2,1:T(2,128)S(1)} slice(f32[16,16,2,2]{0,3,2,1:T(2,128)S(1)} %bitcast.115), slice={[1:16:2], [0:16:1], [0:2:1], [0:2:1]} | slice | bytes 4096 | tf_op jit(solution)/shard_map/slice | solution.py:52
  74.9 0.1 copy.178
  75.5 0.2 multiply_add_fusion
  75.7 0.8 slice.144
  76.5 0.8 slice.147
  77.3 0.1 copy.146
  77.4 0.1 copy.147
  77.5 0.2 multiply_add_fusion.1
  77.7 0.8 slice.148
  78.5 0.8 slice.151
  79.3 0.1 copy.148
  79.4 0.1 copy.149
  79.7 0.2 multiply_add_fusion.2
  79.9 0.2 fusion.8
  80.3 0.2 fusion.20
  80.9 0.2 fusion.21
  81.1 11.7 %all_to_all.16 = f32[8,16,256]{2,1,0:T(8,128)S(1)} all-to-all(f32[8,16,256]{2,1,0:T(8,128)S(1)} %broadcast_in_dim.56), channel_id=1, replica_groups=mesh['kv'=16,'tp'=8] {'tp'}, dimensions={0} | all-to-all | bytes 262144 | tf_op jit(solution)/shard_map/all_to_all | solution.py:17
  92.7 0.6 reduce_sum.59
  (58 shorter events, 2.1 us)
Async XLA Ops:
  0.0 0.9 copy-start
  5.3 30.7 %all-to-all-start = ((f32[16,1,12304]{2,1,0:T(1,128)}), f32[16,1,12304]{2,1,0:T(1,128)S(1)}, u32[]{:S(2)}, u32[]{:S(2)}) async-start(f32[16,1,12304]{2,1,0:T(1,128)} %broadcast_in_dim.51), calls=%async_computation | async-start | bytes 1589248 | tf_op jit(solution)/shard_map/all_to_all | solution.py:17
  14.6 21.3 %copy-start.3 = (s32[16]{0:T(128)S(1)}, s32[16]{0:T(128)}, u32[]{:S(2)}) copy-start(s32[16]{0:T(128)} %param.19) | copy-start | bytes 196
  41.9 14.1 %copy-start.2 = (f32[2]{0:T(128)S(1)}, f32[2]{0:T(128)}, u32[]{:S(2)}) copy-start(f32[2]{0:T(128)} %param.17) | copy-start | bytes 28
  41.9 14.1 %copy-start.4 = (f32[128]{0:T(128)S(1)}, f32[128]{0:T(128)}, u32[]{:S(2)}) copy-start(f32[128]{0:T(128)} %param.18) | copy-start | bytes 1540
  43.6 37.3 %copy-start.1 = (bf16[256,256]{1,0:T(8,128)(2,1)S(1)}, bf16[256,256]{1,0:T(8,128)(2,1)}, u32[]{:S(2)}) copy-start(bf16[256,256]{1,0:T(8,128)(2,1)} %param.16) | copy-start | bytes 393220
  49.4 17.5 %all-to-all-start.1 = ((f32[16,66,128]{2,1,0:T(8,128)}), f32[16,66,128]{2,1,0:T(8,128)S(1)}, u32[]{:S(2)}, u32[]{:S(2)}) async-start(f32[16,66,128]{2,1,0:T(8,128)} %broadcast_in_dim.55), calls=%async_computation.1 | async-start | bytes 1179648 | tf_op jit(solution)/shard_map/all_to_all | solution.py:17
where the time goes:
time: 94.3 us; the launch traced here: 93.3 us
  local copies, waits for them, and re-layouts  36.7 us (39%)
  starting transfers between devices  15.2 us (16%)
  matrix products  12.6 us (13%)
  blocking collectives  11.7 us (12%)
  waiting for transfers between devices  10.8 us (11%)
  other arithmetic  5.96 us (6%)
    unnamed x23, local copies, waits for them, and re-layouts  22.4 us
    all_to_all x2, starting transfers between devices, from_everyone(): return lax.all_to_all(copies, axis, split_axis=0, concat_axis=0, tiled=True)  15.2 us
    all_to_all x1, blocking collectives, from_everyone(): return lax.all_to_all(copies, axis, split_axis=0, concat_axis=0, tiled=True)  11.7 us
    all_to_all x2, waiting for transfers between devices, from_everyone(): return lax.all_to_all(copies, axis, split_axis=0, concat_axis=0, tiled=True)  10.8 us
    slice x10, local copies, waits for them, and re-layouts, joined_by_halves(): part[side::2]  10.4 us
    dot_general x1, matrix products, local(): jnp.einsum('shjp,sphe->shje', cached_weights, value_cache, preferred_elem...  4.84 us
    dot_general x1, matrix products, local(): jnp.einsum('shjd,sphjd->shjp', query, key_blocks, preferred_element_type=...  4.58 us
    broadcast_in_dim x3, local copies, waits for them, and re-layouts, from_everyone(): copies = jnp.broadcast_to(array, (lax.axis_size(axis), *array.shape))  2.21 us
  transfers between devices with their start and end apart: 2, of which 1 were waited for; matrix products, arithmetic and copies ran while one was open for 24% of the time, Pallas kernels for 0%

commit v1 on v0

v1 whole, which is shorter than its diff:
```python
import jax
import jax.numpy as jnp
from jax import lax
from jax.experimental import pallas as pl
from jax.experimental.pallas import tpu as pltpu
from jax.sharding import PartitionSpec as P

D = 4096
DH = 64
HEADS = 2
SEQS = 16
LANES = 128

epsilon = 1e-05
theta_base = 500000.0
floor_value = -1e30

VM = pl.BlockSpec(memory_space=pltpu.VMEM)
SM = pl.BlockSpec(memory_space=pltpu.SMEM)
ANY = pl.BlockSpec(memory_space=pl.ANY)
F32 = jnp.float32
BF16 = jnp.bfloat16
LOADP = pltpu.CompilerParams(vmem_limit_bytes=30 * 1024 * 1024)
BIG = pltpu.CompilerParams(vmem_limit_bytes=30 * 1024 * 1024)


def iotas(rows):
    shape = (rows, LANES)
    return lax.broadcasted_iota(jnp.int32, shape, 0), lax.broadcasted_iota(jnp.int32, shape, 1)


def project_kernel(tokens, gain, query_weight, key_weight, value_weight, out):
    widened = tokens[...].astype(F32)
    squares = jnp.sum(widened * widened, axis=1, keepdims=True)
    normed = (widened * gain[...]).astype(BF16)
    query = jnp.dot(normed, query_weight[...], preferred_element_type=F32)
    key = jnp.dot(normed, key_weight[...], preferred_element_type=F32)
    value = jnp.dot(normed, value_weight[...], preferred_element_type=F32)
    row, lane = iotas(SEQS)
    square_row = jnp.sum(jnp.where(row == lane, squares, 0.0), axis=0, keepdims=True)
    blank = jnp.zeros((3, LANES), F32)
    for dest in range(SEQS):
        out[dest, 0:16, :] = query[:, :LANES]
        out[dest, 16:32, :] = query[:, LANES:]
        out[dest, 32:40, :] = jnp.concatenate(
            [
                square_row,
                key[dest : dest + 1, :LANES],
                key[dest : dest + 1, LANES:],
                value[dest : dest + 1, :LANES],
                value[dest : dest + 1, LANES:],
                blank,
            ],
            axis=0,
        )


def load_kernel(key_in, value_in, key_out, value_out, sems):
    pieces = 4
    size = SEQS // pieces
    copies = []
    for n in range(pieces):
        part = pl.ds(n * size, size)
        copies.append(pltpu.make_async_copy(key_in.at[part], key_out.at[part], sems.at[0, n]))
        copies.append(pltpu.make_async_copy(value_in.at[part], value_out.at[part], sems.at[1, n]))
    for copy in copies:
        copy.start()
    for copy in copies:
        copy.wait()


def turned(x, cosine, sine):
    lane = lax.broadcasted_iota(jnp.int32, x.shape, 1)
    partner = jnp.where(
        (lane // 32) % 2 == 0, pltpu.roll(x, LANES - 32, 1), pltpu.roll(x, 32, 1)
    )
    return (x * cosine + partner * sine).astype(BF16)


def attend_kernel(lengths, own, got, cosine, sine, keys, values, out, query_rows, scale_rows):
    me = own[0]
    base = me * 1024
    summed = jnp.sum(got[...], axis=0)
    row, lane = iotas(SEQS)
    squares = jnp.sum(jnp.where(row == lane, summed[32:33, :], 0.0), axis=1, keepdims=True)
    scaling = jnp.broadcast_to(lax.rsqrt(squares / D + epsilon), (SEQS, LANES))
    scale_rows[...] = scaling
    for head in range(HEADS):
        turned_query = turned(
            summed[16 * head : 16 * head + 16, :] * scaling, cosine[...], sine[...]
        )
        query_rows[head * SEQS : (head + 1) * SEQS, :] = turned_query.astype(F32)
    sub, lane8 = iotas(8)
    map_lanes = (lane8 // DH) == (sub % 2)
    columns = lax.broadcasted_iota(jnp.int32, (8, 2048), 1)
    subs = lax.broadcasted_iota(jnp.int32, (8, 2048), 0)
    own_head = (columns % 2) == ((subs // 2) % 2)
    maxima = jnp.zeros((8, LANES), F32)
    totals = jnp.zeros((8, LANES), F32)
    for pair in range(SEQS // 2):
        first, second = 2 * pair, 2 * pair + 1

        def row_of(head, seq):
            at = head * SEQS + seq
            return jnp.broadcast_to(query_rows[at : at + 1, :], (8, LANES))

        left = jnp.where(sub < 2, row_of(0, first), row_of(1, first))
        left = jnp.where(map_lanes & (sub < 4), left, 0.0)
        right = jnp.where(sub < 6, row_of(0, second), row_of(1, second))
        right = jnp.where(map_lanes & (sub >= 4), right, 0.0)
        queries = jnp.concatenate([left, right], axis=1).astype(BF16)
        both_keys = jnp.concatenate([keys[first], keys[second]], axis=1)
        scores = lax.dot_general(
            queries, both_keys, (((1,), (1,)), ((), ())), preferred_element_type=F32
        ) * DH ** (-0.5)
        limit = jnp.where(
            subs[:, :1] < 4, 2 * (lengths[first] - base), 2 * (lengths[second] - base)
        )
        visible = own_head & (columns < limit)
        masked = jnp.where(visible, scores, floor_value)
        highest = jnp.max(masked, axis=1, keepdims=True)
        weights = jnp.where(visible, jnp.exp(masked - highest), 0.0).astype(BF16)
        total = jnp.sum(weights.astype(F32), axis=1, keepdims=True)
        both_values = jnp.concatenate([values[first], values[second]], axis=1)
        valued = jnp.dot(weights, both_values, preferred_element_type=F32)
        valued = jnp.where(sub < 4, valued[:, :LANES], valued[:, LANES:])
        place = lane8 == pair * 8 + sub
        maxima = maxima + jnp.where(place, highest, 0.0)
        totals = totals + jnp.where(place, total, 0.0)
        for dest in range(SEQS):
            out[dest, pair * 8 : pair * 8 + 8, :] = valued
    scale = scale_rows[pl.ds(me, 1), :]
    row_cosine = cosine[pl.ds(me, 1), :]
    row_sine = sine[pl.ds(me, 1), :]
    lane1 = lax.broadcasted_iota(jnp.int32, (1, LANES), 1)
    fresh_scores = jnp.zeros((1, LANES), F32)
    for head in range(HEADS):
        query = query_rows[pl.ds(head * SEQS + me, 1), :]
        fresh_key = turned(summed[33 + head : 34 + head, :] * scale, row_cosine, row_sine)
        product = query * fresh_key.astype(F32)
        for side in range(2):
            score = jnp.sum(
                jnp.where(lane1 // DH == side, product, 0.0), axis=1, keepdims=True
            ) * DH ** (-0.5)
            at = me * 4 + head * 2 + side
            fresh_scores = fresh_scores + jnp.where(lane1 == at, score, 0.0)
    fresh_value = (summed[35:37, :] * scale).astype(BF16).astype(F32)
    tail = jnp.concatenate(
        [
            jnp.sum(maxima, axis=0, keepdims=True),
            jnp.sum(totals, axis=0, keepdims=True),
            fresh_scores,
            fresh_value,
            jnp.zeros((3, LANES), F32),
        ],
        axis=0,
    )
    for dest in range(SEQS):
        out[dest, 64:72, :] = tail


def finish_kernel(got, block, share, head_gain, out_weight, out, factors, joined):
    rows16, _ = iotas(SEQS)
    maxima = got[:, 64, :]
    totals = got[:, 65, :]
    fresh = jnp.sum(got[:, 66, :], axis=0, keepdims=True)
    in_block = jnp.max(
        jnp.where(rows16 == block[...], maxima, floor_value), axis=0, keepdims=True
    )
    in_block = jnp.maximum(in_block, fresh)
    top = jnp.maximum(jnp.max(maxima, axis=0, keepdims=True), fresh)
    factor = jnp.exp(maxima - top)
    fresh_factor = jnp.exp(fresh - in_block).astype(BF16).astype(F32) * jnp.exp(in_block - top)
    total = jnp.sum(totals * factor, axis=0, keepdims=True) + fresh_factor
    part = share[...] / total
    factors[...] = jnp.zeros((LANES, LANES), F32)
    factors[0:SEQS, :] = factor * part
    factors[SEQS : SEQS + 1, :] = fresh_factor * part
    columns = factors[...].T
    sub, _ = iotas(8)
    for pair in range(SEQS // 2):
        at = pl.ds(pair * 8, 8)

        def row_of(head, seq):
            return jnp.broadcast_to(got[seq, 67 + head : 68 + head, :], (8, LANES))

        first, second = 2 * pair, 2 * pair + 1
        fresh_value = jnp.where(
            sub < 4,
            jnp.where(sub < 2, row_of(0, first), row_of(1, first)),
            jnp.where(sub < 6, row_of(0, second), row_of(1, second)),
        )
        here = columns[pair * 8 : pair * 8 + 8, :]
        joint = here[:, SEQS : SEQS + 1] * fresh_value
        for peer in range(SEQS):
            joint = joint + here[:, peer : peer + 1] * got[peer, at, :]
        joined[at, :] = joint
    sides = []
    for head in range(HEADS):
        mixed = joined[pl.ds(2 * head, SEQS, 4), :] + joined[pl.ds(2 * head + 1, SEQS, 4), :]
        mean = jnp.mean(mixed * mixed, axis=1, keepdims=True)
        sides.append((mixed * lax.rsqrt(mean + epsilon) * head_gain[...]).astype(BF16))
    head_out = jnp.concatenate(sides, axis=1)
    partial_out = jnp.dot(head_out, out_weight[...], preferred_element_type=F32)
    for dest in range(8):
        out[dest] = partial_out


def local(
    tokens,
    norm_gain,
    query_weight,
    key_weight,
    value_weight,
    out_weight,
    lambdas,
    head_gain,
    lengths,
    key_cache,
    value_cache,
):
    sent = pl.pallas_call(
        project_kernel,
        in_specs=[VM] * 5,
        out_specs=VM,
        out_shape=jax.ShapeDtypeStruct((SEQS, 40, LANES), F32),
        name="project",
    )(tokens, norm_gain.reshape(1, -1), query_weight, key_weight, value_weight)
    got = lax.all_to_all(sent, "kv", split_axis=0, concat_axis=0, tiled=True)
    cache_shape = (SEQS, 2048, LANES)
    keys, values = pl.pallas_call(
        load_kernel,
        in_specs=[ANY, ANY],
        out_specs=[VM, VM],
        out_shape=[pltpu.VMEM(cache_shape, BF16), pltpu.VMEM(cache_shape, BF16)],
        scratch_shapes=[pltpu.SemaphoreType.DMA((2, 4))],
        compiler_params=LOADP,
        name="load",
    )(key_cache.reshape(cache_shape), value_cache.reshape(cache_shape))
    halfway = DH // 2
    frequency = theta_base ** (-jnp.arange(halfway, dtype=F32) / halfway)
    angles = lengths.astype(F32)[:, None] * frequency[None, :]
    cosine = jnp.tile(jnp.cos(angles), (1, 4))
    sine = jnp.sin(angles)
    sine = jnp.tile(jnp.concatenate([-sine, sine], axis=1), (1, 2))
    own = lax.axis_index("kv").astype(jnp.int32).reshape(1)
    shared = pl.pallas_call(
        attend_kernel,
        in_specs=[SM, SM, VM, VM, VM, VM, VM],
        out_specs=VM,
        out_shape=jax.ShapeDtypeStruct((SEQS, 72, LANES), F32),
        scratch_shapes=[pltpu.VMEM((32, LANES), F32), pltpu.VMEM((SEQS, LANES), F32)],
        compiler_params=BIG,
        name="attend",
    )(lengths, own, got, cosine, sine, keys, values)
    everyone = lax.all_to_all(shared, "kv", split_axis=0, concat_axis=0, tiled=True)
    block = jnp.pad(jnp.repeat(lengths // 1024, 4), (0, 64)).reshape(1, LANES)
    share = jnp.tile(
        jnp.stack([jnp.ones_like(lambdas), -lambdas], axis=1).reshape(1, 4), (1, 32)
    )
    partial_out = pl.pallas_call(
        finish_kernel,
        in_specs=[VM] * 5,
        out_specs=VM,
        out_shape=jax.ShapeDtypeStruct((8, SEQS, 256), F32),
        scratch_shapes=[pltpu.VMEM((LANES, LANES), F32), pltpu.VMEM((64, LANES), F32)],
        name="finish",
    )(everyone, block, share, head_gain.reshape(1, -1), out_weight)
    shares = lax.all_to_all(partial_out, "tp", split_axis=0, concat_axis=0, tiled=True)
    return shares.sum(axis=0).astype(BF16)


def solution(mesh):
    return jax.shard_map(
        local,
        mesh=mesh,
        in_specs=(
            P(None, "kv"),
            P("kv"),
            P("kv", "tp"),
            P("kv", "tp"),
            P("kv", "tp"),
            P("tp", "kv"),
            P("tp"),
            P(),
            P(),
            P(None, "kv", "tp", None),
            P(None, "kv", "tp", None),
        ),
        out_specs=P(None, "kv"),
        check_vma=False,
    )
```

time: 94.3 us -> 71.1 us (0.75)
  local copies, waits for them, and re-layouts: 36.7 us -> 15.8 us
  Pallas kernels: 0 us -> 16.8 us
  matrix products: 12.6 us -> 0 us
  other arithmetic: 5.96 us -> 1.56 us
  waiting for transfers between devices: 10.8 us -> 9.26 us
    pallas_call x0 -> x4, Pallas kernels: none -> 16.8 us  [the longest x1 6.48 us: local(): pl.pallas_call(attend_kernel, in_specs=[SM, SM, VM, VM, VM, VM, VM], out_...]
    dot_general x6 -> x0, matrix products: 12.6 us -> none  [the longest x1 4.84 us: local(): jnp.einsum('shjp,sphe->shje', cached_weights, value_cache, preferred_elem...]
    slice x20 -> x0, local copies, waits for them, and re-layouts: 10.5 us -> none  [the longest x10 10.4 us: joined_by_halves(): part[side::2]]
    unnamed x23 -> x15, local copies, waits for them, and re-layouts: 22.4 us -> 14.1 us
    reduce_sum x5 -> x1, other arithmetic: 3.02 us -> 0.61 us  [local(): return shares.sum(axis=0).astype(BF16)]
    broadcast_in_dim x3 -> x1, local copies, waits for them, and re-layouts: 2.21 us -> 0.07 us  [local(): block = jnp.pad(jnp.repeat(lengths // 1024, 4), (0, 64)).reshape(1, LANES)]
    all_to_all x2, waiting for transfers between devices: 10.8 us -> 9.26 us  [the longest x1 9.25 us: local(): lax.all_to_all(shared, 'kv', split_axis=0, concat_axis=0, tiled=True)]
    another operation x0 -> x8, local copies, waits for them, and re-layouts: none -> 0.99 us  [the longest x3 0.74 us: local(): jnp.tile(jnp.stack([jnp.ones_like(lambdas), -lambdas], axis=1).reshape(1,...]
  transfers between devices with their start and end apart: 2 -> 2, of which waited for: 1 -> 1; matrix products, arithmetic and copies ran while one was open for 24% -> 4% of each run, Pallas kernels for 0% -> 8%
where the time goes in v1:
time: 71.1 us; the launch traced here: 70.6 us
  Pallas kernels  16.8 us (24%)
  local copies, waits for them, and re-layouts  15.8 us (22%)
  starting transfers between devices  15.2 us (21%)
  blocking collectives  11.9 us (17%)
  waiting for transfers between devices  9.26 us (13%)
  other arithmetic  1.56 us (2%)
    unnamed x15, local copies, waits for them, and re-layouts  14.1 us
    all_to_all x1, blocking collectives, local(): lax.all_to_all(partial_out, 'tp', split_axis=0, concat_axis=0, tiled=True)  11.9 us
    all_to_all x1, waiting for transfers between devices, local(): lax.all_to_all(shared, 'kv', split_axis=0, concat_axis=0, tiled=True)  9.25 us
    all_to_all x1, starting transfers between devices, local(): got = lax.all_to_all(sent, 'kv', split_axis=0, concat_axis=0, tiled=True)  8.59 us
    all_to_all x1, starting transfers between devices, local(): lax.all_to_all(shared, 'kv', split_axis=0, concat_axis=0, tiled=True)  6.65 us
    pallas_call x1, Pallas kernels, local(): pl.pallas_call(attend_kernel, in_specs=[SM, SM, VM, VM, VM, VM, VM], out_...  6.48 us
    pallas_call x1, Pallas kernels, local(): pl.pallas_call(load_kernel, in_specs=[ANY, ANY], out_specs=[VM, VM], out_...  5.93 us
    pallas_call x1, Pallas kernels, local(): pl.pallas_call(finish_kernel, in_specs=[VM] * 5, out_specs=VM, out_shape=...  2.39 us
  transfers between devices with their start and end apart: 2, of which 1 were waited for; matrix products, arithmetic and copies ran while one was open for 4% of the time, Pallas kernels for 8%

profile of v1, /device:TPU:1, one launch (start us, length us, event | category | flops | bytes accessed | tf_op | source)
XLA Modules:
  0.0 70.6 jit_solution(4552677369801852042)
XLA Ops:
  0.0 2.0 %project.1 = f32[16,40,128]{2,1,0:T(8,128)} custom-call(bf16[16,256]{1,0:T(8,128)(2,1)} %tokens.1, f32[1,256]{1,0:T(1,128)} %bitcast.11, bf16[256,256]{1,0:T(8,128)(2,1)} %query_weight.1, bf16[256,256]{1,0:T(8,128)(2,1)} %key_weight.1, bf16[256,256]{1,0:T(8,128)(2,1)} %value_weight.1), custom_call_target="tpu_custom_call" | custom-call | tf_op jit(solution)/shard_map/project/pallas_call | solution.py:222
  2.0 8.6 %all-to-all-start = ((f32[16,40,128]{2,1,0:T(8,128)}), f32[16,40,128]{2,1,0:T(8,128)S(1)}, u32[]{:S(2)}, u32[]{:S(2)}) async-start(f32[16,40,128]{2,1,0:T(8,128)} %project.1), calls=%async_computation | async-start | bytes 655360 | tf_op jit(solution)/shard_map/all_to_all | solution.py:229
  10.6 0.7 %and_select_fusion = (s32[16]{0:T(128)S(1)}, f32[16]{0:T(128)S(1)}) fusion(s32[16]{0:T(128)} %lengths.1), kind=kLoop, calls=%fused_computation.4 | loop fusion | flops 256 | bytes 192 | tf_op jit(solution)/shard_map/jit(floor_divide)/jit(_where)/select_n | solution.py:257
  11.3 0.1 fusion
  11.5 0.1 pad_maximum_fusion
  11.5 0.1 tile.31.sine
  11.6 0.1 tile.29.cosine
  11.7 0.0 copy-start.4
  11.7 5.9 %load.1 = (bf16[16,2048,128]{2,1,0:T(8,128)(2,1)S(1)}, bf16[16,2048,128]{2,1,0:T(8,128)(2,1)S(1)}) custom-call(bf16[16,2048,128]{2,1,0:T(8,128)(2,1)} %bitcast.9, bf16[16,2048,128]{2,1,0:T(8,128)(2,1)} %bitcast.10), custom_call_target="tpu_custom_call" | custom-call | tf_op jit(solution)/shard_map/load/pallas_call | solution.py:231
  17.7 0.0 copy-start
  17.7 3.2 %copy-done = bf16[16,2048,128]{2,1,0:T(8,128)(2,1)} copy-done((bf16[16,2048,128]{2,1,0:T(8,128)(2,1)}, bf16[16,2048,128]{2,1,0:T(8,128)(2,1)S(1)}, u32[]{:S(2)}) %copy-start) | copy-done | bytes 8388632
  20.9 0.0 copy-start.2
  20.9 3.2 %copy-done.2 = bf16[16,2048,128]{2,1,0:T(8,128)(2,1)} copy-done((bf16[16,2048,128]{2,1,0:T(8,128)(2,1)}, bf16[16,2048,128]{2,1,0:T(8,128)(2,1)S(1)}, u32[]{:S(2)}) %copy-start.2) | copy-done | bytes 8388632
  24.1 0.0 all-to-all-done.got
  24.1 0.0 copy-done.4
  24.1 0.0 copy-start.1
  24.1 3.4 %copy-done.1 = bf16[16,2048,128]{2,1,0:T(8,128)(2,1)S(1)} copy-done((bf16[16,2048,128]{2,1,0:T(8,128)(2,1)S(1)}, bf16[16,2048,128]{2,1,0:T(8,128)(2,1)}, u32[]{:S(2)}) %copy-start.1) | copy-done | bytes 8388632
  27.5 0.0 copy-start.3
  27.5 3.4 %copy-done.3 = bf16[16,2048,128]{2,1,0:T(8,128)(2,1)S(1)} copy-done((bf16[16,2048,128]{2,1,0:T(8,128)(2,1)S(1)}, bf16[16,2048,128]{2,1,0:T(8,128)(2,1)}, u32[]{:S(2)}) %copy-start.3) | copy-done | bytes 8388632
  30.9 0.0 copy-start.6
  30.9 6.5 %attend.1 = f32[16,72,128]{2,1,0:T(8,128)} custom-call(s32[16]{0:T(128)S(1)} %copy-done.4, s32[1]{0:T(128)} %bitcast.own, f32[16,40,128]{2,1,0:T(8,128)S(1)} %all-to-all-done.got, f32[16,128]{1,0:T(8,128)S(1)} %tile.29.cosine, f32[16,128]{1,0:T(8,128)S(1)} %tile.31.sine, bf16[16,2048,128]{2,1,0:T(8,128)(2,1)S(1)} %copy-done.1, ...), custom_call_target="tpu_custom_call" | custom-call | tf_op jit(solution)/shard_map/attend/pallas_call | solution.py:247
  37.4 6.7 %all-to-all-start.1 = ((f32[16,72,128]{2,1,0:T(8,128)}), f32[16,72,128]{2,1,0:T(8,128)S(1)}, u32[]{:S(2)}, u32[]{:S(2)}) async-start(f32[16,72,128]{2,1,0:T(8,128)} %attend.1), calls=%async_computation.1 | async-start | bytes 1179648 | tf_op jit(solution)/shard_map/all_to_all | solution.py:256
  44.0 0.1 broadcast_in_dim.2
  44.1 0.1 reshape.71
  44.2 0.0 copy-done.6
  44.2 0.1 copy.14
  44.3 0.1 stack.7.clone
  44.4 0.1 tile.32
  44.5 0.6 tile.34.share
  45.1 0.5 pad_bitcast_fusion.block
  45.6 9.3 %all-to-all-done.1.got = f32[16,72,128]{2,1,0:T(8,128)S(1)} async-done(((f32[16,72,128]{2,1,0:T(8,128)}), f32[16,72,128]{2,1,0:T(8,128)S(1)}, u32[]{:S(2)}, u32[]{:S(2)}) %all-to-all-start.1) | async-done | bytes 589856 | tf_op jit(solution)/shard_map/all_to_all | solution.py:256
  54.9 0.0 copy-start.5
  54.9 0.8 %copy-done.5 = f32[16,72,128]{2,1,0:T(8,128)} copy-done((f32[16,72,128]{2,1,0:T(8,128)}, f32[16,72,128]{2,1,0:T(8,128)S(1)}, u32[]{:S(2)}) %copy-start.5) | copy-done | bytes 589848
  55.7 2.4 %finish.1 = f32[8,16,256]{2,1,0:T(8,128)} custom-call(f32[16,72,128]{2,1,0:T(8,128)} %copy-done.5, s32[1,128]{1,0:T(1,128)} %pad_bitcast_fusion.block, f32[1,128]{1,0:T(1,128)} %tile.34.share, f32[1,128]{1,0:T(1,128)} %bitcast.12, bf16[256,256]{1,0:T(8,128)(2,1)} %out_weight.1), custom_call_target="tpu_custom_call" | custom-call | tf_op jit(solution)/shard_map/finish/pallas_call | solution.py:261
  58.1 11.9 %all_to_all.15 = f32[8,16,256]{2,1,0:T(8,128)S(1)} all-to-all(f32[8,16,256]{2,1,0:T(8,128)} %finish.1), channel_id=1, replica_groups=mesh['kv'=16,'tp'=8] {'tp'}, dimensions={0} | all-to-all | bytes 262144 | tf_op jit(solution)/shard_map/all_to_all | solution.py:269
  70.0 0.6 reduce_sum.9
  (5 shorter events, 0.0 us)
Async XLA Ops:
  2.0 22.1 %all-to-all-start = ((f32[16,40,128]{2,1,0:T(8,128)}), f32[16,40,128]{2,1,0:T(8,128)S(1)}, u32[]{:S(2)}, u32[]{:S(2)}) async-start(f32[16,40,128]{2,1,0:T(8,128)} %project.1), calls=%async_computation | async-start | bytes 655360 | tf_op jit(solution)/shard_map/all_to_all | solution.py:229
  11.7 12.4 %copy-start.4 = (s32[16]{0:T(128)S(1)}, s32[16]{0:T(128)}, u32[]{:S(2)}) copy-start(s32[16]{0:T(128)} %lengths.1) | copy-start | bytes 196
  17.7 3.2 %copy-start = (bf16[16,2048,128]{2,1,0:T(8,128)(2,1)}, bf16[16,2048,128]{2,1,0:T(8,128)(2,1)S(1)}, u32[]{:S(2)}) copy-start(bf16[16,2048,128]{2,1,0:T(8,128)(2,1)S(1)} %get-tuple-element.7.keys) | copy-start | bytes 25165828
  20.9 3.2 %copy-start.2 = (bf16[16,2048,128]{2,1,0:T(8,128)(2,1)}, bf16[16,2048,128]{2,1,0:T(8,128)(2,1)S(1)}, u32[]{:S(2)}) copy-start(bf16[16,2048,128]{2,1,0:T(8,128)(2,1)S(1)} %get-tuple-element.8.values) | copy-start | bytes 25165828
  24.1 3.4 %copy-start.1 = (bf16[16,2048,128]{2,1,0:T(8,128)(2,1)S(1)}, bf16[16,2048,128]{2,1,0:T(8,128)(2,1)}, u32[]{:S(2)}) copy-start(bf16[16,2048,128]{2,1,0:T(8,128)(2,1)} %copy-done) | copy-start | bytes 25165828
  27.5 3.4 %copy-start.3 = (bf16[16,2048,128]{2,1,0:T(8,128)(2,1)S(1)}, bf16[16,2048,128]{2,1,0:T(8,128)(2,1)}, u32[]{:S(2)}) copy-start(bf16[16,2048,128]{2,1,0:T(8,128)(2,1)} %copy-done.2) | copy-start | bytes 25165828
  30.9 13.3 %copy-start.6 = (f32[2]{0:T(128)S(1)}, f32[2]{0:T(128)}, u32[]{:S(2)}) copy-start(f32[2]{0:T(128)} %param.17) | copy-start | bytes 28
  37.4 17.5 %all-to-all-start.1 = ((f32[16,72,128]{2,1,0:T(8,128)}), f32[16,72,128]{2,1,0:T(8,128)S(1)}, u32[]{:S(2)}, u32[]{:S(2)}) async-start(f32[16,72,128]{2,1,0:T(8,128)} %attend.1), calls=%async_computation.1 | async-start | bytes 1179648 | tf_op jit(solution)/shard_map/all_to_all | solution.py:256
  54.9 0.8 %copy-start.5 = (f32[16,72,128]{2,1,0:T(8,128)}, f32[16,72,128]{2,1,0:T(8,128)S(1)}, u32[]{:S(2)}) copy-start(f32[16,72,128]{2,1,0:T(8,128)S(1)} %all-to-all-done.1.got) | copy-start | bytes 1769476

commit v2 on v1

--- a/solution.py
+++ b/solution.py
@@ -20,7 +20,7 @@
 ANY = pl.BlockSpec(memory_space=pl.ANY)
 F32 = jnp.float32
 BF16 = jnp.bfloat16
-LOADP = pltpu.CompilerParams(vmem_limit_bytes=30 * 1024 * 1024)
+SMALL = pltpu.CompilerParams(vmem_limit_bytes=8 * 1024 * 1024)
 BIG = pltpu.CompilerParams(vmem_limit_bytes=30 * 1024 * 1024)
 
 
@@ -55,20 +55,6 @@
         )
 
 
-def load_kernel(key_in, value_in, key_out, value_out, sems):
-    pieces = 4
-    size = SEQS // pieces
-    copies = []
-    for n in range(pieces):
-        part = pl.ds(n * size, size)
-        copies.append(pltpu.make_async_copy(key_in.at[part], key_out.at[part], sems.at[0, n]))
-        copies.append(pltpu.make_async_copy(value_in.at[part], value_out.at[part], sems.at[1, n]))
-    for copy in copies:
-        copy.start()
-    for copy in copies:
-        copy.wait()
-
-
 def turned(x, cosine, sine):
     lane = lax.broadcasted_iota(jnp.int32, x.shape, 1)
     partner = jnp.where(
@@ -77,7 +63,18 @@
     return (x * cosine + partner * sine).astype(BF16)
 
 
-def attend_kernel(lengths, own, got, cosine, sine, keys, values, out, query_rows, scale_rows):
+def attend_kernel(
+    lengths, own, got, cosine, sine, keys_in, values_in, out, keys, values, arrived, query_rows,
+    scale_rows, score_rows, weight_rows
+):
+    copies = []
+    for kind, (source, target) in enumerate(((keys_in, keys), (values_in, values))):
+        for seq in range(SEQS):
+            copies.append(
+                pltpu.make_async_copy(source.at[seq], target.at[seq], arrived.at[kind, seq])
+            )
+    for copy in copies:
+        copy.start()
     me = own[0]
     base = me * 1024
     summed = jnp.sum(got[...], axis=0)
@@ -92,6 +89,25 @@
         query_rows[head * SEQS : (head + 1) * SEQS, :] = turned_query.astype(F32)
     sub, lane8 = iotas(8)
     map_lanes = (lane8 // DH) == (sub % 2)
+    limits = []
+    for pair in range(SEQS // 2):
+        first, second = 2 * pair, 2 * pair + 1
+
+        def row_of(head, seq):
+            at = head * SEQS + seq
+            return jnp.broadcast_to(query_rows[at : at + 1, :], (8, LANES))
+
+        left = jnp.where(sub < 2, row_of(0, first), row_of(1, first))
+        left = jnp.where(map_lanes & (sub < 4), left, 0.0)
+        right = jnp.where(sub < 6, row_of(0, second), row_of(1, second))
+        right = jnp.where(map_lanes & (sub >= 4), right, 0.0)
+        queries = jnp.concatenate([left, right], axis=1).astype(BF16)
+        copies[first].wait()
+        copies[second].wait()
+        both_keys = jnp.concatenate([keys[first], keys[second]], axis=1)
+        score_rows[pair * 8 : pair * 8 + 8, :] = lax.dot_general(
+            queries, both_keys, (((1,), (1,)), ((), ())), preferred_element_type=F32
+        )
     columns = lax.broadcasted_iota(jnp.int32, (8, 2048), 1)
     subs = lax.broadcasted_iota(jnp.int32, (8, 2048), 0)
     own_head = (columns % 2) == ((subs // 2) % 2)
@@ -99,36 +115,19 @@
     totals = jnp.zeros((8, LANES), F32)
     for pair in range(SEQS // 2):
         first, second = 2 * pair, 2 * pair + 1
-
-        def row_of(head, seq):
-            at = head * SEQS + seq
-            return jnp.broadcast_to(query_rows[at : at + 1, :], (8, LANES))
-
-        left = jnp.where(sub < 2, row_of(0, first), row_of(1, first))
-        left = jnp.where(map_lanes & (sub < 4), left, 0.0)
-        right = jnp.where(sub < 6, row_of(0, second), row_of(1, second))
-        right = jnp.where(map_lanes & (sub >= 4), right, 0.0)
-        queries = jnp.concatenate([left, right], axis=1).astype(BF16)
-        both_keys = jnp.concatenate([keys[first], keys[second]], axis=1)
-        scores = lax.dot_general(
-            queries, both_keys, (((1,), (1,)), ((), ())), preferred_element_type=F32
-        ) * DH ** (-0.5)
+        at = slice(pair * 8, pair * 8 + 8)
         limit = jnp.where(
             subs[:, :1] < 4, 2 * (lengths[first] - base), 2 * (lengths[second] - base)
         )
         visible = own_head & (columns < limit)
-        masked = jnp.where(visible, scores, floor_value)
+        masked = jnp.where(visible, score_rows[at, :] * DH ** (-0.5), floor_value)
         highest = jnp.max(masked, axis=1, keepdims=True)
         weights = jnp.where(visible, jnp.exp(masked - highest), 0.0).astype(BF16)
         total = jnp.sum(weights.astype(F32), axis=1, keepdims=True)
-        both_values = jnp.concatenate([values[first], values[second]], axis=1)
-        valued = jnp.dot(weights, both_values, preferred_element_type=F32)
-        valued = jnp.where(sub < 4, valued[:, :LANES], valued[:, LANES:])
+        weight_rows[at, :] = weights
         place = lane8 == pair * 8 + sub
         maxima = maxima + jnp.where(place, highest, 0.0)
         totals = totals + jnp.where(place, total, 0.0)
-        for dest in range(SEQS):
-            out[dest, pair * 8 : pair * 8 + 8, :] = valued
     scale = scale_rows[pl.ds(me, 1), :]
     row_cosine = cosine[pl.ds(me, 1), :]
     row_sine = sine[pl.ds(me, 1), :]
@@ -147,23 +146,50 @@
     fresh_value = (summed[35:37, :] * scale).astype(BF16).astype(F32)
     tail = jnp.concatenate(
         [
-            jnp.sum(maxima, axis=0, keepdims=True),
-            jnp.sum(totals, axis=0, keepdims=True),
-            fresh_scores,
+            *thirds(jnp.sum(maxima, axis=0, keepdims=True)),
+            *thirds(jnp.sum(totals, axis=0, keepdims=True)),
+            *thirds(fresh_scores),
             fresh_value,
-            jnp.zeros((3, LANES), F32),
+            jnp.zeros((5, LANES), F32),
         ],
         axis=0,
-    )
+    ).astype(BF16)
     for dest in range(SEQS):
-        out[dest, 64:72, :] = tail
+        out[dest, 64:80, :] = tail
+    for two in range(SEQS // 4):
+        parts = []
+        for pair in (2 * two, 2 * two + 1):
+            first, second = 2 * pair, 2 * pair + 1
+            copies[SEQS + first].wait()
+            copies[SEQS + second].wait()
+            both_values = jnp.concatenate([values[first], values[second]], axis=1)
+            valued = jnp.dot(
+                weight_rows[pair * 8 : pair * 8 + 8, :],
+                both_values,
+                preferred_element_type=F32,
+            )
+            parts.append(jnp.where(sub < 4, valued[:, :LANES], valued[:, LANES:]))
+        sixteen = jnp.concatenate(parts, axis=0).astype(BF16)
+        for dest in range(SEQS):
+            out[dest, two * 16 : two * 16 + 16, :] = sixteen
+
+
+def thirds(x):
+    high = x.astype(BF16).astype(F32)
+    middle = (x - high).astype(BF16).astype(F32)
+    return high, middle, x - high - middle
 
 
 def finish_kernel(got, block, share, head_gain, out_weight, out, factors, joined):
     rows16, _ = iotas(SEQS)
-    maxima = got[:, 64, :]
-    totals = got[:, 65, :]
-    fresh = jnp.sum(got[:, 66, :], axis=0, keepdims=True)
+    tails = got[:, 64:80, :].astype(F32)
+
+    def whole(at):
+        return tails[:, at, :] + tails[:, at + 1, :] + tails[:, at + 2, :]
+
+    maxima = whole(0)
+    totals = whole(3)
+    fresh = jnp.sum(whole(6), axis=0, keepdims=True)
     in_block = jnp.max(
         jnp.where(rows16 == block[...], maxima, floor_value), axis=0, keepdims=True
     )
@@ -177,24 +203,19 @@
     factors[0:SEQS, :] = factor * part
     factors[SEQS : SEQS + 1, :] = fresh_factor * part
     columns = factors[...].T
-    sub, _ = iotas(8)
-    for pair in range(SEQS // 2):
-        at = pl.ds(pair * 8, 8)
-
-        def row_of(head, seq):
-            return jnp.broadcast_to(got[seq, 67 + head : 68 + head, :], (8, LANES))
-
-        first, second = 2 * pair, 2 * pair + 1
-        fresh_value = jnp.where(
-            sub < 4,
-            jnp.where(sub < 2, row_of(0, first), row_of(1, first)),
-            jnp.where(sub < 6, row_of(0, second), row_of(1, second)),
-        )
-        here = columns[pair * 8 : pair * 8 + 8, :]
+    sub, _ = iotas(16)
+    for four in range(SEQS // 4):
+        here = columns[four * 16 : four * 16 + 16, :]
+        fresh_value = jnp.zeros((16, LANES), F32)
+        for n in range(8):
+            line = tails[four * 4 + n // 2, 9 + n % 2 : 10 + n % 2, :]
+            fresh_value = jnp.where(sub // 2 == n, line, fresh_value)
         joint = here[:, SEQS : SEQS + 1] * fresh_value
         for peer in range(SEQS):
-            joint = joint + here[:, peer : peer + 1] * got[peer, at, :]
-        joined[at, :] = joint
+            joint = joint + here[:, peer : peer + 1] * got[
+                peer, four * 16 : four * 16 + 16, :
+            ].astype(F32)
+        joined[four * 16 : four * 16 + 16, :] = joint
     sides = []
     for head in range(HEADS):
         mixed = joined[pl.ds(2 * head, SEQS, 4), :] + joined[pl.ds(2 * head + 1, SEQS, 4), :]
@@ -224,19 +245,11 @@
         in_specs=[VM] * 5,
         out_specs=VM,
         out_shape=jax.ShapeDtypeStruct((SEQS, 40, LANES), F32),
+        compiler_params=SMALL,
         name="project",
     )(tokens, norm_gain.reshape(1, -1), query_weight, key_weight, value_weight)
     got = lax.all_to_all(sent, "kv", split_axis=0, concat_axis=0, tiled=True)
     cache_shape = (SEQS, 2048, LANES)
-    keys, values = pl.pallas_call(
-        load_kernel,
-        in_specs=[ANY, ANY],
-        out_specs=[VM, VM],
-        out_shape=[pltpu.VMEM(cache_shape, BF16), pltpu.VMEM(cache_shape, BF16)],
-        scratch_shapes=[pltpu.SemaphoreType.DMA((2, 4))],
-        compiler_params=LOADP,
-        name="load",
-    )(key_cache.reshape(cache_shape), value_cache.reshape(cache_shape))
     halfway = DH // 2
     frequency = theta_base ** (-jnp.arange(halfway, dtype=F32) / halfway)
     angles = lengths.astype(F32)[:, None] * frequency[None, :]
@@ -246,13 +259,29 @@
     own = lax.axis_index("kv").astype(jnp.int32).reshape(1)
     shared = pl.pallas_call(
         attend_kernel,
-        in_specs=[SM, SM, VM, VM, VM, VM, VM],
+        in_specs=[SM, SM, VM, VM, VM, ANY, ANY],
         out_specs=VM,
-        out_shape=jax.ShapeDtypeStruct((SEQS, 72, LANES), F32),
-        scratch_shapes=[pltpu.VMEM((32, LANES), F32), pltpu.VMEM((SEQS, LANES), F32)],
+        out_shape=jax.ShapeDtypeStruct((SEQS, 80, LANES), BF16),
+        scratch_shapes=[
+            pltpu.VMEM(cache_shape, BF16),
+            pltpu.VMEM(cache_shape, BF16),
+            pltpu.SemaphoreType.DMA((2, SEQS)),
+            pltpu.VMEM((32, LANES), F32),
+            pltpu.VMEM((SEQS, LANES), F32),
+            pltpu.VMEM((64, 2048), F32),
+            pltpu.VMEM((64, 2048), BF16),
+        ],
         compiler_params=BIG,
         name="attend",
-    )(lengths, own, got, cosine, sine, keys, values)
+    )(
+        lengths,
+        own,
+        got,
+        cosine,
+        sine,
+        key_cache.reshape(cache_shape),
+        value_cache.reshape(cache_shape),
+    )
     everyone = lax.all_to_all(shared, "kv", split_axis=0, concat_axis=0, tiled=True)
     block = jnp.pad(jnp.repeat(lengths // 1024, 4), (0, 64)).reshape(1, LANES)
     share = jnp.tile(
@@ -264,6 +293,7 @@
         out_specs=VM,
         out_shape=jax.ShapeDtypeStruct((8, SEQS, 256), F32),
         scratch_shapes=[pltpu.VMEM((LANES, LANES), F32), pltpu.VMEM((64, LANES), F32)],
+        compiler_params=SMALL,
         name="finish",
     )(everyone, block, share, head_gain.reshape(1, -1), out_weight)
     shares = lax.all_to_all(partial_out, "tp", split_axis=0, concat_axis=0, tiled=True)

time: 71.1 us -> 64.5 us (0.907)
  Pallas kernels: 16.8 us -> 10.9 us
  waiting for transfers between devices: 9.26 us -> 14.8 us
  local copies, waits for them, and re-layouts: 15.8 us -> 12.2 us
  starting transfers between devices: 15.2 us -> 12.1 us
    all_to_all x1, waiting for transfers between devices: 0.01 us -> 7.21 us  [local(): got = lax.all_to_all(sent, 'kv', split_axis=0, concat_axis=0, tiled=True)]
    all_to_all x1, starting transfers between devices: 6.65 us -> 3.55 us  [local(): lax.all_to_all(shared, 'kv', split_axis=0, concat_axis=0, tiled=True)]
    pallas_call x2 -> x1, Pallas kernels: 12.4 us -> 9.39 us  [local(): pl.pallas_call(attend_kernel, in_specs=[SM, SM, VM, VM, VM, ANY, ANY], ou...]
    unnamed x15 -> x23, local copies, waits for them, and re-layouts: 14.1 us -> 11.6 us
    pallas_call x1, Pallas kernels: 2.39 us -> 0.64 us  [local(): pl.pallas_call(finish_kernel, in_specs=[VM] * 5, out_specs=VM, out_shape=...]
    all_to_all x1, waiting for transfers between devices: 9.25 us -> 7.56 us  [local(): lax.all_to_all(shared, 'kv', split_axis=0, concat_axis=0, tiled=True)]
    pallas_call x1, Pallas kernels: 1.98 us -> 0.92 us  [local(): pl.pallas_call(project_kernel, in_specs=[VM] * 5, out_specs=VM, out_shape...]
  transfers between devices with their start and end apart: 2 -> 2, of which waited for: 1 -> 2; matrix products, arithmetic and copies ran while one was open for 4% -> 3% of each run, Pallas kernels for 8% -> 0%
where the time goes in v2:
time: 64.5 us; the launch traced here: 63.9 us
  waiting for transfers between devices  14.8 us (23%)
  local copies, waits for them, and re-layouts  12.2 us (19%)
  blocking collectives  12.2 us (19%)
  starting transfers between devices  12.1 us (19%)
  Pallas kernels  10.9 us (17%)
  other arithmetic  1.56 us (2%)
    all_to_all x1, blocking collectives, local(): lax.all_to_all(partial_out, 'tp', split_axis=0, concat_axis=0, tiled=True)  12.2 us
    unnamed x23, local copies, waits for them, and re-layouts  11.6 us
    pallas_call x1, Pallas kernels, local(): pl.pallas_call(attend_kernel, in_specs=[SM, SM, VM, VM, VM, ANY, ANY], ou...  9.39 us
    all_to_all x1, starting transfers between devices, local(): got = lax.all_to_all(sent, 'kv', split_axis=0, concat_axis=0, tiled=True)  8.59 us
    all_to_all x1, waiting for transfers between devices, local(): lax.all_to_all(shared, 'kv', split_axis=0, concat_axis=0, tiled=True)  7.56 us
    all_to_all x1, waiting for transfers between devices, local(): got = lax.all_to_all(sent, 'kv', split_axis=0, concat_axis=0, tiled=True)  7.21 us
    all_to_all x1, starting transfers between devices, local(): lax.all_to_all(shared, 'kv', split_axis=0, concat_axis=0, tiled=True)  3.55 us
  transfers between devices with their start and end apart: 2, of which 2 were waited for; matrix products, arithmetic and copies ran while one was open for 3% of the time, Pallas kernels for 0%

profile of v2, /device:TPU:1, one launch (start us, length us, event | category | flops | bytes accessed | tf_op | source)
XLA Modules:
  0.0 63.9 jit_solution(5104261369359237246)
XLA Ops:
  0.0 0.0 copy-start.2
  0.0 0.9 %copy-done.2 = bf16[256,256]{1,0:T(8,128)(2,1)S(1)} copy-done((bf16[256,256]{1,0:T(8,128)(2,1)S(1)}, bf16[256,256]{1,0:T(8,128)(2,1)}, u32[]{:S(2)}) %copy-start.2) | copy-done | bytes 131096
  0.9 0.0 copy-start.3
  0.9 0.9 %copy-done.3 = bf16[256,256]{1,0:T(8,128)(2,1)S(1)} copy-done((bf16[256,256]{1,0:T(8,128)(2,1)S(1)}, bf16[256,256]{1,0:T(8,128)(2,1)}, u32[]{:S(2)}) %copy-start.3) | copy-done | bytes 131096
  1.8 0.0 copy-start.4
  1.8 0.9 %copy-done.4 = bf16[256,256]{1,0:T(8,128)(2,1)S(1)} copy-done((bf16[256,256]{1,0:T(8,128)(2,1)S(1)}, bf16[256,256]{1,0:T(8,128)(2,1)}, u32[]{:S(2)}) %copy-start.4) | copy-done | bytes 131096
  2.7 0.0 copy-start.6
  2.7 0.7 %copy-done.6 = bf16[16,256]{1,0:T(8,128)(2,1)S(1)} copy-done((bf16[16,256]{1,0:T(8,128)(2,1)S(1)}, bf16[16,256]{1,0:T(8,128)(2,1)}, u32[]{:S(2)}) %copy-start.6) | copy-done | bytes 8216
  3.4 0.0 copy-start.7
  3.4 0.7 %copy-done.7 = f32[256]{0:T(256)S(1)} copy-done((f32[256]{0:T(256)S(1)}, f32[256]{0:T(256)}, u32[]{:S(2)}) %copy-start.7) | copy-done | bytes 1048
  4.1 0.9 %project.1 = f32[16,40,128]{2,1,0:T(8,128)} custom-call(bf16[16,256]{1,0:T(8,128)(2,1)S(1)} %copy-done.6, f32[1,256]{1,0:T(1,128)S(1)} %bitcast.11, bf16[256,256]{1,0:T(8,128)(2,1)S(1)} %copy-done.2, bf16[256,256]{1,0:T(8,128)(2,1)S(1)} %copy-done.3, bf16[256,256]{1,0:T(8,128)(2,1)S(1)} %copy-done.4), custom_call_target="tpu_custom_call" | custom-call | tf_op jit(solution)/shard_map/project/pallas_call | solution.py:243
  5.0 8.6 %all-to-all-start = ((f32[16,40,128]{2,1,0:T(8,128)}), f32[16,40,128]{2,1,0:T(8,128)S(1)}, u32[]{:S(2)}, u32[]{:S(2)}) async-start(f32[16,40,128]{2,1,0:T(8,128)} %project.1), calls=%async_computation | async-start | bytes 655360 | tf_op jit(solution)/shard_map/all_to_all | solution.py:251
  13.6 0.7 %and_select_fusion = (s32[16]{0:T(128)S(1)}, f32[16]{0:T(128)S(1)}) fusion(s32[16]{0:T(128)} %lengths.1), kind=kLoop, calls=%fused_computation.4 | loop fusion | flops 256 | bytes 192 | tf_op jit(solution)/shard_map/jit(floor_divide)/jit(_where)/select_n | solution.py:286
  14.4 0.1 fusion
  14.5 0.1 tile.29.cosine
  14.6 0.1 pad_maximum_fusion
  14.7 0.1 tile.31.sine
  14.8 0.1 broadcast_in_dim.2
  14.8 0.1 reshape.71
  14.9 7.2 %all-to-all-done.got = f32[16,40,128]{2,1,0:T(8,128)S(1)} async-done(((f32[16,40,128]{2,1,0:T(8,128)}), f32[16,40,128]{2,1,0:T(8,128)S(1)}, u32[]{:S(2)}, u32[]{:S(2)}) %all-to-all-start) | async-done | bytes 327712 | tf_op jit(solution)/shard_map/all_to_all | solution.py:251
  22.1 0.0 copy-start
  22.1 3.4 %copy-done = bf16[16,1024,2,128]{3,2,1,0:T(2,128)(2,1)S(1)} copy-done((bf16[16,1024,2,128]{3,2,1,0:T(2,128)(2,1)S(1)}, bf16[16,1024,2,128]{3,2,1,0:T(2,128)(2,1)}, u32[]{:S(2)}) %copy-start) | copy-done | bytes 8388632
  25.5 0.0 copy-start.1
  25.5 3.4 %copy-done.1 = bf16[16,1024,2,128]{3,2,1,0:T(2,128)(2,1)S(1)} copy-done((bf16[16,1024,2,128]{3,2,1,0:T(2,128)(2,1)S(1)}, bf16[16,1024,2,128]{3,2,1,0:T(2,128)(2,1)}, u32[]{:S(2)}) %copy-start.1) | copy-done | bytes 8388632
  28.9 0.0 copy-start.8
  28.9 0.7 %copy-done.8 = s32[16]{0:T(128)S(1)} copy-done((s32[16]{0:T(128)S(1)}, s32[16]{0:T(128)}, u32[]{:S(2)}) %copy-start.8) | copy-done | bytes 88
  29.6 0.0 copy-start.10
  29.6 0.0 copy-start.5
  29.6 0.0 copy-start.9
  29.6 9.4 %attend.1 = bf16[16,80,128]{2,1,0:T(8,128)(2,1)} custom-call(s32[16]{0:T(128)S(1)} %copy-done.8, s32[1]{0:T(128)} %bitcast.own, f32[16,40,128]{2,1,0:T(8,128)S(1)} %all-to-all-done.got, f32[16,128]{1,0:T(8,128)S(1)} %tile.29.cosine, f32[16,128]{1,0:T(8,128)S(1)} %tile.31.sine, bf16[16,2048,128]{2,1,0:T(8,128)(2,1)S(1)} %bitcast.9, ...), custom_call_target="tpu_custom_call" | custom-call | tf_op jit(solution)/shard_map/attend/pallas_call | solution.py:260
  39.0 3.6 %all-to-all-start.1 = ((bf16[16,80,128]{2,1,0:T(8,128)(2,1)}), bf16[16,80,128]{2,1,0:T(8,128)(2,1)S(1)}, u32[]{:S(2)}, u32[]{:S(2)}) async-start(bf16[16,80,128]{2,1,0:T(8,128)(2,1)} %attend.1), calls=%async_computation.1 | async-start | bytes 655360 | tf_op jit(solution)/shard_map/all_to_all | solution.py:285
  42.5 0.0 copy-done.10
  42.5 0.1 copy.14
  42.6 0.1 stack.7.clone
  42.7 0.1 tile.32
  42.8 0.1 tile.34.share
  42.9 7.6 %all-to-all-done.1.got = bf16[16,80,128]{2,1,0:T(8,128)(2,1)S(1)} async-done(((bf16[16,80,128]{2,1,0:T(8,128)(2,1)}), bf16[16,80,128]{2,1,0:T(8,128)(2,1)S(1)}, u32[]{:S(2)}, u32[]{:S(2)}) %all-to-all-start.1) | async-done | bytes 327712 | tf_op jit(solution)/shard_map/all_to_all | solution.py:285
  50.5 0.0 copy-done.5
  50.5 0.0 copy-done.9
  50.5 0.6 finish.1
  51.1 12.2 %all_to_all.15 = f32[8,16,256]{2,1,0:T(8,128)S(1)} all-to-all(f32[8,16,256]{2,1,0:T(8,128)S(1)} %finish.1), channel_id=1, replica_groups=mesh['kv'=16,'tp'=8] {'tp'}, dimensions={0} | all-to-all | bytes 262144 | tf_op jit(solution)/shard_map/all_to_all | solution.py:299
  63.3 0.6 reduce_sum.9
  (6 shorter events, 0.0 us)
Async XLA Ops:
  0.0 0.9 %copy-start.2 = (bf16[256,256]{1,0:T(8,128)(2,1)S(1)}, bf16[256,256]{1,0:T(8,128)(2,1)}, u32[]{:S(2)}) copy-start(bf16[256,256]{1,0:T(8,128)(2,1)} %query_weight.1) | copy-start | bytes 393220
  0.9 0.9 %copy-start.3 = (bf16[256,256]{1,0:T(8,128)(2,1)S(1)}, bf16[256,256]{1,0:T(8,128)(2,1)}, u32[]{:S(2)}) copy-start(bf16[256,256]{1,0:T(8,128)(2,1)} %key_weight.1) | copy-start | bytes 393220
  1.8 0.9 %copy-start.4 = (bf16[256,256]{1,0:T(8,128)(2,1)S(1)}, bf16[256,256]{1,0:T(8,128)(2,1)}, u32[]{:S(2)}) copy-start(bf16[256,256]{1,0:T(8,128)(2,1)} %value_weight.1) | copy-start | bytes 393220
  2.7 0.7 %copy-start.6 = (bf16[16,256]{1,0:T(8,128)(2,1)S(1)}, bf16[16,256]{1,0:T(8,128)(2,1)}, u32[]{:S(2)}) copy-start(bf16[16,256]{1,0:T(8,128)(2,1)} %tokens.1) | copy-start | bytes 24580
  3.4 0.7 %copy-start.7 = (f32[256]{0:T(256)S(1)}, f32[256]{0:T(256)}, u32[]{:S(2)}) copy-start(f32[256]{0:T(256)} %param.12) | copy-start | bytes 3076
  5.0 17.1 %all-to-all-start = ((f32[16,40,128]{2,1,0:T(8,128)}), f32[16,40,128]{2,1,0:T(8,128)S(1)}, u32[]{:S(2)}, u32[]{:S(2)}) async-start(f32[16,40,128]{2,1,0:T(8,128)} %project.1), calls=%async_computation | async-start | bytes 655360 | tf_op jit(solution)/shard_map/all_to_all | solution.py:251
  22.1 3.4 %copy-start = (bf16[16,1024,2,128]{3,2,1,0:T(2,128)(2,1)S(1)}, bf16[16,1024,2,128]{3,2,1,0:T(2,128)(2,1)}, u32[]{:S(2)}) copy-start(bf16[16,1024,2,128]{3,2,1,0:T(2,128)(2,1)} %param.20) | copy-start | bytes 25165828
  25.5 3.4 %copy-start.1 = (bf16[16,1024,2,128]{3,2,1,0:T(2,128)(2,1)S(1)}, bf16[16,1024,2,128]{3,2,1,0:T(2,128)(2,1)}, u32[]{:S(2)}) copy-start(bf16[16,1024,2,128]{3,2,1,0:T(2,128)(2,1)} %param.21) | copy-start | bytes 25165828
  28.9 0.7 %copy-start.8 = (s32[16]{0:T(128)S(1)}, s32[16]{0:T(128)}, u32[]{:S(2)}) copy-start(s32[16]{0:T(128)} %lengths.1) | copy-start | bytes 196
  29.6 13.0 %copy-start.10 = (f32[2]{0:T(128)S(1)}, f32[2]{0:T(128)}, u32[]{:S(2)}) copy-start(f32[2]{0:T(128)} %param.17) | copy-start | bytes 28
  29.6 20.9 %copy-start.5 = (bf16[256,256]{1,0:T(8,128)(2,1)S(1)}, bf16[256,256]{1,0:T(8,128)(2,1)}, u32[]{:S(2)}) copy-start(bf16[256,256]{1,0:T(8,128)(2,1)} %out_weight.1) | copy-start | bytes 393220
  29.6 20.9 %copy-start.9 = (f32[128]{0:T(128)S(1)}, f32[128]{0:T(128)}, u32[]{:S(2)}) copy-start(f32[128]{0:T(128)} %param.18) | copy-start | bytes 1540
  39.0 11.5 %all-to-all-start.1 = ((bf16[16,80,128]{2,1,0:T(8,128)(2,1)}), bf16[16,80,128]{2,1,0:T(8,128)(2,1)S(1)}, u32[]{:S(2)}, u32[]{:S(2)}) async-start(bf16[16,80,128]{2,1,0:T(8,128)(2,1)} %attend.1), calls=%async_computation.1 | async-start | bytes 655360 | tf_op jit(solution)/shard_map/all_to_all | solution.py:285

commit v3 on v2

--- a/solution.py
+++ b/solution.py
@@ -17,25 +17,45 @@
 
 VM = pl.BlockSpec(memory_space=pltpu.VMEM)
 SM = pl.BlockSpec(memory_space=pltpu.SMEM)
-ANY = pl.BlockSpec(memory_space=pl.ANY)
+ANY = pl.BlockSpec(memory_space=pltpu.HBM)
 F32 = jnp.float32
 BF16 = jnp.bfloat16
 SMALL = pltpu.CompilerParams(vmem_limit_bytes=8 * 1024 * 1024)
 BIG = pltpu.CompilerParams(vmem_limit_bytes=30 * 1024 * 1024)
 
 
+def in_hbm(x):
+    return pltpu.with_memory_space_constraint(x, pltpu.HBM)
+
+
 def iotas(rows):
     shape = (rows, LANES)
     return lax.broadcasted_iota(jnp.int32, shape, 0), lax.broadcasted_iota(jnp.int32, shape, 1)
 
 
-def project_kernel(tokens, gain, query_weight, key_weight, value_weight, out):
+def project_kernel(
+    tokens_in, gain_in, query_in, key_in, value_in, out, tokens, gain, weights, small, large
+):
+    near = (
+        pltpu.make_async_copy(tokens_in, tokens, small.at[0]),
+        pltpu.make_async_copy(gain_in, gain, small.at[1]),
+    )
+    far = [
+        pltpu.make_async_copy(source, weights.at[n], large.at[n])
+        for n, source in enumerate((query_in, key_in, value_in))
+    ]
+    for copy in (*near, *far):
+        copy.start()
+    for copy in near:
+        copy.wait()
     widened = tokens[...].astype(F32)
     squares = jnp.sum(widened * widened, axis=1, keepdims=True)
     normed = (widened * gain[...]).astype(BF16)
-    query = jnp.dot(normed, query_weight[...], preferred_element_type=F32)
-    key = jnp.dot(normed, key_weight[...], preferred_element_type=F32)
-    value = jnp.dot(normed, value_weight[...], preferred_element_type=F32)
+    products = []
+    for n in range(3):
+        far[n].wait()
+        products.append(jnp.dot(normed, weights[n], preferred_element_type=F32))
+    query, key, value = products
     row, lane = iotas(SEQS)
     square_row = jnp.sum(jnp.where(row == lane, squares, 0.0), axis=0, keepdims=True)
     blank = jnp.zeros((3, LANES), F32)
@@ -64,7 +84,7 @@
 
 
 def attend_kernel(
-    lengths, own, got, cosine, sine, keys_in, values_in, out, keys, values, arrived, query_rows,
+    own, limits, got, cosine, sine, keys_in, values_in, out, keys, values, arrived, query_rows,
     scale_rows, score_rows, weight_rows
 ):
     copies = []
@@ -76,7 +96,6 @@
     for copy in copies:
         copy.start()
     me = own[0]
-    base = me * 1024
     summed = jnp.sum(got[...], axis=0)
     row, lane = iotas(SEQS)
     squares = jnp.sum(jnp.where(row == lane, summed[32:33, :], 0.0), axis=1, keepdims=True)
@@ -89,7 +108,6 @@
         query_rows[head * SEQS : (head + 1) * SEQS, :] = turned_query.astype(F32)
     sub, lane8 = iotas(8)
     map_lanes = (lane8 // DH) == (sub % 2)
-    limits = []
     for pair in range(SEQS // 2):
         first, second = 2 * pair, 2 * pair + 1
 
@@ -116,10 +134,7 @@
     for pair in range(SEQS // 2):
         first, second = 2 * pair, 2 * pair + 1
         at = slice(pair * 8, pair * 8 + 8)
-        limit = jnp.where(
-            subs[:, :1] < 4, 2 * (lengths[first] - base), 2 * (lengths[second] - base)
-        )
-        visible = own_head & (columns < limit)
+        visible = own_head & (columns < limits[at, :1])
         masked = jnp.where(visible, score_rows[at, :] * DH ** (-0.5), floor_value)
         highest = jnp.max(masked, axis=1, keepdims=True)
         weights = jnp.where(visible, jnp.exp(masked - highest), 0.0).astype(BF16)
@@ -242,12 +257,25 @@
 ):
     sent = pl.pallas_call(
         project_kernel,
-        in_specs=[VM] * 5,
+        in_specs=[ANY] * 5,
         out_specs=VM,
         out_shape=jax.ShapeDtypeStruct((SEQS, 40, LANES), F32),
+        scratch_shapes=[
+            pltpu.VMEM((SEQS, 256), BF16),
+            pltpu.VMEM((1, 256), F32),
+            pltpu.VMEM((3, 256, 256), BF16),
+            pltpu.SemaphoreType.DMA((2,)),
+            pltpu.SemaphoreType.DMA((3,)),
+        ],
         compiler_params=SMALL,
         name="project",
-    )(tokens, norm_gain.reshape(1, -1), query_weight, key_weight, value_weight)
+    )(
+        in_hbm(tokens),
+        in_hbm(norm_gain.reshape(1, -1)),
+        in_hbm(query_weight),
+        in_hbm(key_weight),
+        in_hbm(value_weight),
+    )
     got = lax.all_to_all(sent, "kv", split_axis=0, concat_axis=0, tiled=True)
     cache_shape = (SEQS, 2048, LANES)
     halfway = DH // 2
@@ -257,9 +285,12 @@
     sine = jnp.sin(angles)
     sine = jnp.tile(jnp.concatenate([-sine, sine], axis=1), (1, 2))
     own = lax.axis_index("kv").astype(jnp.int32).reshape(1)
+    limits = jnp.broadcast_to(
+        jnp.repeat(2 * (lengths - own * 1024), 4).reshape(64, 1), (64, LANES)
+    )
     shared = pl.pallas_call(
         attend_kernel,
-        in_specs=[SM, SM, VM, VM, VM, ANY, ANY],
+        in_specs=[SM, VM, VM, VM, VM, ANY, ANY],
         out_specs=VM,
         out_shape=jax.ShapeDtypeStruct((SEQS, 80, LANES), BF16),
         scratch_shapes=[
@@ -274,13 +305,13 @@
         compiler_params=BIG,
         name="attend",
     )(
-        lengths,
         own,
+        limits,
         got,
         cosine,
         sine,
-        key_cache.reshape(cache_shape),
-        value_cache.reshape(cache_shape),
+        in_hbm(key_cache.reshape(cache_shape)),
+        in_hbm(value_cache.reshape(cache_shape)),
     )
     everyone = lax.all_to_all(shared, "kv", split_axis=0, concat_axis=0, tiled=True)
     block = jnp.pad(jnp.repeat(lengths // 1024, 4), (0, 64)).reshape(1, LANES)

time: 64.5 us -> 53.5 us (0.83)
  local copies, waits for them, and re-layouts: 12.2 us -> 0.94 us
  Pallas kernels: 10.9 us -> 11.6 us
    unnamed x23 -> x7, local copies, waits for them, and re-layouts: 11.6 us -> 0.1 us
    pallas_call x2, Pallas kernels: 10.3 us -> 11 us  [the longest x1 8.85 us: local(): pl.pallas_call(attend_kernel, in_specs=[SM, VM, VM, VM, VM, ANY, ANY], ou...]
where the time goes in v3:
time: 53.5 us; the launch traced here: 53.2 us
  waiting for transfers between devices  14.6 us (27%)
  starting transfers between devices  12.2 us (23%)
  blocking collectives  12.2 us (23%)
  Pallas kernels  11.6 us (22%)
  other arithmetic  1.56 us (3%)
  local copies, waits for them, and re-layouts  0.94 us (2%)
    all_to_all x1, blocking collectives, local(): lax.all_to_all(partial_out, 'tp', split_axis=0, concat_axis=0, tiled=True)  12.2 us
    pallas_call x1, Pallas kernels, local(): pl.pallas_call(attend_kernel, in_specs=[SM, VM, VM, VM, VM, ANY, ANY], ou...  8.85 us
    all_to_all x1, starting transfers between devices, local(): got = lax.all_to_all(sent, 'kv', split_axis=0, concat_axis=0, tiled=True)  8.6 us
    all_to_all x1, waiting for transfers between devices, local(): lax.all_to_all(shared, 'kv', split_axis=0, concat_axis=0, tiled=True)  7.56 us
    all_to_all x1, waiting for transfers between devices, local(): got = lax.all_to_all(sent, 'kv', split_axis=0, concat_axis=0, tiled=True)  7.05 us
    all_to_all x1, starting transfers between devices, local(): lax.all_to_all(shared, 'kv', split_axis=0, concat_axis=0, tiled=True)  3.55 us
    pallas_call x1, Pallas kernels, local(): pl.pallas_call(project_kernel, in_specs=[ANY] * 5, out_specs=VM, out_shap...  2.14 us
  transfers between devices with their start and end apart: 2, of which 2 were waited for; matrix products, arithmetic and copies ran while one was open for 3% of the time, Pallas kernels for 0%

profile of v3, /device:TPU:1, one launch (start us, length us, event | category | flops | bytes accessed | tf_op | source)
XLA Modules:
  0.0 53.2 jit_solution(12003055488913438646)
XLA Ops:
  0.0 2.1 %project.1 = f32[16,40,128]{2,1,0:T(8,128)} custom-call(bf16[16,256]{1,0:T(8,128)(2,1)} %tokens_in.1, f32[1,256]{1,0:T(1,128)} %bitcast.13, bf16[256,256]{1,0:T(8,128)(2,1)} %query_in.1, bf16[256,256]{1,0:T(8,128)(2,1)} %key_in.1, bf16[256,256]{1,0:T(8,128)(2,1)} %value_in.1), custom_call_target="tpu_custom_call" | custom-call | tf_op jit(solution)/shard_map/project/pallas_call | solution.py:258
  2.2 8.6 %all-to-all-start = ((f32[16,40,128]{2,1,0:T(8,128)}), f32[16,40,128]{2,1,0:T(8,128)S(1)}, u32[]{:S(2)}, u32[]{:S(2)}) async-start(f32[16,40,128]{2,1,0:T(8,128)} %project.1), calls=%async_computation | async-start | bytes 655360 | tf_op jit(solution)/shard_map/all_to_all | solution.py:279
  10.8 0.7 %and_select_fusion = (s32[16]{0:T(128)S(1)}, s32[16]{0:T(128)S(1)}, f32[16]{0:T(128)S(1)}) fusion(s32[16]{0:T(128)} %param.19, s32[]{:T(128)} %bitcast.1), kind=kLoop, calls=%fused_computation.4 | loop fusion | flops 288 | bytes 260 | tf_op jit(solution)/shard_map/jit(floor_divide)/jit(_where)/select_n | solution.py:317
  11.5 0.1 broadcast_in_dim.15
  11.6 0.1 broadcast_in_dim.16
  11.7 0.1 fusion
  11.8 0.1 tile.29.cosine
  11.9 0.1 pad_maximum_fusion
  12.0 0.1 tile.31.sine
  12.1 0.1 broadcast_in_dim.18
  12.1 0.1 reshape.72
  12.2 7.0 %all-to-all-done.got = f32[16,40,128]{2,1,0:T(8,128)S(1)} async-done(((f32[16,40,128]{2,1,0:T(8,128)}), f32[16,40,128]{2,1,0:T(8,128)S(1)}, u32[]{:S(2)}, u32[]{:S(2)}) %all-to-all-start) | async-done | bytes 327712 | tf_op jit(solution)/shard_map/all_to_all | solution.py:279
  19.3 0.1 broadcast_in_dim.17.limits
  19.4 0.0 copy-start.2
  19.4 0.0 copy-start
  19.4 0.0 copy-start.1
  19.4 8.8 %attend.1 = bf16[16,80,128]{2,1,0:T(8,128)(2,1)} custom-call(s32[1]{0:T(128)} %bitcast.own, s32[64,128]{1,0:T(8,128)S(1)} %broadcast_in_dim.17.limits, f32[16,40,128]{2,1,0:T(8,128)S(1)} %all-to-all-done.got, f32[16,128]{1,0:T(8,128)S(1)} %tile.29.cosine, f32[16,128]{1,0:T(8,128)S(1)} %tile.31.sine, bf16[16,2048,128]{2,1,0:T(8,128)(2,1)} %bitcast.11, ...), custom_call_target="tpu_custom_call" | custom-call | tf_op jit(solution)/shard_map/attend/pallas_call | solution.py:291
  28.2 3.6 %all-to-all-start.1 = ((bf16[16,80,128]{2,1,0:T(8,128)(2,1)}), bf16[16,80,128]{2,1,0:T(8,128)(2,1)S(1)}, u32[]{:S(2)}, u32[]{:S(2)}) async-start(bf16[16,80,128]{2,1,0:T(8,128)(2,1)} %attend.1), calls=%async_computation.1 | async-start | bytes 655360 | tf_op jit(solution)/shard_map/all_to_all | solution.py:316
  31.8 0.0 copy-done.2
  31.8 0.1 copy.14
  31.9 0.1 stack.7.clone
  32.0 0.1 tile.32
  32.1 0.1 tile.34.share
  32.2 7.6 %all-to-all-done.1.got = bf16[16,80,128]{2,1,0:T(8,128)(2,1)S(1)} async-done(((bf16[16,80,128]{2,1,0:T(8,128)(2,1)}), bf16[16,80,128]{2,1,0:T(8,128)(2,1)S(1)}, u32[]{:S(2)}, u32[]{:S(2)}) %all-to-all-start.1) | async-done | bytes 327712 | tf_op jit(solution)/shard_map/all_to_all | solution.py:316
  39.7 0.0 copy-done
  39.7 0.0 copy-done.1
  39.8 0.6 %finish.1 = f32[8,16,256]{2,1,0:T(8,128)S(1)} custom-call(bf16[16,80,128]{2,1,0:T(8,128)(2,1)S(1)} %all-to-all-done.1.got, s32[1,128]{1,0:T(1,128)S(1)} %pad_bitcast_fusion.block, f32[1,128]{1,0:T(1,128)S(1)} %tile.34.share, f32[1,128]{1,0:T(1,128)S(1)} %bitcast.10, bf16[256,256]{1,0:T(8,128)(2,1)S(1)} %copy-done), custom_call_target="tpu_custom_call" | custom-call | tf_op jit(solution)/shard_map/finish/pallas_call | solution.py:321
  40.4 12.2 %all_to_all.15 = f32[8,16,256]{2,1,0:T(8,128)S(1)} all-to-all(f32[8,16,256]{2,1,0:T(8,128)S(1)} %finish.1), channel_id=1, replica_groups=mesh['kv'=16,'tp'=8] {'tp'}, dimensions={0} | all-to-all | bytes 262144 | tf_op jit(solution)/shard_map/all_to_all | solution.py:330
  52.6 0.6 %reduce_sum.9 = bf16[16,256]{1,0:T(8,128)(2,1)} reduce(f32[8,16,256]{2,1,0:T(8,128)S(1)} %all_to_all.15, f32[]{:T(128)} %constant.35.clone.1), dimensions={0}, to_apply=%region_0.1 | reduce | flops 28672 | bytes 139268 | tf_op jit(solution)/shard_map/reduce_sum | solution.py:331
  (6 shorter events, 0.0 us)
Async XLA Ops:
  2.2 17.1 %all-to-all-start = ((f32[16,40,128]{2,1,0:T(8,128)}), f32[16,40,128]{2,1,0:T(8,128)S(1)}, u32[]{:S(2)}, u32[]{:S(2)}) async-start(f32[16,40,128]{2,1,0:T(8,128)} %project.1), calls=%async_computation | async-start | bytes 655360 | tf_op jit(solution)/shard_map/all_to_all | solution.py:279
  19.4 12.4 %copy-start.2 = (f32[2]{0:T(128)S(1)}, f32[2]{0:T(128)}, u32[]{:S(2)}) copy-start(f32[2]{0:T(128)} %param.17) | copy-start | bytes 28
  19.4 20.4 %copy-start = (bf16[256,256]{1,0:T(8,128)(2,1)S(1)}, bf16[256,256]{1,0:T(8,128)(2,1)}, u32[]{:S(2)}) copy-start(bf16[256,256]{1,0:T(8,128)(2,1)} %out_weight.1) | copy-start | bytes 393220
  19.4 20.4 %copy-start.1 = (f32[128]{0:T(128)S(1)}, f32[128]{0:T(128)}, u32[]{:S(2)}) copy-start(f32[128]{0:T(128)} %param.18) | copy-start | bytes 1540
  28.2 11.5 %all-to-all-start.1 = ((bf16[16,80,128]{2,1,0:T(8,128)(2,1)}), bf16[16,80,128]{2,1,0:T(8,128)(2,1)S(1)}, u32[]{:S(2)}, u32[]{:S(2)}) async-start(bf16[16,80,128]{2,1,0:T(8,128)(2,1)} %attend.1), calls=%async_computation.1 | async-start | bytes 655360 | tf_op jit(solution)/shard_map/all_to_all | solution.py:316

commit v4 on v3

--- a/solution.py
+++ b/solution.py
@@ -1,5 +1,6 @@
 import jax
 import jax.numpy as jnp
+import numpy as np
 from jax import lax
 from jax.experimental import pallas as pl
 from jax.experimental.pallas import tpu as pltpu
@@ -14,6 +15,7 @@
 epsilon = 1e-05
 theta_base = 500000.0
 floor_value = -1e30
+AHEAD = 10
 
 VM = pl.BlockSpec(memory_space=pltpu.VMEM)
 SM = pl.BlockSpec(memory_space=pltpu.SMEM)
@@ -34,12 +36,21 @@
 
 
 def project_kernel(
-    tokens_in, gain_in, query_in, key_in, value_in, out, tokens, gain, weights, small, large
+    tokens_in, gain_in, lengths_in, lambdas_in, rates_in, query_in, key_in, value_in, out, tables,
+    tokens, gain, lengths, lambdas, rates, weights, small, large,
 ):
-    near = (
-        pltpu.make_async_copy(tokens_in, tokens, small.at[0]),
-        pltpu.make_async_copy(gain_in, gain, small.at[1]),
-    )
+    near = [
+        pltpu.make_async_copy(source, target, small.at[n])
+        for n, (source, target) in enumerate(
+            (
+                (tokens_in, tokens),
+                (gain_in, gain),
+                (lengths_in, lengths),
+                (lambdas_in, lambdas),
+                (rates_in, rates),
+            )
+        )
+    ]
     far = [
         pltpu.make_async_copy(source, weights.at[n], large.at[n])
         for n, source in enumerate((query_in, key_in, value_in))
@@ -51,13 +62,31 @@
     widened = tokens[...].astype(F32)
     squares = jnp.sum(widened * widened, axis=1, keepdims=True)
     normed = (widened * gain[...]).astype(BF16)
+    row, lane = iotas(SEQS)
+    square_row = jnp.sum(jnp.where(row == lane, squares, 0.0), axis=0, keepdims=True)
+    row16 = lax.broadcasted_iota(jnp.int32, (SEQS, SEQS), 0)
+    lane16 = lax.broadcasted_iota(jnp.int32, (SEQS, SEQS), 1)
+    held = lengths[...].astype(F32)
+    held_column = jnp.sum(jnp.where(row16 == lane16, held, 0.0), axis=1, keepdims=True)
+    angles = held_column * rates[...]
+    tables[0:16, :] = jnp.cos(angles)
+    sine = jnp.sin(angles)
+    tables[16:32, :] = jnp.where((lane // 32) % 2 == 0, -sine, sine)
+    lane1 = lax.broadcasted_iota(jnp.int32, (1, LANES), 1)
+    lambda_row = jnp.where((lane1 // 2) % 2 == 0, lambdas[:, 0:1], lambdas[:, 1:2])
+    tables[32:40, :] = jnp.concatenate(
+        [
+            jnp.sum(jnp.where(row == lane // 4, held_column, 0.0), axis=0, keepdims=True),
+            jnp.where(lane1 % 2 == 0, 1.0, -lambda_row),
+            jnp.zeros((6, LANES), F32),
+        ],
+        axis=0,
+    )
     products = []
     for n in range(3):
         far[n].wait()
         products.append(jnp.dot(normed, weights[n], preferred_element_type=F32))
     query, key, value = products
-    row, lane = iotas(SEQS)
-    square_row = jnp.sum(jnp.where(row == lane, squares, 0.0), axis=0, keepdims=True)
     blank = jnp.zeros((3, LANES), F32)
     for dest in range(SEQS):
         out[dest, 0:16, :] = query[:, :LANES]
@@ -84,8 +113,8 @@
 
 
 def attend_kernel(
-    own, limits, got, cosine, sine, keys_in, values_in, out, keys, values, arrived, query_rows,
-    scale_rows, score_rows, weight_rows
+    tables, got, keys_in, values_in, out, keys, values, arrived, query_rows, scale_rows,
+    score_rows, weight_rows,
 ):
     copies = []
     for kind, (source, target) in enumerate(((keys_in, keys), (values_in, values))):
@@ -93,9 +122,17 @@
             copies.append(
                 pltpu.make_async_copy(source.at[seq], target.at[seq], arrived.at[kind, seq])
             )
-    for copy in copies:
+    for copy in copies[:AHEAD]:
         copy.start()
-    me = own[0]
+
+    def arrive(kind, seq):
+        at = kind * SEQS + seq
+        copies[at].wait()
+        if at + AHEAD < 2 * SEQS:
+            copies[at + AHEAD].start()
+
+    me = lax.axis_index("kv")
+    cosine, sine = tables[0:16, :], tables[16:32, :]
     summed = jnp.sum(got[...], axis=0)
     row, lane = iotas(SEQS)
     squares = jnp.sum(jnp.where(row == lane, summed[32:33, :], 0.0), axis=1, keepdims=True)
@@ -103,7 +140,7 @@
     scale_rows[...] = scaling
     for head in range(HEADS):
         turned_query = turned(
-            summed[16 * head : 16 * head + 16, :] * scaling, cosine[...], sine[...]
+            summed[16 * head : 16 * head + 16, :] * scaling, cosine, sine
         )
         query_rows[head * SEQS : (head + 1) * SEQS, :] = turned_query.astype(F32)
     sub, lane8 = iotas(8)
@@ -120,8 +157,8 @@
         right = jnp.where(sub < 6, row_of(0, second), row_of(1, second))
         right = jnp.where(map_lanes & (sub >= 4), right, 0.0)
         queries = jnp.concatenate([left, right], axis=1).astype(BF16)
-        copies[first].wait()
-        copies[second].wait()
+        arrive(0, first)
+        arrive(0, second)
         both_keys = jnp.concatenate([keys[first], keys[second]], axis=1)
         score_rows[pair * 8 : pair * 8 + 8, :] = lax.dot_general(
             queries, both_keys, (((1,), (1,)), ((), ())), preferred_element_type=F32
@@ -134,7 +171,10 @@
     for pair in range(SEQS // 2):
         first, second = 2 * pair, 2 * pair + 1
         at = slice(pair * 8, pair * 8 + 8)
-        visible = own_head & (columns < limits[at, :1])
+        limit = jnp.sum(
+            jnp.where(lane8 == pair * 8 + sub, tables[32:33, :], 0.0), axis=1, keepdims=True
+        ).astype(jnp.int32)
+        visible = own_head & (columns < 2 * (limit - me * 1024))
         masked = jnp.where(visible, score_rows[at, :] * DH ** (-0.5), floor_value)
         highest = jnp.max(masked, axis=1, keepdims=True)
         weights = jnp.where(visible, jnp.exp(masked - highest), 0.0).astype(BF16)
@@ -144,8 +184,8 @@
         maxima = maxima + jnp.where(place, highest, 0.0)
         totals = totals + jnp.where(place, total, 0.0)
     scale = scale_rows[pl.ds(me, 1), :]
-    row_cosine = cosine[pl.ds(me, 1), :]
-    row_sine = sine[pl.ds(me, 1), :]
+    row_cosine = tables[pl.ds(me, 1), :]
+    row_sine = tables[pl.ds(SEQS + me, 1), :]
     lane1 = lax.broadcasted_iota(jnp.int32, (1, LANES), 1)
     fresh_scores = jnp.zeros((1, LANES), F32)
     for head in range(HEADS):
@@ -175,8 +215,8 @@
         parts = []
         for pair in (2 * two, 2 * two + 1):
             first, second = 2 * pair, 2 * pair + 1
-            copies[SEQS + first].wait()
-            copies[SEQS + second].wait()
+            arrive(1, first)
+            arrive(1, second)
             both_values = jnp.concatenate([values[first], values[second]], axis=1)
             valued = jnp.dot(
                 weight_rows[pair * 8 : pair * 8 + 8, :],
@@ -195,7 +235,7 @@
     return high, middle, x - high - middle
 
 
-def finish_kernel(got, block, share, head_gain, out_weight, out, factors, joined):
+def finish_kernel(got, tables, head_gain, out_weight, out, factors, joined):
     rows16, _ = iotas(SEQS)
     tails = got[:, 64:80, :].astype(F32)
 
@@ -205,15 +245,16 @@
     maxima = whole(0)
     totals = whole(3)
     fresh = jnp.sum(whole(6), axis=0, keepdims=True)
+    block = tables[32:33, :].astype(jnp.int32) // 1024
     in_block = jnp.max(
-        jnp.where(rows16 == block[...], maxima, floor_value), axis=0, keepdims=True
+        jnp.where(rows16 == block, maxima, floor_value), axis=0, keepdims=True
     )
     in_block = jnp.maximum(in_block, fresh)
     top = jnp.maximum(jnp.max(maxima, axis=0, keepdims=True), fresh)
     factor = jnp.exp(maxima - top)
     fresh_factor = jnp.exp(fresh - in_block).astype(BF16).astype(F32) * jnp.exp(in_block - top)
     total = jnp.sum(totals * factor, axis=0, keepdims=True) + fresh_factor
-    part = share[...] / total
+    part = tables[33:34, :] / total
     factors[...] = jnp.zeros((LANES, LANES), F32)
     factors[0:SEQS, :] = factor * part
     factors[SEQS : SEQS + 1, :] = fresh_factor * part
@@ -255,16 +296,23 @@
     key_cache,
     value_cache,
 ):
-    sent = pl.pallas_call(
+    rates = np.tile(theta_base ** (-np.arange(DH // 2) / (DH // 2)), 4)
+    sent, tables = pl.pallas_call(
         project_kernel,
-        in_specs=[ANY] * 5,
-        out_specs=VM,
-        out_shape=jax.ShapeDtypeStruct((SEQS, 40, LANES), F32),
+        in_specs=[ANY] * 8,
+        out_specs=[VM, VM],
+        out_shape=[
+            jax.ShapeDtypeStruct((SEQS, 40, LANES), F32),
+            jax.ShapeDtypeStruct((40, LANES), F32),
+        ],
         scratch_shapes=[
             pltpu.VMEM((SEQS, 256), BF16),
             pltpu.VMEM((1, 256), F32),
+            pltpu.VMEM((1, SEQS), jnp.int32),
+            pltpu.VMEM((1, HEADS), F32),
+            pltpu.VMEM((1, LANES), F32),
             pltpu.VMEM((3, 256, 256), BF16),
-            pltpu.SemaphoreType.DMA((2,)),
+            pltpu.SemaphoreType.DMA((5,)),
             pltpu.SemaphoreType.DMA((3,)),
         ],
         compiler_params=SMALL,
@@ -272,25 +320,18 @@
     )(
         in_hbm(tokens),
         in_hbm(norm_gain.reshape(1, -1)),
+        in_hbm(lengths.reshape(1, -1)),
+        in_hbm(lambdas.reshape(1, -1)),
+        in_hbm(jnp.asarray(rates, F32).reshape(1, -1)),
         in_hbm(query_weight),
         in_hbm(key_weight),
         in_hbm(value_weight),
     )
     got = lax.all_to_all(sent, "kv", split_axis=0, concat_axis=0, tiled=True)
     cache_shape = (SEQS, 2048, LANES)
-    halfway = DH // 2
-    frequency = theta_base ** (-jnp.arange(halfway, dtype=F32) / halfway)
-    angles = lengths.astype(F32)[:, None] * frequency[None, :]
-    cosine = jnp.tile(jnp.cos(angles), (1, 4))
-    sine = jnp.sin(angles)
-    sine = jnp.tile(jnp.concatenate([-sine, sine], axis=1), (1, 2))
-    own = lax.axis_index("kv").astype(jnp.int32).reshape(1)
-    limits = jnp.broadcast_to(
-        jnp.repeat(2 * (lengths - own * 1024), 4).reshape(64, 1), (64, LANES)
-    )
     shared = pl.pallas_call(
         attend_kernel,
-        in_specs=[SM, VM, VM, VM, VM, ANY, ANY],
+        in_specs=[VM, VM, ANY, ANY],
         out_specs=VM,
         out_shape=jax.ShapeDtypeStruct((SEQS, 80, LANES), BF16),
         scratch_shapes=[
@@ -305,28 +346,21 @@
         compiler_params=BIG,
         name="attend",
     )(
-        own,
-        limits,
+        tables,
         got,
-        cosine,
-        sine,
         in_hbm(key_cache.reshape(cache_shape)),
         in_hbm(value_cache.reshape(cache_shape)),
     )
     everyone = lax.all_to_all(shared, "kv", split_axis=0, concat_axis=0, tiled=True)
-    block = jnp.pad(jnp.repeat(lengths // 1024, 4), (0, 64)).reshape(1, LANES)
-    share = jnp.tile(
-        jnp.stack([jnp.ones_like(lambdas), -lambdas], axis=1).reshape(1, 4), (1, 32)
-    )
     partial_out = pl.pallas_call(
         finish_kernel,
-        in_specs=[VM] * 5,
+        in_specs=[VM] * 4,
         out_specs=VM,
         out_shape=jax.ShapeDtypeStruct((8, SEQS, 256), F32),
         scratch_shapes=[pltpu.VMEM((LANES, LANES), F32), pltpu.VMEM((64, LANES), F32)],
         compiler_params=SMALL,
         name="finish",
-    )(everyone, block, share, head_gain.reshape(1, -1), out_weight)
+    )(everyone, tables, head_gain.reshape(1, -1), out_weight)
     shares = lax.all_to_all(partial_out, "tp", split_axis=0, concat_axis=0, tiled=True)
     return shares.sum(axis=0).astype(BF16)
 

time: 53.5 us -> 51 us (0.953)
  blocking collectives: 12.2 us -> 40 us
  waiting for transfers between devices: 14.6 us -> 0 us
  starting transfers between devices: 12.2 us -> 0 us
  Pallas kernels: 11.6 us -> 10.2 us
  other arithmetic: 1.56 us -> 0.61 us
  local copies, waits for them, and re-layouts: 0.94 us -> 0.01 us
    all_to_all x0 -> x2, blocking collectives: none -> 27.8 us  [the longest x1 16.9 us: local(): got = lax.all_to_all(sent, 'kv', split_axis=0, concat_axis=0, tiled=True)]
    all_to_all x2 -> x0, waiting for transfers between devices: 14.6 us -> none  [the longest x1 7.56 us: local(): lax.all_to_all(shared, 'kv', split_axis=0, concat_axis=0, tiled=True)]
    all_to_all x2 -> x0, starting transfers between devices: 12.2 us -> none  [the longest x1 8.6 us: local(): got = lax.all_to_all(sent, 'kv', split_axis=0, concat_axis=0, tiled=True)]
    pallas_call x3, Pallas kernels: 11.6 us -> 10.2 us  [the longest x1 8.04 us: local(): pl.pallas_call(attend_kernel, in_specs=[VM, VM, ANY, ANY], out_specs=VM,...]
    select_n x1 -> x0, other arithmetic: 0.74 us -> none  [local(): block = jnp.pad(jnp.repeat(lengths // 1024, 4), (0, 64)).reshape(1, LANES)]
  transfers between devices with their start and end apart: 2 -> 0, of which waited for: 2 -> 0; matrix products, arithmetic and copies ran while one was open for 3% -> 0% of each run, Pallas kernels for 0% -> 0%
where the time goes in v4:
time: 51 us; the launch traced here: 50.8 us
  blocking collectives  40 us (78%)
  Pallas kernels  10.2 us (20%)
  other arithmetic  0.61 us (1%)
    all_to_all x1, blocking collectives, local(): got = lax.all_to_all(sent, 'kv', split_axis=0, concat_axis=0, tiled=True)  16.9 us
    all_to_all x1, blocking collectives, local(): lax.all_to_all(partial_out, 'tp', split_axis=0, concat_axis=0, tiled=True)  12.2 us
    all_to_all x1, blocking collectives, local(): lax.all_to_all(shared, 'kv', split_axis=0, concat_axis=0, tiled=True)  10.9 us
    pallas_call x1, Pallas kernels, local(): pl.pallas_call(attend_kernel, in_specs=[VM, VM, ANY, ANY], out_specs=VM,...  8.04 us
    pallas_call x1, Pallas kernels, local(): pl.pallas_call(project_kernel, in_specs=[ANY] * 8, out_specs=[VM, VM], ou...  1.52 us

profile of v4, /device:TPU:1, one launch (start us, length us, event | category | flops | bytes accessed | tf_op | source)
XLA Modules:
  0.0 50.8 jit_solution(14725248278982620483)
XLA Ops:
  0.0 1.5 %project.1 = (f32[16,40,128]{2,1,0:T(8,128)S(1)}, f32[40,128]{1,0:T(8,128)S(1)}) custom-call(bf16[16,256]{1,0:T(8,128)(2,1)} %tokens_in.1, f32[1,256]{1,0:T(1,128)} %bitcast.9, s32[1,16]{1,0:T(1,128)} %bitcast.10, f32[1,2]{1,0:T(1,128)} %bitcast.11, f32[1,128]{1,0:T(1,128)} %constant.8.rates_in, bf16[256,256]{1,0:T(8,128)(2,1)} %query_in.1, ...), custom_call_target="tpu_custom_call" | custom-call | tf_op jit(solution)/shard_map/project/pallas_call | solution.py:300
  1.5 16.9 %all_to_all.15.got = f32[16,40,128]{2,1,0:T(8,128)S(1)} all-to-all(f32[16,40,128]{2,1,0:T(8,128)S(1)} %get-tuple-element.8), channel_id=1, replica_groups=mesh['kv'=16,'tp'=8] {'kv'}, dimensions={0} | all-to-all | bytes 655360 | tf_op jit(solution)/shard_map/all_to_all | solution.py:330
  18.4 0.0 copy-start
  18.4 0.0 copy-start.1
  18.4 8.0 %attend.1 = bf16[16,80,128]{2,1,0:T(8,128)(2,1)S(1)} custom-call(f32[40,128]{1,0:T(8,128)S(1)} %get-tuple-element.7.tables, f32[16,40,128]{2,1,0:T(8,128)S(1)} %all_to_all.15.got, bf16[16,2048,128]{2,1,0:T(8,128)(2,1)} %bitcast.7, bf16[16,2048,128]{2,1,0:T(8,128)(2,1)} %bitcast.8), custom_call_target="tpu_custom_call" | custom-call | tf_op jit(solution)/shard_map/attend/pallas_call | solution.py:332
  26.5 10.9 %all_to_all.16.got = bf16[16,80,128]{2,1,0:T(8,128)(2,1)S(1)} all-to-all(bf16[16,80,128]{2,1,0:T(8,128)(2,1)S(1)} %attend.1), channel_id=1, replica_groups=mesh['kv'=16,'tp'=8] {'kv'}, dimensions={0} | all-to-all | bytes 655360 | tf_op jit(solution)/shard_map/all_to_all | solution.py:354
  37.4 0.0 copy-done
  37.4 0.0 copy-done.1
  37.4 0.6 %finish.1 = f32[8,16,256]{2,1,0:T(8,128)S(1)} custom-call(bf16[16,80,128]{2,1,0:T(8,128)(2,1)S(1)} %all_to_all.16.got, f32[40,128]{1,0:T(8,128)S(1)} %get-tuple-element.7.tables, f32[1,128]{1,0:T(1,128)S(1)} %bitcast.6, bf16[256,256]{1,0:T(8,128)(2,1)S(1)} %copy-done), custom_call_target="tpu_custom_call" | custom-call | tf_op jit(solution)/shard_map/finish/pallas_call | solution.py:355
  38.0 12.2 %all_to_all.17 = f32[8,16,256]{2,1,0:T(8,128)S(1)} all-to-all(f32[8,16,256]{2,1,0:T(8,128)S(1)} %finish.1), channel_id=1, replica_groups=mesh['kv'=16,'tp'=8] {'tp'}, dimensions={0} | all-to-all | bytes 262144 | tf_op jit(solution)/shard_map/all_to_all | solution.py:364
  50.2 0.6 %reduce_sum.9 = bf16[16,256]{1,0:T(8,128)(2,1)} reduce(f32[8,16,256]{2,1,0:T(8,128)S(1)} %all_to_all.17, f32[]{:T(128)} %constant.1.clone.1), dimensions={0}, to_apply=%region_0.0 | reduce | flops 28672 | bytes 139268 | tf_op jit(solution)/shard_map/reduce_sum | solution.py:365
Async XLA Ops:
  18.4 18.9 %copy-start = (bf16[256,256]{1,0:T(8,128)(2,1)S(1)}, bf16[256,256]{1,0:T(8,128)(2,1)}, u32[]{:S(2)}) copy-start(bf16[256,256]{1,0:T(8,128)(2,1)} %out_weight.1) | copy-start | bytes 393220
  18.4 18.9 %copy-start.1 = (f32[128]{0:T(128)S(1)}, f32[128]{0:T(128)}, u32[]{:S(2)}) copy-start(f32[128]{0:T(128)} %param.19) | copy-start | bytes 1540

commit v5 on v4

--- a/solution.py
+++ b/solution.py
@@ -15,7 +15,6 @@
 epsilon = 1e-05
 theta_base = 500000.0
 floor_value = -1e30
-AHEAD = 10
 
 VM = pl.BlockSpec(memory_space=pltpu.VMEM)
 SM = pl.BlockSpec(memory_space=pltpu.SMEM)
@@ -114,7 +113,7 @@
 
 def attend_kernel(
     tables, got, keys_in, values_in, out, keys, values, arrived, query_rows, scale_rows,
-    score_rows, weight_rows,
+    asked_rows, score_rows, weight_rows,
 ):
     copies = []
     for kind, (source, target) in enumerate(((keys_in, keys), (values_in, values))):
@@ -122,15 +121,8 @@
             copies.append(
                 pltpu.make_async_copy(source.at[seq], target.at[seq], arrived.at[kind, seq])
             )
-    for copy in copies[:AHEAD]:
+    for copy in copies:
         copy.start()
-
-    def arrive(kind, seq):
-        at = kind * SEQS + seq
-        copies[at].wait()
-        if at + AHEAD < 2 * SEQS:
-            copies[at + AHEAD].start()
-
     me = lax.axis_index("kv")
     cosine, sine = tables[0:16, :], tables[16:32, :]
     summed = jnp.sum(got[...], axis=0)
@@ -143,46 +135,85 @@
             summed[16 * head : 16 * head + 16, :] * scaling, cosine, sine
         )
         query_rows[head * SEQS : (head + 1) * SEQS, :] = turned_query.astype(F32)
-    sub, lane8 = iotas(8)
-    map_lanes = (lane8 // DH) == (sub % 2)
-    for pair in range(SEQS // 2):
-        first, second = 2 * pair, 2 * pair + 1
-
-        def row_of(head, seq):
-            at = head * SEQS + seq
-            return jnp.broadcast_to(query_rows[at : at + 1, :], (8, LANES))
-
-        left = jnp.where(sub < 2, row_of(0, first), row_of(1, first))
-        left = jnp.where(map_lanes & (sub < 4), left, 0.0)
-        right = jnp.where(sub < 6, row_of(0, second), row_of(1, second))
-        right = jnp.where(map_lanes & (sub >= 4), right, 0.0)
-        queries = jnp.concatenate([left, right], axis=1).astype(BF16)
-        arrive(0, first)
-        arrive(0, second)
-        both_keys = jnp.concatenate([keys[first], keys[second]], axis=1)
-        score_rows[pair * 8 : pair * 8 + 8, :] = lax.dot_general(
-            queries, both_keys, (((1,), (1,)), ((), ())), preferred_element_type=F32
-        )
-    columns = lax.broadcasted_iota(jnp.int32, (8, 2048), 1)
-    subs = lax.broadcasted_iota(jnp.int32, (8, 2048), 0)
+    map_lanes = (lane // DH) == (row % 2)
+
+    def row_of(head, seq):
+        at = head * SEQS + seq
+        return jnp.broadcast_to(query_rows[at : at + 1, :], (SEQS, LANES))
+
+    for group in range(4):
+        first = 4 * group
+        left = jnp.where(
+            row < 8,
+            jnp.where(row < 2, row_of(0, first), row_of(1, first)),
+            jnp.where(row < 10, row_of(0, first + 2), row_of(1, first + 2)),
+        )
+        right = jnp.where(
+            row < 8,
+            jnp.where(row < 6, row_of(0, first + 1), row_of(1, first + 1)),
+            jnp.where(row < 14, row_of(0, first + 3), row_of(1, first + 3)),
+        )
+        left = jnp.where(map_lanes & (row % 8 < 4), left, 0.0)
+        right = jnp.where(map_lanes & (row % 8 >= 4), right, 0.0)
+        asked_rows[group * 16 : group * 16 + 16, :] = jnp.concatenate(
+            [left, right], axis=1
+        ).astype(BF16)
+
+    columns = lax.broadcasted_iota(jnp.int32, (SEQS, 2048), 1)
+    subs = lax.broadcasted_iota(jnp.int32, (SEQS, 2048), 0)
     own_head = (columns % 2) == ((subs // 2) % 2)
-    maxima = jnp.zeros((8, LANES), F32)
-    totals = jnp.zeros((8, LANES), F32)
-    for pair in range(SEQS // 2):
-        first, second = 2 * pair, 2 * pair + 1
-        at = slice(pair * 8, pair * 8 + 8)
-        limit = jnp.sum(
-            jnp.where(lane8 == pair * 8 + sub, tables[32:33, :], 0.0), axis=1, keepdims=True
-        ).astype(jnp.int32)
+    lengths_of = tables[32:33, :].astype(jnp.int32)
+    sums = [jnp.zeros((SEQS, LANES), F32), jnp.zeros((SEQS, LANES), F32)]
+
+    def score(group):
+        for copy in copies[4 * group : 4 * group + 4]:
+            copy.wait()
+        for pair in (2 * group, 2 * group + 1):
+            at = slice(pair * 8, pair * 8 + 8)
+            both_keys = jnp.concatenate([keys[2 * pair], keys[2 * pair + 1]], axis=1)
+            score_rows[at, :] = lax.dot_general(
+                asked_rows[at, :],
+                both_keys,
+                (((1,), (1,)), ((), ())),
+                preferred_element_type=F32,
+            )
+
+    def weigh(group):
+        at = slice(group * 16, group * 16 + 16)
+        place = lane == group * 16 + row
+        limit = jnp.sum(jnp.where(place, lengths_of, 0), axis=1, keepdims=True)
         visible = own_head & (columns < 2 * (limit - me * 1024))
         masked = jnp.where(visible, score_rows[at, :] * DH ** (-0.5), floor_value)
         highest = jnp.max(masked, axis=1, keepdims=True)
         weights = jnp.where(visible, jnp.exp(masked - highest), 0.0).astype(BF16)
+        weight_rows[at, :] = weights
         total = jnp.sum(weights.astype(F32), axis=1, keepdims=True)
-        weight_rows[at, :] = weights
-        place = lane8 == pair * 8 + sub
-        maxima = maxima + jnp.where(place, highest, 0.0)
-        totals = totals + jnp.where(place, total, 0.0)
+        sums[0] = sums[0] + jnp.where(place, highest, 0.0)
+        sums[1] = sums[1] + jnp.where(place, total, 0.0)
+
+    def value(pair):
+        both_values = jnp.concatenate([values[2 * pair], values[2 * pair + 1]], axis=1)
+        valued = jnp.dot(
+            weight_rows[pair * 8 : pair * 8 + 8, :], both_values, preferred_element_type=F32
+        )
+        return jnp.where(row[:8] < 4, valued[:, :LANES], valued[:, LANES:])
+
+    def arrive(seqs):
+        for seq in seqs:
+            copies[SEQS + seq].wait()
+
+    def give(group, parts):
+        sixteen = jnp.concatenate(parts, axis=0).astype(BF16)
+        for dest in range(SEQS):
+            out[dest, group * 16 : group * 16 + 16, :] = sixteen
+
+    score(0)
+    for group in range(1, 4):
+        score(group)
+        weigh(group - 1)
+    arrive(range(4))
+    give(0, [value(0), value(1)])
+    weigh(3)
     scale = scale_rows[pl.ds(me, 1), :]
     row_cosine = tables[pl.ds(me, 1), :]
     row_sine = tables[pl.ds(SEQS + me, 1), :]
@@ -193,16 +224,16 @@
         fresh_key = turned(summed[33 + head : 34 + head, :] * scale, row_cosine, row_sine)
         product = query * fresh_key.astype(F32)
         for side in range(2):
-            score = jnp.sum(
+            fresh = jnp.sum(
                 jnp.where(lane1 // DH == side, product, 0.0), axis=1, keepdims=True
             ) * DH ** (-0.5)
             at = me * 4 + head * 2 + side
-            fresh_scores = fresh_scores + jnp.where(lane1 == at, score, 0.0)
+            fresh_scores = fresh_scores + jnp.where(lane1 == at, fresh, 0.0)
     fresh_value = (summed[35:37, :] * scale).astype(BF16).astype(F32)
     tail = jnp.concatenate(
         [
-            *thirds(jnp.sum(maxima, axis=0, keepdims=True)),
-            *thirds(jnp.sum(totals, axis=0, keepdims=True)),
+            *thirds(jnp.sum(sums[0], axis=0, keepdims=True)),
+            *thirds(jnp.sum(sums[1], axis=0, keepdims=True)),
             *thirds(fresh_scores),
             fresh_value,
             jnp.zeros((5, LANES), F32),
@@ -211,22 +242,13 @@
     ).astype(BF16)
     for dest in range(SEQS):
         out[dest, 64:80, :] = tail
-    for two in range(SEQS // 4):
-        parts = []
-        for pair in (2 * two, 2 * two + 1):
-            first, second = 2 * pair, 2 * pair + 1
-            arrive(1, first)
-            arrive(1, second)
-            both_values = jnp.concatenate([values[first], values[second]], axis=1)
-            valued = jnp.dot(
-                weight_rows[pair * 8 : pair * 8 + 8, :],
-                both_values,
-                preferred_element_type=F32,
-            )
-            parts.append(jnp.where(sub < 4, valued[:, :LANES], valued[:, LANES:]))
-        sixteen = jnp.concatenate(parts, axis=0).astype(BF16)
-        for dest in range(SEQS):
-            out[dest, two * 16 : two * 16 + 16, :] = sixteen
+    for group in range(1, 3):
+        arrive(range(4 * group, 4 * group + 4))
+        give(group, [value(2 * group), value(2 * group + 1)])
+    arrive((12, 13))
+    early = value(6)
+    arrive((14, 15))
+    give(3, [early, value(7)])
 
 
 def thirds(x):
@@ -281,6 +303,27 @@
     partial_out = jnp.dot(head_out, out_weight[...], preferred_element_type=F32)
     for dest in range(8):
         out[dest] = partial_out
+
+
+def attend_call(tables, got, keys, values, name):
+    return pl.pallas_call(
+        attend_kernel,
+        in_specs=[VM, VM, ANY, ANY],
+        out_specs=VM,
+        out_shape=jax.ShapeDtypeStruct((SEQS, 80, LANES), BF16),
+        scratch_shapes=[
+            pltpu.VMEM(keys.shape, BF16),
+            pltpu.VMEM(values.shape, BF16),
+            pltpu.SemaphoreType.DMA((2, SEQS)),
+            pltpu.VMEM((32, LANES), F32),
+            pltpu.VMEM((SEQS, LANES), F32),
+            pltpu.VMEM((64, 256), BF16),
+            pltpu.VMEM((64, 2048), F32),
+            pltpu.VMEM((64, 2048), BF16),
+        ],
+        compiler_params=BIG,
+        name=name,
+    )(tables, got, in_hbm(keys), in_hbm(values))
 
 
 def local(
@@ -329,27 +372,8 @@
     )
     got = lax.all_to_all(sent, "kv", split_axis=0, concat_axis=0, tiled=True)
     cache_shape = (SEQS, 2048, LANES)
-    shared = pl.pallas_call(
-        attend_kernel,
-        in_specs=[VM, VM, ANY, ANY],
-        out_specs=VM,
-        out_shape=jax.ShapeDtypeStruct((SEQS, 80, LANES), BF16),
-        scratch_shapes=[
-            pltpu.VMEM(cache_shape, BF16),
-            pltpu.VMEM(cache_shape, BF16),
-            pltpu.SemaphoreType.DMA((2, SEQS)),
-            pltpu.VMEM((32, LANES), F32),
-            pltpu.VMEM((SEQS, LANES), F32),
-            pltpu.VMEM((64, 2048), F32),
-            pltpu.VMEM((64, 2048), BF16),
-        ],
-        compiler_params=BIG,
-        name="attend",
-    )(
-        tables,
-        got,
-        in_hbm(key_cache.reshape(cache_shape)),
-        in_hbm(value_cache.reshape(cache_shape)),
+    shared = attend_call(
+        tables, got, key_cache.reshape(cache_shape), value_cache.reshape(cache_shape), "attend"
     )
     everyone = lax.all_to_all(shared, "kv", split_axis=0, concat_axis=0, tiled=True)
     partial_out = pl.pallas_call(

time: 51 us -> 49.6 us (0.973)
  Pallas kernels: 10.2 us -> 8.81 us
    pallas_call x1, Pallas kernels: 8.04 us -> 6.65 us  [attend_call(): pl.pallas_call(attend_kernel, in_specs=[VM, VM, ANY, ANY], out_specs=VM,...]
where the time goes in v5:
time: 49.6 us; the launch traced here: 49.4 us
  blocking collectives  40 us (81%)
  Pallas kernels  8.81 us (18%)
  other arithmetic  0.61 us (1%)
    all_to_all x1, blocking collectives, local(): got = lax.all_to_all(sent, 'kv', split_axis=0, concat_axis=0, tiled=True)  16.9 us
    all_to_all x1, blocking collectives, local(): lax.all_to_all(partial_out, 'tp', split_axis=0, concat_axis=0, tiled=True)  12.2 us
    all_to_all x1, blocking collectives, local(): lax.all_to_all(shared, 'kv', split_axis=0, concat_axis=0, tiled=True)  10.9 us
    pallas_call x1, Pallas kernels, attend_call(): pl.pallas_call(attend_kernel, in_specs=[VM, VM, ANY, ANY], out_specs=VM,...  6.65 us
    pallas_call x1, Pallas kernels, local(): pl.pallas_call(project_kernel, in_specs=[ANY] * 8, out_specs=[VM, VM], ou...  1.52 us

profile of v5, /device:TPU:1, one launch (start us, length us, event | category | flops | bytes accessed | tf_op | source)
XLA Modules:
  0.0 49.4 jit_solution(7686182033373957175)
XLA Ops:
  0.0 1.5 %project.1 = (f32[16,40,128]{2,1,0:T(8,128)S(1)}, f32[40,128]{1,0:T(8,128)S(1)}) custom-call(bf16[16,256]{1,0:T(8,128)(2,1)} %tokens_in.1, f32[1,256]{1,0:T(1,128)} %bitcast.9, s32[1,16]{1,0:T(1,128)} %bitcast.10, f32[1,2]{1,0:T(1,128)} %bitcast.11, f32[1,128]{1,0:T(1,128)} %constant.8.rates_in, bf16[256,256]{1,0:T(8,128)(2,1)} %query_in.1, ...), custom_call_target="tpu_custom_call" | custom-call | tf_op jit(solution)/shard_map/project/pallas_call | solution.py:343
  1.5 16.9 %all_to_all.15.got = f32[16,40,128]{2,1,0:T(8,128)S(1)} all-to-all(f32[16,40,128]{2,1,0:T(8,128)S(1)} %get-tuple-element.8), channel_id=1, replica_groups=mesh['kv'=16,'tp'=8] {'kv'}, dimensions={0} | all-to-all | bytes 655360 | tf_op jit(solution)/shard_map/all_to_all | solution.py:373
  18.4 0.0 copy-start
  18.4 0.0 copy-start.1
  18.4 6.6 %attend.1 = bf16[16,80,128]{2,1,0:T(8,128)(2,1)S(1)} custom-call(f32[40,128]{1,0:T(8,128)S(1)} %get-tuple-element.7.tables, f32[16,40,128]{2,1,0:T(8,128)S(1)} %all_to_all.15.got, bf16[16,2048,128]{2,1,0:T(8,128)(2,1)} %bitcast.7, bf16[16,2048,128]{2,1,0:T(8,128)(2,1)} %bitcast.8), custom_call_target="tpu_custom_call" | custom-call | tf_op jit(solution)/shard_map/attend/pallas_call | solution.py:309
  25.1 10.9 %all_to_all.16.got = bf16[16,80,128]{2,1,0:T(8,128)(2,1)S(1)} all-to-all(bf16[16,80,128]{2,1,0:T(8,128)(2,1)S(1)} %attend.1), channel_id=1, replica_groups=mesh['kv'=16,'tp'=8] {'kv'}, dimensions={0} | all-to-all | bytes 655360 | tf_op jit(solution)/shard_map/all_to_all | solution.py:378
  36.0 0.0 copy-done
  36.0 0.0 copy-done.1
  36.0 0.6 %finish.1 = f32[8,16,256]{2,1,0:T(8,128)S(1)} custom-call(bf16[16,80,128]{2,1,0:T(8,128)(2,1)S(1)} %all_to_all.16.got, f32[40,128]{1,0:T(8,128)S(1)} %get-tuple-element.7.tables, f32[1,128]{1,0:T(1,128)S(1)} %bitcast.6, bf16[256,256]{1,0:T(8,128)(2,1)S(1)} %copy-done), custom_call_target="tpu_custom_call" | custom-call | tf_op jit(solution)/shard_map/finish/pallas_call | solution.py:379
  36.6 12.2 %all_to_all.17 = f32[8,16,256]{2,1,0:T(8,128)S(1)} all-to-all(f32[8,16,256]{2,1,0:T(8,128)S(1)} %finish.1), channel_id=1, replica_groups=mesh['kv'=16,'tp'=8] {'tp'}, dimensions={0} | all-to-all | bytes 262144 | tf_op jit(solution)/shard_map/all_to_all | solution.py:388
  48.8 0.6 %reduce_sum.9 = bf16[16,256]{1,0:T(8,128)(2,1)} reduce(f32[8,16,256]{2,1,0:T(8,128)S(1)} %all_to_all.17, f32[]{:T(128)} %constant.1.clone.1), dimensions={0}, to_apply=%region_0.0 | reduce | flops 28672 | bytes 139268 | tf_op jit(solution)/shard_map/reduce_sum | solution.py:389
Async XLA Ops:
  18.4 17.5 %copy-start = (bf16[256,256]{1,0:T(8,128)(2,1)S(1)}, bf16[256,256]{1,0:T(8,128)(2,1)}, u32[]{:S(2)}) copy-start(bf16[256,256]{1,0:T(8,128)(2,1)} %out_weight.1) | copy-start | bytes 393220
  18.4 17.5 %copy-start.1 = (f32[128]{0:T(128)S(1)}, f32[128]{0:T(128)}, u32[]{:S(2)}) copy-start(f32[128]{0:T(128)} %param.19) | copy-start | bytes 1540

commit v6 on v5

--- a/solution.py
+++ b/solution.py
@@ -163,7 +163,7 @@
     subs = lax.broadcasted_iota(jnp.int32, (SEQS, 2048), 0)
     own_head = (columns % 2) == ((subs // 2) % 2)
     lengths_of = tables[32:33, :].astype(jnp.int32)
-    sums = [jnp.zeros((SEQS, LANES), F32), jnp.zeros((SEQS, LANES), F32)]
+    sums = [jnp.zeros((SEQS, LANES), F32)]
 
     def score(group):
         for copy in copies[4 * group : 4 * group + 4]:
@@ -188,8 +188,8 @@
         weights = jnp.where(visible, jnp.exp(masked - highest), 0.0).astype(BF16)
         weight_rows[at, :] = weights
         total = jnp.sum(weights.astype(F32), axis=1, keepdims=True)
-        sums[0] = sums[0] + jnp.where(place, highest, 0.0)
-        sums[1] = sums[1] + jnp.where(place, total, 0.0)
+        beside = lane == 64 + group * 16 + row
+        sums[0] = sums[0] + jnp.where(place, highest, jnp.where(beside, total, 0.0))
 
     def value(pair):
         both_values = jnp.concatenate([values[2 * pair], values[2 * pair + 1]], axis=1)
@@ -233,15 +233,13 @@
     tail = jnp.concatenate(
         [
             *thirds(jnp.sum(sums[0], axis=0, keepdims=True)),
-            *thirds(jnp.sum(sums[1], axis=0, keepdims=True)),
             *thirds(fresh_scores),
             fresh_value,
-            jnp.zeros((5, LANES), F32),
         ],
         axis=0,
     ).astype(BF16)
     for dest in range(SEQS):
-        out[dest, 64:80, :] = tail
+        out[dest, 64:72, :] = tail
     for group in range(1, 3):
         arrive(range(4 * group, 4 * group + 4))
         give(group, [value(2 * group), value(2 * group + 1)])
@@ -259,14 +257,16 @@
 
 def finish_kernel(got, tables, head_gain, out_weight, out, factors, joined):
     rows16, _ = iotas(SEQS)
-    tails = got[:, 64:80, :].astype(F32)
+    tails = got[:, 64:72, :].astype(F32)
 
     def whole(at):
         return tails[:, at, :] + tails[:, at + 1, :] + tails[:, at + 2, :]
 
-    maxima = whole(0)
-    totals = whole(3)
-    fresh = jnp.sum(whole(6), axis=0, keepdims=True)
+    left = lax.broadcasted_iota(jnp.int32, (1, LANES), 1) < 64
+    both = whole(0)
+    maxima = jnp.where(left, both, 0.0)
+    totals = jnp.where(left, pltpu.roll(both, 64, 1), 1.0)
+    fresh = jnp.sum(whole(3), axis=0, keepdims=True)
     block = tables[32:33, :].astype(jnp.int32) // 1024
     in_block = jnp.max(
         jnp.where(rows16 == block, maxima, floor_value), axis=0, keepdims=True
@@ -286,7 +286,7 @@
         here = columns[four * 16 : four * 16 + 16, :]
         fresh_value = jnp.zeros((16, LANES), F32)
         for n in range(8):
-            line = tails[four * 4 + n // 2, 9 + n % 2 : 10 + n % 2, :]
+            line = tails[four * 4 + n // 2, 6 + n % 2 : 7 + n % 2, :]
             fresh_value = jnp.where(sub // 2 == n, line, fresh_value)
         joint = here[:, SEQS : SEQS + 1] * fresh_value
         for peer in range(SEQS):
@@ -300,7 +300,9 @@
         mean = jnp.mean(mixed * mixed, axis=1, keepdims=True)
         sides.append((mixed * lax.rsqrt(mean + epsilon) * head_gain[...]).astype(BF16))
     head_out = jnp.concatenate(sides, axis=1)
-    partial_out = jnp.dot(head_out, out_weight[...], preferred_element_type=F32)
+    partial_out = jnp.dot(
+        head_out, out_weight[...], preferred_element_type=F32
+    ).astype(BF16)
     for dest in range(8):
         out[dest] = partial_out
 
@@ -310,7 +312,7 @@
         attend_kernel,
         in_specs=[VM, VM, ANY, ANY],
         out_specs=VM,
-        out_shape=jax.ShapeDtypeStruct((SEQS, 80, LANES), BF16),
+        out_shape=jax.ShapeDtypeStruct((SEQS, 72, LANES), BF16),
         scratch_shapes=[
             pltpu.VMEM(keys.shape, BF16),
             pltpu.VMEM(values.shape, BF16),
@@ -380,13 +382,13 @@
         finish_kernel,
         in_specs=[VM] * 4,
         out_specs=VM,
-        out_shape=jax.ShapeDtypeStruct((8, SEQS, 256), F32),
+        out_shape=jax.ShapeDtypeStruct((8, SEQS, 256), BF16),
         scratch_shapes=[pltpu.VMEM((LANES, LANES), F32), pltpu.VMEM((64, LANES), F32)],
         compiler_params=SMALL,
         name="finish",
     )(everyone, tables, head_gain.reshape(1, -1), out_weight)
     shares = lax.all_to_all(partial_out, "tp", split_axis=0, concat_axis=0, tiled=True)
-    return shares.sum(axis=0).astype(BF16)
+    return shares.astype(F32).sum(axis=0).astype(BF16)
 
 
 def solution(mesh):

time: 49.6 us -> 49.1 us (0.990)
  blocking collectives: 40 us -> 39.4 us
where the time goes in v6:
time: 49.1 us; the launch traced here: 48.9 us
  blocking collectives  39.4 us (80%)
  Pallas kernels  8.81 us (18%)
  other arithmetic  0.61 us (1%)
    all_to_all x1, blocking collectives, local(): got = lax.all_to_all(sent, 'kv', split_axis=0, concat_axis=0, tiled=True)  16.9 us
    all_to_all x1, blocking collectives, local(): lax.all_to_all(partial_out, 'tp', split_axis=0, concat_axis=0, tiled=True)  11.8 us
    all_to_all x1, blocking collectives, local(): lax.all_to_all(shared, 'kv', split_axis=0, concat_axis=0, tiled=True)  10.7 us
    pallas_call x1, Pallas kernels, attend_call(): pl.pallas_call(attend_kernel, in_specs=[VM, VM, ANY, ANY], out_specs=VM,...  6.65 us
    pallas_call x1, Pallas kernels, local(): pl.pallas_call(project_kernel, in_specs=[ANY] * 8, out_specs=[VM, VM], ou...  1.52 us

profile of v6, /device:TPU:1, one launch (start us, length us, event | category | flops | bytes accessed | tf_op | source)
XLA Modules:
  0.0 48.9 jit_solution(16433612708930107295)
XLA Ops:
  0.0 1.5 %project.1 = (f32[16,40,128]{2,1,0:T(8,128)S(1)}, f32[40,128]{1,0:T(8,128)S(1)}) custom-call(bf16[16,256]{1,0:T(8,128)(2,1)} %tokens_in.1, f32[1,256]{1,0:T(1,128)} %bitcast.9, s32[1,16]{1,0:T(1,128)} %bitcast.10, f32[1,2]{1,0:T(1,128)} %bitcast.11, f32[1,128]{1,0:T(1,128)} %constant.9.rates_in, bf16[256,256]{1,0:T(8,128)(2,1)} %query_in.1, ...), custom_call_target="tpu_custom_call" | custom-call | tf_op jit(solution)/shard_map/project/pallas_call | solution.py:345
  1.5 16.9 %all_to_all.15.got = f32[16,40,128]{2,1,0:T(8,128)S(1)} all-to-all(f32[16,40,128]{2,1,0:T(8,128)S(1)} %get-tuple-element.8), channel_id=1, replica_groups=mesh['kv'=16,'tp'=8] {'kv'}, dimensions={0} | all-to-all | bytes 655360 | tf_op jit(solution)/shard_map/all_to_all | solution.py:375
  18.4 0.0 copy-start
  18.4 0.0 copy-start.1
  18.4 6.6 %attend.1 = bf16[16,72,128]{2,1,0:T(8,128)(2,1)S(1)} custom-call(f32[40,128]{1,0:T(8,128)S(1)} %get-tuple-element.7.tables, f32[16,40,128]{2,1,0:T(8,128)S(1)} %all_to_all.15.got, bf16[16,2048,128]{2,1,0:T(8,128)(2,1)} %bitcast.7, bf16[16,2048,128]{2,1,0:T(8,128)(2,1)} %bitcast.8), custom_call_target="tpu_custom_call" | custom-call | tf_op jit(solution)/shard_map/attend/pallas_call | solution.py:311
  25.1 10.7 %all_to_all.16.got = bf16[16,72,128]{2,1,0:T(8,128)(2,1)S(1)} all-to-all(bf16[16,72,128]{2,1,0:T(8,128)(2,1)S(1)} %attend.1), channel_id=1, replica_groups=mesh['kv'=16,'tp'=8] {'kv'}, dimensions={0} | all-to-all | bytes 589824 | tf_op jit(solution)/shard_map/all_to_all | solution.py:380
  35.8 0.0 copy-done
  35.8 0.0 copy-done.1
  35.8 0.6 %finish.1 = bf16[8,16,256]{2,1,0:T(8,128)(2,1)S(1)} custom-call(bf16[16,72,128]{2,1,0:T(8,128)(2,1)S(1)} %all_to_all.16.got, f32[40,128]{1,0:T(8,128)S(1)} %get-tuple-element.7.tables, f32[1,128]{1,0:T(1,128)S(1)} %bitcast.6, bf16[256,256]{1,0:T(8,128)(2,1)S(1)} %copy-done), custom_call_target="tpu_custom_call" | custom-call | tf_op jit(solution)/shard_map/finish/pallas_call | solution.py:381
  36.4 11.8 %all_to_all.17 = bf16[8,16,256]{2,1,0:T(8,128)(2,1)S(1)} all-to-all(bf16[8,16,256]{2,1,0:T(8,128)(2,1)S(1)} %finish.1), channel_id=1, replica_groups=mesh['kv'=16,'tp'=8] {'tp'}, dimensions={0} | all-to-all | bytes 131072 | tf_op jit(solution)/shard_map/all_to_all | solution.py:390
  48.2 0.6 %reduce_sum.12 = bf16[16,256]{1,0:T(8,128)(2,1)} reduce(bf16[8,16,256]{2,1,0:T(8,128)(2,1)S(1)} %all_to_all.17, bf16[]{:T(256)} %constant.4.clone.1), dimensions={0}, to_apply=%region_0.0 | reduce | flops 28672 | bytes 73730 | tf_op jit(solution)/shard_map/reduce_sum | solution.py:391
Async XLA Ops:
  18.4 17.3 %copy-start = (bf16[256,256]{1,0:T(8,128)(2,1)S(1)}, bf16[256,256]{1,0:T(8,128)(2,1)}, u32[]{:S(2)}) copy-start(bf16[256,256]{1,0:T(8,128)(2,1)} %out_weight.1) | copy-start | bytes 393220
  18.4 17.3 %copy-start.1 = (f32[128]{0:T(128)S(1)}, f32[128]{0:T(128)}, u32[]{:S(2)}) copy-start(f32[128]{0:T(128)} %param.19) | copy-start | bytes 1540

commit v7 on v6

--- a/solution.py
+++ b/solution.py
@@ -21,12 +21,16 @@
 ANY = pl.BlockSpec(memory_space=pltpu.HBM)
 F32 = jnp.float32
 BF16 = jnp.bfloat16
-SMALL = pltpu.CompilerParams(vmem_limit_bytes=8 * 1024 * 1024)
-BIG = pltpu.CompilerParams(vmem_limit_bytes=30 * 1024 * 1024)
+SMALL = pltpu.CompilerParams(vmem_limit_bytes=16 * 1024 * 1024)
+BIG = pltpu.CompilerParams(vmem_limit_bytes=26 * 1024 * 1024)
 
 
 def in_hbm(x):
     return pltpu.with_memory_space_constraint(x, pltpu.HBM)
+
+
+def in_vmem(x):
+    return pltpu.with_memory_space_constraint(x, pltpu.VMEM)
 
 
 def iotas(rows):
@@ -35,8 +39,9 @@
 
 
 def project_kernel(
-    tokens_in, gain_in, lengths_in, lambdas_in, rates_in, query_in, key_in, value_in, out, tables,
-    tokens, gain, lengths, lambdas, rates, weights, small, large,
+    tokens_in, gain_in, lengths_in, lambdas_in, rates_in, query_in, key_in, value_in, out,
+    out_one, out_two, out_three, tables,
+    tokens, gain, lengths, lambdas, rates, weights, fresh, small, large,
 ):
     near = [
         pltpu.make_async_copy(source, target, small.at[n])
@@ -86,21 +91,42 @@
         far[n].wait()
         products.append(jnp.dot(normed, weights[n], preferred_element_type=F32))
     query, key, value = products
+    fresh[0:16, :] = key[:, :LANES]
+    fresh[16:32, :] = key[:, LANES:]
+    fresh[32:48, :] = value[:, :LANES]
+    fresh[48:64, :] = value[:, LANES:]
+    column = lax.axis_index("kv") % 4
+    head = jnp.concatenate([square_row, jnp.zeros((7, LANES), F32)], axis=0)
+    for turn, target in enumerate((out, out_one, out_two, out_three)):
+        target[0:16, :] = query[:, :LANES]
+        target[16:32, :] = query[:, LANES:]
+        target[32:40, :] = head
+        other = column ^ turn
+        target[40:56, :] = jnp.concatenate(
+            [fresh[pl.ds(16 * part + other, 4, 4), :] for part in range(4)], axis=0
+        )
+
+
+def halfway_kernel(mine, one, two, three, out, out_one, out_two, out_three, total):
+    total[...] = (mine[...] + one[...]) + (two[...] + three[...])
+    plane = lax.axis_index("kv") // 4
     blank = jnp.zeros((3, LANES), F32)
-    for dest in range(SEQS):
-        out[dest, 0:16, :] = query[:, :LANES]
-        out[dest, 16:32, :] = query[:, LANES:]
-        out[dest, 32:40, :] = jnp.concatenate(
-            [
-                square_row,
-                key[dest : dest + 1, :LANES],
-                key[dest : dest + 1, LANES:],
-                value[dest : dest + 1, :LANES],
-                value[dest : dest + 1, LANES:],
-                blank,
-            ],
-            axis=0,
-        )
+    for turn, target in enumerate((out, out_one, out_two, out_three)):
+        target[0:32, :] = total[0:32, :]
+        target[32:40, :] = jnp.concatenate(
+            [total[32:33, :], total[pl.ds(40 + (plane ^ turn), 4, 4), :], blank], axis=0
+        )
+
+
+def swapped(arrays, step):
+    mine, *others = arrays
+    return [
+        mine,
+        *(
+            lax.ppermute(x, "kv", [(i, i ^ (step * (n + 1))) for i in range(16)])
+            for n, x in enumerate(others)
+        ),
+    ]
 
 
 def turned(x, cosine, sine):
@@ -112,20 +138,12 @@
 
 
 def attend_kernel(
-    tables, got, keys_in, values_in, out, keys, values, arrived, query_rows, scale_rows,
-    asked_rows, score_rows, weight_rows,
+    tables, mine, one, two, three, keys, values, out, query_rows, scale_rows, asked_rows,
+    score_rows, weight_rows,
 ):
-    copies = []
-    for kind, (source, target) in enumerate(((keys_in, keys), (values_in, values))):
-        for seq in range(SEQS):
-            copies.append(
-                pltpu.make_async_copy(source.at[seq], target.at[seq], arrived.at[kind, seq])
-            )
-    for copy in copies:
-        copy.start()
     me = lax.axis_index("kv")
     cosine, sine = tables[0:16, :], tables[16:32, :]
-    summed = jnp.sum(got[...], axis=0)
+    summed = (mine[...] + one[...]) + (two[...] + three[...])
     row, lane = iotas(SEQS)
     squares = jnp.sum(jnp.where(row == lane, summed[32:33, :], 0.0), axis=1, keepdims=True)
     scaling = jnp.broadcast_to(lax.rsqrt(squares / D + epsilon), (SEQS, LANES))
@@ -166,8 +184,6 @@
     sums = [jnp.zeros((SEQS, LANES), F32)]
 
     def score(group):
-        for copy in copies[4 * group : 4 * group + 4]:
-            copy.wait()
         for pair in (2 * group, 2 * group + 1):
             at = slice(pair * 8, pair * 8 + 8)
             both_keys = jnp.concatenate([keys[2 * pair], keys[2 * pair + 1]], axis=1)
@@ -198,10 +214,6 @@
         )
         return jnp.where(row[:8] < 4, valued[:, :LANES], valued[:, LANES:])
 
-    def arrive(seqs):
-        for seq in seqs:
-            copies[SEQS + seq].wait()
-
     def give(group, parts):
         sixteen = jnp.concatenate(parts, axis=0).astype(BF16)
         for dest in range(SEQS):
@@ -211,7 +223,6 @@
     for group in range(1, 4):
         score(group)
         weigh(group - 1)
-    arrive(range(4))
     give(0, [value(0), value(1)])
     weigh(3)
     scale = scale_rows[pl.ds(me, 1), :]
@@ -240,13 +251,8 @@
     ).astype(BF16)
     for dest in range(SEQS):
         out[dest, 64:72, :] = tail
-    for group in range(1, 3):
-        arrive(range(4 * group, 4 * group + 4))
+    for group in range(1, 4):
         give(group, [value(2 * group), value(2 * group + 1)])
-    arrive((12, 13))
-    early = value(6)
-    arrive((14, 15))
-    give(3, [early, value(7)])
 
 
 def thirds(x):
@@ -307,16 +313,39 @@
         out[dest] = partial_out
 
 
+def load_kernel(source, target, arrived):
+    copies = [
+        pltpu.make_async_copy(
+            source.at[pl.ds(4 * n, 4)], target.at[pl.ds(4 * n, 4)], arrived.at[n]
+        )
+        for n in range(4)
+    ]
+    for copy in copies:
+        copy.start()
+    for copy in copies:
+        copy.wait()
+
+
+def load_call(source, name):
+    return pl.pallas_call(
+        load_kernel,
+        in_specs=[ANY],
+        out_specs=VM,
+        out_shape=pltpu.VMEM(source.shape, BF16),
+        scratch_shapes=[pltpu.SemaphoreType.DMA((4,))],
+        compiler_params=SMALL,
+        cost_estimate=pl.CostEstimate(flops=2**31, bytes_accessed=2**24, transcendentals=0),
+        name=name,
+    )(in_hbm(source))
+
+
 def attend_call(tables, got, keys, values, name):
     return pl.pallas_call(
         attend_kernel,
-        in_specs=[VM, VM, ANY, ANY],
+        in_specs=[VM] * 7,
         out_specs=VM,
         out_shape=jax.ShapeDtypeStruct((SEQS, 72, LANES), BF16),
         scratch_shapes=[
-            pltpu.VMEM(keys.shape, BF16),
-            pltpu.VMEM(values.shape, BF16),
-            pltpu.SemaphoreType.DMA((2, SEQS)),
             pltpu.VMEM((32, LANES), F32),
             pltpu.VMEM((SEQS, LANES), F32),
             pltpu.VMEM((64, 256), BF16),
@@ -325,7 +354,7 @@
         ],
         compiler_params=BIG,
         name=name,
-    )(tables, got, in_hbm(keys), in_hbm(values))
+    )(tables, *got, keys, values)
 
 
 def local(
@@ -342,12 +371,12 @@
     value_cache,
 ):
     rates = np.tile(theta_base ** (-np.arange(DH // 2) / (DH // 2)), 4)
-    sent, tables = pl.pallas_call(
+    *sent, tables = pl.pallas_call(
         project_kernel,
         in_specs=[ANY] * 8,
-        out_specs=[VM, VM],
+        out_specs=[VM] * 5,
         out_shape=[
-            jax.ShapeDtypeStruct((SEQS, 40, LANES), F32),
+            *[jax.ShapeDtypeStruct((56, LANES), F32)] * 4,
             jax.ShapeDtypeStruct((40, LANES), F32),
         ],
         scratch_shapes=[
@@ -357,6 +386,7 @@
             pltpu.VMEM((1, HEADS), F32),
             pltpu.VMEM((1, LANES), F32),
             pltpu.VMEM((3, 256, 256), BF16),
+            pltpu.VMEM((64, LANES), F32),
             pltpu.SemaphoreType.DMA((5,)),
             pltpu.SemaphoreType.DMA((3,)),
         ],
@@ -372,10 +402,23 @@
         in_hbm(key_weight),
         in_hbm(value_weight),
     )
-    got = lax.all_to_all(sent, "kv", split_axis=0, concat_axis=0, tiled=True)
+    halves = pl.pallas_call(
+        halfway_kernel,
+        in_specs=[VM] * 4,
+        out_specs=[VM] * 4,
+        out_shape=[jax.ShapeDtypeStruct((40, LANES), F32)] * 4,
+        scratch_shapes=[pltpu.VMEM((56, LANES), F32)],
+        compiler_params=SMALL,
+        name="halfway",
+    )(*swapped(sent, 1))
+    got = swapped(halves, 4)
     cache_shape = (SEQS, 2048, LANES)
     shared = attend_call(
-        tables, got, key_cache.reshape(cache_shape), value_cache.reshape(cache_shape), "attend"
+        tables,
+        got,
+        load_call(key_cache.reshape(cache_shape), "keys"),
+        load_call(value_cache.reshape(cache_shape), "values"),
+        "attend",
     )
     everyone = lax.all_to_all(shared, "kv", split_axis=0, concat_axis=0, tiled=True)
     partial_out = pl.pallas_call(

time: 49.1 us -> 50.2 us (1.022)
  blocking collectives: 39.4 us -> 25.7 us
  starting transfers between devices: 0 us -> 9.84 us
  Pallas kernels: 8.81 us -> 12.7 us
  waiting for transfers between devices: 0 us -> 1.02 us
    all_to_all x1 -> x0, blocking collectives: 16.9 us -> none  [local(): got = lax.all_to_all(sent, 'kv', split_axis=0, concat_axis=0, tiled=True)]
    ppermute x0 -> x6, starting transfers between devices: none -> 9.84 us  [swapped(): lax.ppermute(x, 'kv', [(i, i ^ step * (n + 1)) for i in range(16)])]
    pallas_call x2 -> x5, Pallas kernels: 8.17 us -> 12.1 us  [the longest x2 7 us: load_call(): pl.pallas_call(load_kernel, in_specs=[ANY], out_specs=VM, out_shape=pltpu...]
    all_to_all x1, blocking collectives: 10.7 us -> 13 us  [local(): lax.all_to_all(shared, 'kv', split_axis=0, concat_axis=0, tiled=True)]
    ppermute x0 -> x6, waiting for transfers between devices: none -> 1.02 us  [swapped(): lax.ppermute(x, 'kv', [(i, i ^ step * (n + 1)) for i in range(16)])]
    all_to_all x1, blocking collectives: 11.8 us -> 12.7 us  [local(): lax.all_to_all(partial_out, 'tp', split_axis=0, concat_axis=0, tiled=True)]
  transfers between devices with their start and end apart: 0 -> 6, of which waited for: 0 -> 2; matrix products, arithmetic and copies ran while one was open for 0% -> 0% of each run, Pallas kernels for 0% -> 14%
where the time goes in v7:
time: 50.2 us; the launch traced here: 50 us
  blocking collectives  25.7 us (51%)
  Pallas kernels  12.7 us (25%)
  starting transfers between devices  9.84 us (20%)
  waiting for transfers between devices  1.02 us (2%)
  other arithmetic  0.61 us (1%)
    all_to_all x1, blocking collectives, local(): lax.all_to_all(shared, 'kv', split_axis=0, concat_axis=0, tiled=True)  13 us
    all_to_all x1, blocking collectives, local(): lax.all_to_all(partial_out, 'tp', split_axis=0, concat_axis=0, tiled=True)  12.7 us
    ppermute x6, starting transfers between devices, swapped(): lax.ppermute(x, 'kv', [(i, i ^ step * (n + 1)) for i in range(16)])  9.84 us
    pallas_call x2, Pallas kernels, load_call(): pl.pallas_call(load_kernel, in_specs=[ANY], out_specs=VM, out_shape=pltpu...  7 us
    pallas_call x1, Pallas kernels, attend_call(): pl.pallas_call(attend_kernel, in_specs=[VM] * 7, out_specs=VM, out_shape=...  3.53 us
    pallas_call x1, Pallas kernels, local(): pl.pallas_call(project_kernel, in_specs=[ANY] * 8, out_specs=[VM] * 5, ou...  1.52 us
    ppermute x6, waiting for transfers between devices, swapped(): lax.ppermute(x, 'kv', [(i, i ^ step * (n + 1)) for i in range(16)])  1.02 us
  transfers between devices with their start and end apart: 6, of which 2 were waited for; matrix products, arithmetic and copies ran while one was open for 0% of the time, Pallas kernels for 14%

profile of v7, /device:TPU:1, one launch (start us, length us, event | category | flops | bytes accessed | tf_op | source)
XLA Modules:
  0.0 50.0 jit_solution(8607301300374823805)
XLA Ops:
  0.0 1.5 %project.1 = (f32[56,128]{1,0:T(8,128)S(1)}, f32[56,128]{1,0:T(8,128)S(1)}, f32[56,128]{1,0:T(8,128)S(1)}, f32[56,128]{1,0:T(8,128)S(1)}, f32[40,128]{1,0:T(8,128)S(1)}) custom-call(bf16[16,256]{1,0:T(8,128)(2,1)} %tokens_in.1, f32[1,256]{1,0:T(1,128)} %bitcast.9, s32[1,16]{1,0:T(1,128)} %bitcast.10, f32[1,2]{1,0:T(1,128)} %bitcast.11, ...), custom_call_target="tpu_custom_call" | custom-call | tf_op jit(solution)/shard_map/project/pallas_call | solution.py:374
  1.5 2.2 %collective-permute-start = (f32[56,128]{1,0:T(8,128)S(1)}, f32[56,128]{1,0:T(8,128)S(1)}, u32[]{:S(2)}, u32[]{:S(2)}) collective-permute-start(f32[56,128]{1,0:T(8,128)S(1)} %get-tuple-element.16), channel_id=1, source_target_pairs={{0,8},{8,0},{16,24},{24,16},{32,40},{40,32},{48,56},{56,48},{64,72... | collective-permute-start | bytes 86024 | tf_op jit(solution)/shard_map/ppermute | solution.py:126
  3.7 2.6 %collective-permute-start.1 = (f32[56,128]{1,0:T(8,128)S(1)}, f32[56,128]{1,0:T(8,128)S(1)}, u32[]{:S(2)}, u32[]{:S(2)}) collective-permute-start(f32[56,128]{1,0:T(8,128)S(1)} %get-tuple-element.17), channel_id=1, source_target_pairs={{0,16},{8,24},{16,0},{24,8},{32,48},{40,56},{48,32},{56,40},{64,80... | collective-permute-start | bytes 86024 | tf_op jit(solution)/shard_map/ppermute | solution.py:126
  6.3 0.0 collective-permute-start.2
  6.3 3.5 %keys.1 = bf16[16,2048,128]{2,1,0:T(8,128)(2,1)S(1)} custom-call(bf16[16,2048,128]{2,1,0:T(8,128)(2,1)} %bitcast.7), custom_call_target="tpu_custom_call" | custom-call | flops 2147483648 | bytes 16777216 | tf_op jit(solution)/shard_map/keys/pallas_call | solution.py:330
  9.9 0.0 collective-permute-done.one
  9.9 0.0 collective-permute-done.1.two
  9.9 0.4 collective-permute-done.2.three
  10.3 1.7 %collective-permute-start.3 = (f32[40,128]{1,0:T(8,128)S(1)}, f32[40,128]{1,0:T(8,128)S(1)}, u32[]{:S(2)}, u32[]{:S(2)}) collective-permute-start(f32[40,128]{1,0:T(8,128)S(1)} %get-tuple-element.20), channel_id=1, source_target_pairs={{0,32},{8,40},{16,48},{24,56},{32,0},{40,8},{48,16},{56,24},{64,96... | collective-permute-start | bytes 61448 | tf_op jit(solution)/shard_map/ppermute | solution.py:126
  12.0 3.3 %collective-permute-start.4 = (f32[40,128]{1,0:T(8,128)S(1)}, f32[40,128]{1,0:T(8,128)S(1)}, u32[]{:S(2)}, u32[]{:S(2)}) collective-permute-start(f32[40,128]{1,0:T(8,128)S(1)} %get-tuple-element.21), channel_id=1, source_target_pairs={{0,64},{8,72},{16,80},{24,88},{32,96},{40,104},{48,112},{56,120},{... | collective-permute-start | bytes 61448 | tf_op jit(solution)/shard_map/ppermute | solution.py:126
  15.3 0.0 collective-permute-start.5
  15.3 3.5 %values.1 = bf16[16,2048,128]{2,1,0:T(8,128)(2,1)S(1)} custom-call(bf16[16,2048,128]{2,1,0:T(8,128)(2,1)} %bitcast.8), custom_call_target="tpu_custom_call" | custom-call | flops 2147483648 | bytes 16777216 | tf_op jit(solution)/shard_map/values/pallas_call | solution.py:330
  18.8 0.0 collective-permute-done.3.one
  18.8 0.0 collective-permute-done.4.two
  18.9 0.6 %collective-permute-done.5.three = f32[40,128]{1,0:T(8,128)S(1)} collective-permute-done((f32[40,128]{1,0:T(8,128)S(1)}, f32[40,128]{1,0:T(8,128)S(1)}, u32[]{:S(2)}, u32[]{:S(2)}) %collective-permute-start.5) | collective-permute-done | bytes 20512 | tf_op jit(solution)/shard_map/ppermute | solution.py:126
  19.5 0.0 copy-start
  19.5 0.0 copy-start.1
  19.5 3.5 %attend.1 = bf16[16,72,128]{2,1,0:T(8,128)(2,1)S(1)} custom-call(f32[40,128]{1,0:T(8,128)S(1)} %get-tuple-element.14.tables, f32[40,128]{1,0:T(8,128)S(1)} %get-tuple-element.19.mine, f32[40,128]{1,0:T(8,128)S(1)} %collective-permute-done.3.one, f32[40,128]{1,0:T(8,128)S(1)} %collective-permute-done.4.two, f32[40,128]{1,0:T(8,128)S(1)} %collective-permute-done.5.three, ...), custom_call_target="tpu_custom_call" | custom-call | tf_op jit(solution)/shard_map/attend/pallas_call | solution.py:343
  23.0 13.0 %all_to_all.10.got = bf16[16,72,128]{2,1,0:T(8,128)(2,1)S(1)} all-to-all(bf16[16,72,128]{2,1,0:T(8,128)(2,1)S(1)} %attend.1), channel_id=1, replica_groups=mesh['kv'=16,'tp'=8] {'kv'}, dimensions={0} | all-to-all | bytes 589824 | tf_op jit(solution)/shard_map/all_to_all | solution.py:423
  36.0 0.0 copy-done
  36.0 0.0 copy-done.1
  36.0 0.6 %finish.1 = bf16[8,16,256]{2,1,0:T(8,128)(2,1)S(1)} custom-call(bf16[16,72,128]{2,1,0:T(8,128)(2,1)S(1)} %all_to_all.10.got, f32[40,128]{1,0:T(8,128)S(1)} %get-tuple-element.14.tables, f32[1,128]{1,0:T(1,128)S(1)} %bitcast.6, bf16[256,256]{1,0:T(8,128)(2,1)S(1)} %copy-done), custom_call_target="tpu_custom_call" | custom-call | tf_op jit(solution)/shard_map/finish/pallas_call | solution.py:424
  36.7 12.7 %all_to_all.11 = bf16[8,16,256]{2,1,0:T(8,128)(2,1)S(1)} all-to-all(bf16[8,16,256]{2,1,0:T(8,128)(2,1)S(1)} %finish.1), channel_id=1, replica_groups=mesh['kv'=16,'tp'=8] {'tp'}, dimensions={0} | all-to-all | bytes 131072 | tf_op jit(solution)/shard_map/all_to_all | solution.py:433
  49.4 0.6 %reduce_sum.12 = bf16[16,256]{1,0:T(8,128)(2,1)} reduce(bf16[8,16,256]{2,1,0:T(8,128)(2,1)S(1)} %all_to_all.11, bf16[]{:T(256)} %constant.4.clone.1), dimensions={0}, to_apply=%region_0.0 | reduce | flops 28672 | bytes 73730 | tf_op jit(solution)/shard_map/reduce_sum | solution.py:434
  (1 shorter events, 0.0 us)
Async XLA Ops:
  1.5 8.3 %collective-permute-start = (f32[56,128]{1,0:T(8,128)S(1)}, f32[56,128]{1,0:T(8,128)S(1)}, u32[]{:S(2)}, u32[]{:S(2)}) collective-permute-start(f32[56,128]{1,0:T(8,128)S(1)} %get-tuple-element.16), channel_id=1, source_target_pairs={{0,8},{8,0},{16,24},{24,16},{32,40},{40,32},{48,56},{56,48},{64,72... | collective-permute-start | bytes 86024 | tf_op jit(solution)/shard_map/ppermute | solution.py:126
  3.7 6.1 %collective-permute-start.1 = (f32[56,128]{1,0:T(8,128)S(1)}, f32[56,128]{1,0:T(8,128)S(1)}, u32[]{:S(2)}, u32[]{:S(2)}) collective-permute-start(f32[56,128]{1,0:T(8,128)S(1)} %get-tuple-element.17), channel_id=1, source_target_pairs={{0,16},{8,24},{16,0},{24,8},{32,48},{40,56},{48,32},{56,40},{64,80... | collective-permute-start | bytes 86024 | tf_op jit(solution)/shard_map/ppermute | solution.py:126
  6.3 3.9 %collective-permute-start.2 = (f32[56,128]{1,0:T(8,128)S(1)}, f32[56,128]{1,0:T(8,128)S(1)}, u32[]{:S(2)}, u32[]{:S(2)}) collective-permute-start(f32[56,128]{1,0:T(8,128)S(1)} %get-tuple-element.18), channel_id=1, source_target_pairs={{0,24},{8,16},{16,8},{24,0},{32,56},{40,48},{48,40},{56,32},{64,88... | collective-permute-start | bytes 86024 | tf_op jit(solution)/shard_map/ppermute | solution.py:126
  10.3 8.5 %collective-permute-start.3 = (f32[40,128]{1,0:T(8,128)S(1)}, f32[40,128]{1,0:T(8,128)S(1)}, u32[]{:S(2)}, u32[]{:S(2)}) collective-permute-start(f32[40,128]{1,0:T(8,128)S(1)} %get-tuple-element.20), channel_id=1, source_target_pairs={{0,32},{8,40},{16,48},{24,56},{32,0},{40,8},{48,16},{56,24},{64,96... | collective-permute-start | bytes 61448 | tf_op jit(solution)/shard_map/ppermute | solution.py:126
  12.0 6.8 %collective-permute-start.4 = (f32[40,128]{1,0:T(8,128)S(1)}, f32[40,128]{1,0:T(8,128)S(1)}, u32[]{:S(2)}, u32[]{:S(2)}) collective-permute-start(f32[40,128]{1,0:T(8,128)S(1)} %get-tuple-element.21), channel_id=1, source_target_pairs={{0,64},{8,72},{16,80},{24,88},{32,96},{40,104},{48,112},{56,120},{... | collective-permute-start | bytes 61448 | tf_op jit(solution)/shard_map/ppermute | solution.py:126
  15.3 4.1 %collective-permute-start.5 = (f32[40,128]{1,0:T(8,128)S(1)}, f32[40,128]{1,0:T(8,128)S(1)}, u32[]{:S(2)}, u32[]{:S(2)}) collective-permute-start(f32[40,128]{1,0:T(8,128)S(1)} %get-tuple-element.22), channel_id=1, source_target_pairs={{0,96},{8,104},{16,112},{24,120},{32,64},{40,72},{48,80},{56,88},{... | collective-permute-start | bytes 61448 | tf_op jit(solution)/shard_map/ppermute | solution.py:126
  19.5 16.5 %copy-start = (bf16[256,256]{1,0:T(8,128)(2,1)S(1)}, bf16[256,256]{1,0:T(8,128)(2,1)}, u32[]{:S(2)}) copy-start(bf16[256,256]{1,0:T(8,128)(2,1)} %out_weight.1) | copy-start | bytes 393220
  19.5 16.5 %copy-start.1 = (f32[128]{0:T(128)S(1)}, f32[128]{0:T(128)}, u32[]{:S(2)}) copy-start(f32[128]{0:T(128)} %param.19) | copy-start | bytes 1540

commit v8 on v6

--- a/solution.py
+++ b/solution.py
@@ -15,6 +15,7 @@
 epsilon = 1e-05
 theta_base = 500000.0
 floor_value = -1e30
+EARLY = 5
 
 VM = pl.BlockSpec(memory_space=pltpu.VMEM)
 SM = pl.BlockSpec(memory_space=pltpu.SMEM)
@@ -35,8 +36,8 @@
 
 
 def project_kernel(
-    tokens_in, gain_in, lengths_in, lambdas_in, rates_in, query_in, key_in, value_in, out, tables,
-    tokens, gain, lengths, lambdas, rates, weights, small, large,
+    tokens_in, gain_in, lengths_in, lambdas_in, rates_in, query_in, key_in, value_in, keys_in, out,
+    tables, early_keys, tokens, gain, lengths, lambdas, rates, weights, small, large, early,
 ):
     near = [
         pltpu.make_async_copy(source, target, small.at[n])
@@ -54,7 +55,10 @@
         pltpu.make_async_copy(source, weights.at[n], large.at[n])
         for n, source in enumerate((query_in, key_in, value_in))
     ]
-    for copy in (*near, *far):
+    ahead = [
+        pltpu.make_async_copy(keys_in.at[n], early_keys.at[n], early.at[n]) for n in range(EARLY)
+    ]
+    for copy in (*near, *far, *ahead):
         copy.start()
     for copy in near:
         copy.wait()
@@ -101,6 +105,8 @@
             ],
             axis=0,
         )
+    for copy in ahead:
+        copy.wait()
 
 
 def turned(x, cosine, sine):
@@ -112,17 +118,23 @@
 
 
 def attend_kernel(
-    tables, got, keys_in, values_in, out, keys, values, arrived, query_rows, scale_rows,
+    tables, got, early_keys, keys_in, values_in, out, keys, values, arrived, query_rows, scale_rows,
     asked_rows, score_rows, weight_rows,
 ):
-    copies = []
-    for kind, (source, target) in enumerate(((keys_in, keys), (values_in, values))):
-        for seq in range(SEQS):
-            copies.append(
-                pltpu.make_async_copy(source.at[seq], target.at[seq], arrived.at[kind, seq])
-            )
-    for copy in copies:
+    key_copies = {
+        seq: pltpu.make_async_copy(keys_in.at[seq], keys.at[seq - EARLY], arrived.at[0, seq])
+        for seq in range(EARLY, SEQS)
+    }
+    value_copies = [
+        pltpu.make_async_copy(values_in.at[seq], values.at[seq], arrived.at[1, seq])
+        for seq in range(SEQS)
+    ]
+    for copy in (*key_copies.values(), *value_copies):
         copy.start()
+
+    def keys_of(seq):
+        return early_keys[seq] if seq < EARLY else keys[seq - EARLY]
+
     me = lax.axis_index("kv")
     cosine, sine = tables[0:16, :], tables[16:32, :]
     summed = jnp.sum(got[...], axis=0)
@@ -166,11 +178,12 @@
     sums = [jnp.zeros((SEQS, LANES), F32)]
 
     def score(group):
-        for copy in copies[4 * group : 4 * group + 4]:
-            copy.wait()
+        for seq in range(4 * group, 4 * group + 4):
+            if seq >= EARLY:
+                key_copies[seq].wait()
         for pair in (2 * group, 2 * group + 1):
             at = slice(pair * 8, pair * 8 + 8)
-            both_keys = jnp.concatenate([keys[2 * pair], keys[2 * pair + 1]], axis=1)
+            both_keys = jnp.concatenate([keys_of(2 * pair), keys_of(2 * pair + 1)], axis=1)
             score_rows[at, :] = lax.dot_general(
                 asked_rows[at, :],
                 both_keys,
@@ -200,7 +213,7 @@
 
     def arrive(seqs):
         for seq in seqs:
-            copies[SEQS + seq].wait()
+            value_copies[seq].wait()
 
     def give(group, parts):
         sixteen = jnp.concatenate(parts, axis=0).astype(BF16)
@@ -307,14 +320,14 @@
         out[dest] = partial_out
 
 
-def attend_call(tables, got, keys, values, name):
+def attend_call(tables, got, early_keys, keys, values, name):
     return pl.pallas_call(
         attend_kernel,
-        in_specs=[VM, VM, ANY, ANY],
+        in_specs=[VM, VM, VM, ANY, ANY],
         out_specs=VM,
         out_shape=jax.ShapeDtypeStruct((SEQS, 72, LANES), BF16),
         scratch_shapes=[
-            pltpu.VMEM(keys.shape, BF16),
+            pltpu.VMEM((SEQS - EARLY, *keys.shape[1:]), BF16),
             pltpu.VMEM(values.shape, BF16),
             pltpu.SemaphoreType.DMA((2, SEQS)),
             pltpu.VMEM((32, LANES), F32),
@@ -325,7 +338,7 @@
         ],
         compiler_params=BIG,
         name=name,
-    )(tables, got, in_hbm(keys), in_hbm(values))
+    )(tables, got, early_keys, in_hbm(keys), in_hbm(values))
 
 
 def local(
@@ -341,14 +354,17 @@
     key_cache,
     value_cache,
 ):
+    cache_shape = (SEQS, 2048, LANES)
+    keys = key_cache.reshape(cache_shape)
     rates = np.tile(theta_base ** (-np.arange(DH // 2) / (DH // 2)), 4)
-    sent, tables = pl.pallas_call(
+    sent, tables, early_keys = pl.pallas_call(
         project_kernel,
-        in_specs=[ANY] * 8,
-        out_specs=[VM, VM],
+        in_specs=[ANY] * 9,
+        out_specs=[VM] * 3,
         out_shape=[
             jax.ShapeDtypeStruct((SEQS, 40, LANES), F32),
             jax.ShapeDtypeStruct((40, LANES), F32),
+            pltpu.VMEM((EARLY, *cache_shape[1:]), BF16),
         ],
         scratch_shapes=[
             pltpu.VMEM((SEQS, 256), BF16),
@@ -359,6 +375,7 @@
             pltpu.VMEM((3, 256, 256), BF16),
             pltpu.SemaphoreType.DMA((5,)),
             pltpu.SemaphoreType.DMA((3,)),
+            pltpu.SemaphoreType.DMA((EARLY,)),
         ],
         compiler_params=SMALL,
         name="project",
@@ -371,11 +388,11 @@
         in_hbm(query_weight),
         in_hbm(key_weight),
         in_hbm(value_weight),
+        in_hbm(keys),
     )
     got = lax.all_to_all(sent, "kv", split_axis=0, concat_axis=0, tiled=True)
-    cache_shape = (SEQS, 2048, LANES)
     shared = attend_call(
-        tables, got, key_cache.reshape(cache_shape), value_cache.reshape(cache_shape), "attend"
+        tables, got, early_keys, keys, value_cache.reshape(cache_shape), "attend"
     )
     everyone = lax.all_to_all(shared, "kv", split_axis=0, concat_axis=0, tiled=True)
     partial_out = pl.pallas_call(

time: 49.1 us -> 49 us (level)
  no operation moved by 1% of the time
where the time goes in v8:
time: 49 us; the launch traced here: 48.8 us
  blocking collectives  39.4 us (80%)
  Pallas kernels  8.71 us (18%)
  other arithmetic  0.61 us (1%)
    all_to_all x1, blocking collectives, local(): got = lax.all_to_all(sent, 'kv', split_axis=0, concat_axis=0, tiled=True)  16.9 us
    all_to_all x1, blocking collectives, local(): lax.all_to_all(partial_out, 'tp', split_axis=0, concat_axis=0, tiled=True)  11.8 us
    all_to_all x1, blocking collectives, local(): lax.all_to_all(shared, 'kv', split_axis=0, concat_axis=0, tiled=True)  10.7 us
    pallas_call x1, Pallas kernels, attend_call(): pl.pallas_call(attend_kernel, in_specs=[VM, VM, VM, ANY, ANY], out_specs=...  5.92 us
    pallas_call x1, Pallas kernels, local(): pl.pallas_call(project_kernel, in_specs=[ANY] * 9, out_specs=[VM] * 3, ou...  2.15 us

profile of v8, /device:TPU:1, one launch (start us, length us, event | category | flops | bytes accessed | tf_op | source)
XLA Modules:
  0.0 48.8 jit_solution(14613246109139918854)
XLA Ops:
  0.0 2.2 %project.1 = (f32[16,40,128]{2,1,0:T(8,128)S(1)}, f32[40,128]{1,0:T(8,128)S(1)}, bf16[5,2048,128]{2,1,0:T(8,128)(2,1)S(1)}) custom-call(bf16[16,256]{1,0:T(8,128)(2,1)} %tokens_in.1, f32[1,256]{1,0:T(1,128)} %bitcast.10, s32[1,16]{1,0:T(1,128)} %bitcast.11, f32[1,2]{1,0:T(1,128)} %bitcast.12, f32[1,128]{1,0:T(1,128)} %constant.9.rates_in, ...), custom_call_target="tpu_custom_call" | custom-call | tf_op jit(solution)/shard_map/project/pallas_call | solution.py:360
  2.2 16.9 %all_to_all.15.got = f32[16,40,128]{2,1,0:T(8,128)S(1)} all-to-all(f32[16,40,128]{2,1,0:T(8,128)S(1)} %get-tuple-element.9), channel_id=1, replica_groups=mesh['kv'=16,'tp'=8] {'kv'}, dimensions={0} | all-to-all | bytes 655360 | tf_op jit(solution)/shard_map/all_to_all | solution.py:393
  19.1 0.0 copy-start
  19.1 0.0 copy-start.1
  19.1 5.9 %attend.1 = bf16[16,72,128]{2,1,0:T(8,128)(2,1)S(1)} custom-call(f32[40,128]{1,0:T(8,128)S(1)} %get-tuple-element.8.tables, f32[16,40,128]{2,1,0:T(8,128)S(1)} %all_to_all.15.got, bf16[5,2048,128]{2,1,0:T(8,128)(2,1)S(1)} %get-tuple-element.10.early_keys, bf16[16,2048,128]{2,1,0:T(8,128)(2,1)} %bitcast.8, bf16[16,2048,128]{2,1,0:T(8,128)(2,1)} %bitcast.9), custom_call_target="tpu_custom_call" | custom-call | tf_op jit(solution)/shard_map/attend/pallas_call | solution.py:324
  25.0 10.7 %all_to_all.16.got = bf16[16,72,128]{2,1,0:T(8,128)(2,1)S(1)} all-to-all(bf16[16,72,128]{2,1,0:T(8,128)(2,1)S(1)} %attend.1), channel_id=1, replica_groups=mesh['kv'=16,'tp'=8] {'kv'}, dimensions={0} | all-to-all | bytes 589824 | tf_op jit(solution)/shard_map/all_to_all | solution.py:397
  35.7 0.0 copy-done
  35.7 0.0 copy-done.1
  35.7 0.6 %finish.1 = bf16[8,16,256]{2,1,0:T(8,128)(2,1)S(1)} custom-call(bf16[16,72,128]{2,1,0:T(8,128)(2,1)S(1)} %all_to_all.16.got, f32[40,128]{1,0:T(8,128)S(1)} %get-tuple-element.8.tables, f32[1,128]{1,0:T(1,128)S(1)} %bitcast.6, bf16[256,256]{1,0:T(8,128)(2,1)S(1)} %copy-done), custom_call_target="tpu_custom_call" | custom-call | tf_op jit(solution)/shard_map/finish/pallas_call | solution.py:398
  36.3 11.8 %all_to_all.17 = bf16[8,16,256]{2,1,0:T(8,128)(2,1)S(1)} all-to-all(bf16[8,16,256]{2,1,0:T(8,128)(2,1)S(1)} %finish.1), channel_id=1, replica_groups=mesh['kv'=16,'tp'=8] {'tp'}, dimensions={0} | all-to-all | bytes 131072 | tf_op jit(solution)/shard_map/all_to_all | solution.py:407
  48.1 0.6 %reduce_sum.12 = bf16[16,256]{1,0:T(8,128)(2,1)} reduce(bf16[8,16,256]{2,1,0:T(8,128)(2,1)S(1)} %all_to_all.17, bf16[]{:T(256)} %constant.4.clone.1), dimensions={0}, to_apply=%region_0.0 | reduce | flops 28672 | bytes 73730 | tf_op jit(solution)/shard_map/reduce_sum | solution.py:408
Async XLA Ops:
  19.1 16.6 %copy-start = (bf16[256,256]{1,0:T(8,128)(2,1)S(1)}, bf16[256,256]{1,0:T(8,128)(2,1)}, u32[]{:S(2)}) copy-start(bf16[256,256]{1,0:T(8,128)(2,1)} %out_weight.1) | copy-start | bytes 393220
  19.1 16.6 %copy-start.1 = (f32[128]{0:T(128)S(1)}, f32[128]{0:T(128)}, u32[]{:S(2)}) copy-start(f32[128]{0:T(128)} %param.19) | copy-start | bytes 1540

commit v9 on v6

--- a/solution.py
+++ b/solution.py
@@ -51,7 +51,7 @@
         )
     ]
     far = [
-        pltpu.make_async_copy(source, weights.at[n], large.at[n])
+        pltpu.make_async_copy(source, weights.at[:, 256 * n : 256 * n + 256], large.at[n])
         for n, source in enumerate((query_in, key_in, value_in))
     ]
     for copy in (*near, *far):
@@ -81,11 +81,10 @@
         ],
         axis=0,
     )
-    products = []
-    for n in range(3):
-        far[n].wait()
-        products.append(jnp.dot(normed, weights[n], preferred_element_type=F32))
-    query, key, value = products
+    for copy in far:
+        copy.wait()
+    products = jnp.dot(normed, weights[...], preferred_element_type=F32)
+    query, key, value = products[:, :256], products[:, 256:512], products[:, 512:]
     blank = jnp.zeros((3, LANES), F32)
     for dest in range(SEQS):
         out[dest, 0:16, :] = query[:, :LANES]
@@ -192,10 +191,19 @@
         sums[0] = sums[0] + jnp.where(place, highest, jnp.where(beside, total, 0.0))
 
     def value(pair):
-        both_values = jnp.concatenate([values[2 * pair], values[2 * pair + 1]], axis=1)
-        valued = jnp.dot(
-            weight_rows[pair * 8 : pair * 8 + 8, :], both_values, preferred_element_type=F32
-        )
+        return sides_of(weighed(pair, slice(0, 2048)))
+
+    def weighed(pair, part):
+        both_values = jnp.concatenate(
+            [values[2 * pair, part, :], values[2 * pair + 1, part, :]], axis=1
+        )
+        return jnp.dot(
+            weight_rows[pair * 8 : pair * 8 + 8, part],
+            both_values,
+            preferred_element_type=F32,
+        )
+
+    def sides_of(valued):
         return jnp.where(row[:8] < 4, valued[:, :LANES], valued[:, LANES:])
 
     def arrive(seqs):
@@ -243,10 +251,8 @@
     for group in range(1, 3):
         arrive(range(4 * group, 4 * group + 4))
         give(group, [value(2 * group), value(2 * group + 1)])
-    arrive((12, 13))
-    early = value(6)
-    arrive((14, 15))
-    give(3, [early, value(7)])
+    arrive(range(12, 16))
+    give(3, [value(6), value(7)])
 
 
 def thirds(x):
@@ -356,7 +362,7 @@
             pltpu.VMEM((1, SEQS), jnp.int32),
             pltpu.VMEM((1, HEADS), F32),
             pltpu.VMEM((1, LANES), F32),
-            pltpu.VMEM((3, 256, 256), BF16),
+            pltpu.VMEM((256, 768), BF16),
             pltpu.SemaphoreType.DMA((5,)),
             pltpu.SemaphoreType.DMA((3,)),
         ],

time: 49.1 us -> 48.7 us (level)
  no operation moved by 1% of the time
where the time goes in v9:
time: 48.7 us; the launch traced here: 48.5 us
  blocking collectives  39.4 us (81%)
  Pallas kernels  8.48 us (17%)
  other arithmetic  0.61 us (1%)
    all_to_all x1, blocking collectives, local(): got = lax.all_to_all(sent, 'kv', split_axis=0, concat_axis=0, tiled=True)  16.9 us
    all_to_all x1, blocking collectives, local(): lax.all_to_all(partial_out, 'tp', split_axis=0, concat_axis=0, tiled=True)  11.8 us
    all_to_all x1, blocking collectives, local(): lax.all_to_all(shared, 'kv', split_axis=0, concat_axis=0, tiled=True)  10.7 us
    pallas_call x1, Pallas kernels, attend_call(): pl.pallas_call(attend_kernel, in_specs=[VM, VM, ANY, ANY], out_specs=VM,...  6.46 us
    pallas_call x1, Pallas kernels, local(): pl.pallas_call(project_kernel, in_specs=[ANY] * 8, out_specs=[VM, VM], ou...  1.37 us

profile of v9, /device:TPU:1, one launch (start us, length us, event | category | flops | bytes accessed | tf_op | source)
XLA Modules:
  0.0 48.5 jit_solution(11804786257997726471)
XLA Ops:
  0.0 1.4 %project.1 = (f32[16,40,128]{2,1,0:T(8,128)S(1)}, f32[40,128]{1,0:T(8,128)S(1)}) custom-call(bf16[16,256]{1,0:T(8,128)(2,1)} %tokens_in.1, f32[1,256]{1,0:T(1,128)} %bitcast.9, s32[1,16]{1,0:T(1,128)} %bitcast.10, f32[1,2]{1,0:T(1,128)} %bitcast.11, f32[1,128]{1,0:T(1,128)} %constant.9.rates_in, bf16[256,256]{1,0:T(8,128)(2,1)} %query_in.1, ...), custom_call_target="tpu_custom_call" | custom-call | tf_op jit(solution)/shard_map/project/pallas_call | solution.py:351
  1.4 16.9 %all_to_all.15.got = f32[16,40,128]{2,1,0:T(8,128)S(1)} all-to-all(f32[16,40,128]{2,1,0:T(8,128)S(1)} %get-tuple-element.8), channel_id=1, replica_groups=mesh['kv'=16,'tp'=8] {'kv'}, dimensions={0} | all-to-all | bytes 655360 | tf_op jit(solution)/shard_map/all_to_all | solution.py:381
  18.3 0.0 copy-start
  18.3 0.0 copy-start.1
  18.3 6.5 %attend.1 = bf16[16,72,128]{2,1,0:T(8,128)(2,1)S(1)} custom-call(f32[40,128]{1,0:T(8,128)S(1)} %get-tuple-element.7.tables, f32[16,40,128]{2,1,0:T(8,128)S(1)} %all_to_all.15.got, bf16[16,2048,128]{2,1,0:T(8,128)(2,1)} %bitcast.7, bf16[16,2048,128]{2,1,0:T(8,128)(2,1)} %bitcast.8), custom_call_target="tpu_custom_call" | custom-call | tf_op jit(solution)/shard_map/attend/pallas_call | solution.py:317
  24.8 10.7 %all_to_all.16.got = bf16[16,72,128]{2,1,0:T(8,128)(2,1)S(1)} all-to-all(bf16[16,72,128]{2,1,0:T(8,128)(2,1)S(1)} %attend.1), channel_id=1, replica_groups=mesh['kv'=16,'tp'=8] {'kv'}, dimensions={0} | all-to-all | bytes 589824 | tf_op jit(solution)/shard_map/all_to_all | solution.py:386
  35.5 0.0 copy-done
  35.5 0.0 copy-done.1
  35.5 0.6 %finish.1 = bf16[8,16,256]{2,1,0:T(8,128)(2,1)S(1)} custom-call(bf16[16,72,128]{2,1,0:T(8,128)(2,1)S(1)} %all_to_all.16.got, f32[40,128]{1,0:T(8,128)S(1)} %get-tuple-element.7.tables, f32[1,128]{1,0:T(1,128)S(1)} %bitcast.6, bf16[256,256]{1,0:T(8,128)(2,1)S(1)} %copy-done), custom_call_target="tpu_custom_call" | custom-call | tf_op jit(solution)/shard_map/finish/pallas_call | solution.py:387
  36.1 11.8 %all_to_all.17 = bf16[8,16,256]{2,1,0:T(8,128)(2,1)S(1)} all-to-all(bf16[8,16,256]{2,1,0:T(8,128)(2,1)S(1)} %finish.1), channel_id=1, replica_groups=mesh['kv'=16,'tp'=8] {'tp'}, dimensions={0} | all-to-all | bytes 131072 | tf_op jit(solution)/shard_map/all_to_all | solution.py:396
  47.9 0.6 %reduce_sum.12 = bf16[16,256]{1,0:T(8,128)(2,1)} reduce(bf16[8,16,256]{2,1,0:T(8,128)(2,1)S(1)} %all_to_all.17, bf16[]{:T(256)} %constant.4.clone.1), dimensions={0}, to_apply=%region_0.0 | reduce | flops 28672 | bytes 73730 | tf_op jit(solution)/shard_map/reduce_sum | solution.py:397
Async XLA Ops:
  18.3 17.2 %copy-start = (bf16[256,256]{1,0:T(8,128)(2,1)S(1)}, bf16[256,256]{1,0:T(8,128)(2,1)}, u32[]{:S(2)}) copy-start(bf16[256,256]{1,0:T(8,128)(2,1)} %out_weight.1) | copy-start | bytes 393220
  18.3 17.2 %copy-start.1 = (f32[128]{0:T(128)S(1)}, f32[128]{0:T(128)}, u32[]{:S(2)}) copy-start(f32[128]{0:T(128)} %param.19) | copy-start | bytes 1540

commit v10 on v7

--- a/solution.py
+++ b/solution.py
@@ -1,3 +1,5 @@
+import functools
+
 import jax
 import jax.numpy as jnp
 import numpy as np
@@ -21,16 +23,12 @@
 ANY = pl.BlockSpec(memory_space=pltpu.HBM)
 F32 = jnp.float32
 BF16 = jnp.bfloat16
-SMALL = pltpu.CompilerParams(vmem_limit_bytes=16 * 1024 * 1024)
-BIG = pltpu.CompilerParams(vmem_limit_bytes=26 * 1024 * 1024)
+SMALL = pltpu.CompilerParams(vmem_limit_bytes=8 * 1024 * 1024)
+BIG = pltpu.CompilerParams(vmem_limit_bytes=30 * 1024 * 1024)
 
 
 def in_hbm(x):
     return pltpu.with_memory_space_constraint(x, pltpu.HBM)
-
-
-def in_vmem(x):
-    return pltpu.with_memory_space_constraint(x, pltpu.VMEM)
 
 
 def iotas(rows):
@@ -56,7 +54,7 @@
         )
     ]
     far = [
-        pltpu.make_async_copy(source, weights.at[n], large.at[n])
+        pltpu.make_async_copy(source, weights.at[:, 256 * n : 256 * n + 256], large.at[n])
         for n, source in enumerate((query_in, key_in, value_in))
     ]
     for copy in (*near, *far):
@@ -86,11 +84,10 @@
         ],
         axis=0,
     )
-    products = []
-    for n in range(3):
-        far[n].wait()
-        products.append(jnp.dot(normed, weights[n], preferred_element_type=F32))
-    query, key, value = products
+    for copy in far:
+        copy.wait()
+    products = jnp.dot(normed, weights[...], preferred_element_type=F32)
+    query, key, value = products[:, :256], products[:, 256:512], products[:, 512:]
     fresh[0:16, :] = key[:, :LANES]
     fresh[16:32, :] = key[:, LANES:]
     fresh[32:48, :] = value[:, :LANES]
@@ -138,9 +135,19 @@
 
 
 def attend_kernel(
-    tables, mine, one, two, three, keys, values, out, query_rows, scale_rows, asked_rows,
-    score_rows, weight_rows,
+    tables, mine, one, two, three, first_keys, second_keys, values_in, out, values, arrived, query_rows, scale_rows,
+    asked_rows, score_rows, weight_rows,
 ):
+    copies = [
+        pltpu.make_async_copy(values_in.at[seq], values.at[seq], arrived.at[seq])
+        for seq in range(SEQS)
+    ]
+    for copy in copies:
+        copy.start()
+
+    def keys_of(seq):
+        return first_keys[seq] if seq < 8 else second_keys[seq - 8]
+
     me = lax.axis_index("kv")
     cosine, sine = tables[0:16, :], tables[16:32, :]
     summed = (mine[...] + one[...]) + (two[...] + three[...])
@@ -186,7 +193,7 @@
     def score(group):
         for pair in (2 * group, 2 * group + 1):
             at = slice(pair * 8, pair * 8 + 8)
-            both_keys = jnp.concatenate([keys[2 * pair], keys[2 * pair + 1]], axis=1)
+            both_keys = jnp.concatenate([keys_of(2 * pair), keys_of(2 * pair + 1)], axis=1)
             score_rows[at, :] = lax.dot_general(
                 asked_rows[at, :],
                 both_keys,
@@ -208,11 +215,24 @@
         sums[0] = sums[0] + jnp.where(place, highest, jnp.where(beside, total, 0.0))
 
     def value(pair):
-        both_values = jnp.concatenate([values[2 * pair], values[2 * pair + 1]], axis=1)
-        valued = jnp.dot(
-            weight_rows[pair * 8 : pair * 8 + 8, :], both_values, preferred_element_type=F32
-        )
+        return sides_of(weighed(pair, slice(0, 2048)))
+
+    def weighed(pair, part):
+        both_values = jnp.concatenate(
+            [values[2 * pair, part, :], values[2 * pair + 1, part, :]], axis=1
+        )
+        return jnp.dot(
+            weight_rows[pair * 8 : pair * 8 + 8, part],
+            both_values,
+            preferred_element_type=F32,
+        )
+
+    def sides_of(valued):
         return jnp.where(row[:8] < 4, valued[:, :LANES], valued[:, LANES:])
+
+    def arrive(seqs):
+        for seq in seqs:
+            copies[seq].wait()
 
     def give(group, parts):
         sixteen = jnp.concatenate(parts, axis=0).astype(BF16)
@@ -223,6 +243,7 @@
     for group in range(1, 4):
         score(group)
         weigh(group - 1)
+    arrive(range(4))
     give(0, [value(0), value(1)])
     weigh(3)
     scale = scale_rows[pl.ds(me, 1), :]
@@ -251,8 +272,11 @@
     ).astype(BF16)
     for dest in range(SEQS):
         out[dest, 64:72, :] = tail
-    for group in range(1, 4):
+    for group in range(1, 3):
+        arrive(range(4 * group, 4 * group + 4))
         give(group, [value(2 * group), value(2 * group + 1)])
+    arrive(range(12, 16))
+    give(3, [value(6), value(7)])
 
 
 def thirds(x):
@@ -313,10 +337,10 @@
         out[dest] = partial_out
 
 
-def load_kernel(source, target, arrived):
+def load_kernel(first, source, target, arrived):
     copies = [
         pltpu.make_async_copy(
-            source.at[pl.ds(4 * n, 4)], target.at[pl.ds(4 * n, 4)], arrived.at[n]
+            source.at[pl.ds(first + 2 * n, 2)], target.at[pl.ds(2 * n, 2)], arrived.at[n]
         )
         for n in range(4)
     ]
@@ -326,12 +350,12 @@
         copy.wait()
 
 
-def load_call(source, name):
+def load_call(source, first, name):
     return pl.pallas_call(
-        load_kernel,
+        functools.partial(load_kernel, first),
         in_specs=[ANY],
         out_specs=VM,
-        out_shape=pltpu.VMEM(source.shape, BF16),
+        out_shape=pltpu.VMEM((8, *source.shape[1:]), BF16),
         scratch_shapes=[pltpu.SemaphoreType.DMA((4,))],
         compiler_params=SMALL,
         cost_estimate=pl.CostEstimate(flops=2**31, bytes_accessed=2**24, transcendentals=0),
@@ -339,13 +363,15 @@
     )(in_hbm(source))
 
 
-def attend_call(tables, got, keys, values, name):
+def attend_call(tables, got, first_keys, second_keys, values, name):
     return pl.pallas_call(
         attend_kernel,
-        in_specs=[VM] * 7,
+        in_specs=[*[VM] * 7, ANY],
         out_specs=VM,
         out_shape=jax.ShapeDtypeStruct((SEQS, 72, LANES), BF16),
         scratch_shapes=[
+            pltpu.VMEM(values.shape, BF16),
+            pltpu.SemaphoreType.DMA((SEQS,)),
             pltpu.VMEM((32, LANES), F32),
             pltpu.VMEM((SEQS, LANES), F32),
             pltpu.VMEM((64, 256), BF16),
@@ -354,7 +380,7 @@
         ],
         compiler_params=BIG,
         name=name,
-    )(tables, *got, keys, values)
+    )(tables, *got, first_keys, second_keys, in_hbm(values))
 
 
 def local(
@@ -385,7 +411,7 @@
             pltpu.VMEM((1, SEQS), jnp.int32),
             pltpu.VMEM((1, HEADS), F32),
             pltpu.VMEM((1, LANES), F32),
-            pltpu.VMEM((3, 256, 256), BF16),
+            pltpu.VMEM((256, 768), BF16),
             pltpu.VMEM((64, LANES), F32),
             pltpu.SemaphoreType.DMA((5,)),
             pltpu.SemaphoreType.DMA((3,)),
@@ -413,11 +439,13 @@
     )(*swapped(sent, 1))
     got = swapped(halves, 4)
     cache_shape = (SEQS, 2048, LANES)
+    keys = key_cache.reshape(cache_shape)
     shared = attend_call(
         tables,
         got,
-        load_call(key_cache.reshape(cache_shape), "keys"),
-        load_call(value_cache.reshape(cache_shape), "values"),
+        load_call(keys, 0, "first"),
+        load_call(keys, 8, "second"),
+        value_cache.reshape(cache_shape),
         "attend",
     )
     everyone = lax.all_to_all(shared, "kv", split_axis=0, concat_axis=0, tiled=True)

time: 50.2 us -> 49.5 us (0.986)
  waiting for transfers between devices: 1.02 us -> 3.61 us
  Pallas kernels: 12.7 us -> 11 us
  blocking collectives: 25.7 us -> 24.2 us
    ppermute x6, waiting for transfers between devices: 1.02 us -> 3.61 us  [swapped(): lax.ppermute(x, 'kv', [(i, i ^ step * (n + 1)) for i in range(16)])]
    all_to_all x1, blocking collectives: 13 us -> 10.4 us  [local(): lax.all_to_all(shared, 'kv', split_axis=0, concat_axis=0, tiled=True)]
    pallas_call x3, Pallas kernels: 10.5 us -> 8.95 us  [the longest x1 4.54 us: attend_call(): pl.pallas_call(attend_kernel, in_specs=[*[VM] * 7, ANY], out_specs=VM, ou...]
    all_to_all x1, blocking collectives: 12.7 us -> 13.8 us  [local(): lax.all_to_all(partial_out, 'tp', split_axis=0, concat_axis=0, tiled=True)]
  transfers between devices with their start and end apart: 6 -> 6, of which waited for: 2 -> 2; matrix products, arithmetic and copies ran while one was open for 0% -> 0% of each run, Pallas kernels for 14% -> 9%
where the time goes in v10:
time: 49.5 us; the launch traced here: 49.3 us
  blocking collectives  24.2 us (49%)
  Pallas kernels  11 us (22%)
  starting transfers between devices  9.84 us (20%)
  waiting for transfers between devices  3.61 us (7%)
  other arithmetic  0.61 us (1%)
    all_to_all x1, blocking collectives, local(): lax.all_to_all(partial_out, 'tp', split_axis=0, concat_axis=0, tiled=True)  13.8 us
    all_to_all x1, blocking collectives, local(): lax.all_to_all(shared, 'kv', split_axis=0, concat_axis=0, tiled=True)  10.4 us
    ppermute x6, starting transfers between devices, swapped(): lax.ppermute(x, 'kv', [(i, i ^ step * (n + 1)) for i in range(16)])  9.84 us
    pallas_call x1, Pallas kernels, attend_call(): pl.pallas_call(attend_kernel, in_specs=[*[VM] * 7, ANY], out_specs=VM, ou...  4.54 us
    pallas_call x2, Pallas kernels, load_call(): pl.pallas_call(functools.partial(load_kernel, first), in_specs=[ANY], out...  4.41 us
    ppermute x6, waiting for transfers between devices, swapped(): lax.ppermute(x, 'kv', [(i, i ^ step * (n + 1)) for i in range(16)])  3.61 us
    pallas_call x1, Pallas kernels, local(): pl.pallas_call(project_kernel, in_specs=[ANY] * 8, out_specs=[VM] * 5, ou...  1.37 us
  transfers between devices with their start and end apart: 6, of which 2 were waited for; matrix products, arithmetic and copies ran while one was open for 0% of the time, Pallas kernels for 9%

profile of v10, /device:TPU:1, one launch (start us, length us, event | category | flops | bytes accessed | tf_op | source)
XLA Modules:
  0.0 49.3 jit_solution(6819350142140588293)
XLA Ops:
  0.0 1.4 %project.1 = (f32[56,128]{1,0:T(8,128)S(1)}, f32[56,128]{1,0:T(8,128)S(1)}, f32[56,128]{1,0:T(8,128)S(1)}, f32[56,128]{1,0:T(8,128)S(1)}, f32[40,128]{1,0:T(8,128)S(1)}) custom-call(bf16[16,256]{1,0:T(8,128)(2,1)} %tokens_in.1, f32[1,256]{1,0:T(1,128)} %bitcast.10, s32[1,16]{1,0:T(1,128)} %bitcast.11, f32[1,2]{1,0:T(1,128)} %bitcast.12, ...), custom_call_target="tpu_custom_call" | custom-call | tf_op jit(solution)/shard_map/project/pallas_call | solution.py:400
  1.4 2.2 %collective-permute-start = (f32[56,128]{1,0:T(8,128)S(1)}, f32[56,128]{1,0:T(8,128)S(1)}, u32[]{:S(2)}, u32[]{:S(2)}) collective-permute-start(f32[56,128]{1,0:T(8,128)S(1)} %get-tuple-element.16), channel_id=1, source_target_pairs={{0,8},{8,0},{16,24},{24,16},{32,40},{40,32},{48,56},{56,48},{64,72... | collective-permute-start | bytes 86024 | tf_op jit(solution)/shard_map/ppermute | solution.py:123
  3.6 2.6 %collective-permute-start.1 = (f32[56,128]{1,0:T(8,128)S(1)}, f32[56,128]{1,0:T(8,128)S(1)}, u32[]{:S(2)}, u32[]{:S(2)}) collective-permute-start(f32[56,128]{1,0:T(8,128)S(1)} %get-tuple-element.17), channel_id=1, source_target_pairs={{0,16},{8,24},{16,0},{24,8},{32,48},{40,56},{48,32},{56,40},{64,80... | collective-permute-start | bytes 86024 | tf_op jit(solution)/shard_map/ppermute | solution.py:123
  6.2 0.0 collective-permute-start.2
  6.2 2.2 %second.1.second_keys = bf16[8,2048,128]{2,1,0:T(8,128)(2,1)S(1)} custom-call(bf16[16,2048,128]{2,1,0:T(8,128)(2,1)} %bitcast.7), custom_call_target="tpu_custom_call" | custom-call | flops 2147483648 | bytes 16777216 | tf_op jit(solution)/shard_map/second/pallas_call | solution.py:354
  8.4 0.0 collective-permute-done.one
  8.4 0.0 collective-permute-done.1.two
  8.4 1.7 %collective-permute-done.2.three = f32[56,128]{1,0:T(8,128)S(1)} collective-permute-done((f32[56,128]{1,0:T(8,128)S(1)}, f32[56,128]{1,0:T(8,128)S(1)}, u32[]{:S(2)}, u32[]{:S(2)}) %collective-permute-start.2) | collective-permute-done | bytes 28704 | tf_op jit(solution)/shard_map/ppermute | solution.py:123
  10.2 1.7 %collective-permute-start.3 = (f32[40,128]{1,0:T(8,128)S(1)}, f32[40,128]{1,0:T(8,128)S(1)}, u32[]{:S(2)}, u32[]{:S(2)}) collective-permute-start(f32[40,128]{1,0:T(8,128)S(1)} %get-tuple-element.20), channel_id=1, source_target_pairs={{0,32},{8,40},{16,48},{24,56},{32,0},{40,8},{48,16},{56,24},{64,96... | collective-permute-start | bytes 61448 | tf_op jit(solution)/shard_map/ppermute | solution.py:123
  11.9 3.3 %collective-permute-start.4 = (f32[40,128]{1,0:T(8,128)S(1)}, f32[40,128]{1,0:T(8,128)S(1)}, u32[]{:S(2)}, u32[]{:S(2)}) collective-permute-start(f32[40,128]{1,0:T(8,128)S(1)} %get-tuple-element.21), channel_id=1, source_target_pairs={{0,64},{8,72},{16,80},{24,88},{32,96},{40,104},{48,112},{56,120},{... | collective-permute-start | bytes 61448 | tf_op jit(solution)/shard_map/ppermute | solution.py:123
  15.2 0.0 collective-permute-start.5
  15.2 2.2 %first.1.first_keys = bf16[8,2048,128]{2,1,0:T(8,128)(2,1)S(1)} custom-call(bf16[16,2048,128]{2,1,0:T(8,128)(2,1)} %bitcast.8), custom_call_target="tpu_custom_call" | custom-call | flops 2147483648 | bytes 16777216 | tf_op jit(solution)/shard_map/first/pallas_call | solution.py:354
  17.4 0.0 collective-permute-done.3.one
  17.4 0.0 collective-permute-done.4.two
  17.4 1.9 %collective-permute-done.5.three = f32[40,128]{1,0:T(8,128)S(1)} collective-permute-done((f32[40,128]{1,0:T(8,128)S(1)}, f32[40,128]{1,0:T(8,128)S(1)}, u32[]{:S(2)}, u32[]{:S(2)}) %collective-permute-start.5) | collective-permute-done | bytes 20512 | tf_op jit(solution)/shard_map/ppermute | solution.py:123
  19.3 0.0 copy-start
  19.3 0.0 copy-start.1
  19.3 4.5 %attend.1 = bf16[16,72,128]{2,1,0:T(8,128)(2,1)S(1)} custom-call(f32[40,128]{1,0:T(8,128)S(1)} %get-tuple-element.14.tables, f32[40,128]{1,0:T(8,128)S(1)} %get-tuple-element.19.mine, f32[40,128]{1,0:T(8,128)S(1)} %collective-permute-done.3.one, f32[40,128]{1,0:T(8,128)S(1)} %collective-permute-done.4.two, f32[40,128]{1,0:T(8,128)S(1)} %collective-permute-done.5.three, ...), custom_call_target="tpu_custom_call" | custom-call | tf_op jit(solution)/shard_map/attend/pallas_call | solution.py:367
  23.9 10.4 %all_to_all.10.got = bf16[16,72,128]{2,1,0:T(8,128)(2,1)S(1)} all-to-all(bf16[16,72,128]{2,1,0:T(8,128)(2,1)S(1)} %attend.1), channel_id=1, replica_groups=mesh['kv'=16,'tp'=8] {'kv'}, dimensions={0} | all-to-all | bytes 589824 | tf_op jit(solution)/shard_map/all_to_all | solution.py:451
  34.3 0.0 copy-done
  34.3 0.0 copy-done.1
  34.3 0.6 %finish.1 = bf16[8,16,256]{2,1,0:T(8,128)(2,1)S(1)} custom-call(bf16[16,72,128]{2,1,0:T(8,128)(2,1)S(1)} %all_to_all.10.got, f32[40,128]{1,0:T(8,128)S(1)} %get-tuple-element.14.tables, f32[1,128]{1,0:T(1,128)S(1)} %bitcast.6, bf16[256,256]{1,0:T(8,128)(2,1)S(1)} %copy-done), custom_call_target="tpu_custom_call" | custom-call | tf_op jit(solution)/shard_map/finish/pallas_call | solution.py:452
  34.9 13.8 %all_to_all.11 = bf16[8,16,256]{2,1,0:T(8,128)(2,1)S(1)} all-to-all(bf16[8,16,256]{2,1,0:T(8,128)(2,1)S(1)} %finish.1), channel_id=1, replica_groups=mesh['kv'=16,'tp'=8] {'tp'}, dimensions={0} | all-to-all | bytes 131072 | tf_op jit(solution)/shard_map/all_to_all | solution.py:461
  48.7 0.6 %reduce_sum.12 = bf16[16,256]{1,0:T(8,128)(2,1)} reduce(bf16[8,16,256]{2,1,0:T(8,128)(2,1)S(1)} %all_to_all.11, bf16[]{:T(256)} %constant.4.clone.1), dimensions={0}, to_apply=%region_0.0 | reduce | flops 28672 | bytes 73730 | tf_op jit(solution)/shard_map/reduce_sum | solution.py:462
  (1 shorter events, 0.0 us)
Async XLA Ops:
  1.4 7.0 %collective-permute-start = (f32[56,128]{1,0:T(8,128)S(1)}, f32[56,128]{1,0:T(8,128)S(1)}, u32[]{:S(2)}, u32[]{:S(2)}) collective-permute-start(f32[56,128]{1,0:T(8,128)S(1)} %get-tuple-element.16), channel_id=1, source_target_pairs={{0,8},{8,0},{16,24},{24,16},{32,40},{40,32},{48,56},{56,48},{64,72... | collective-permute-start | bytes 86024 | tf_op jit(solution)/shard_map/ppermute | solution.py:123
  3.6 4.9 %collective-permute-start.1 = (f32[56,128]{1,0:T(8,128)S(1)}, f32[56,128]{1,0:T(8,128)S(1)}, u32[]{:S(2)}, u32[]{:S(2)}) collective-permute-start(f32[56,128]{1,0:T(8,128)S(1)} %get-tuple-element.17), channel_id=1, source_target_pairs={{0,16},{8,24},{16,0},{24,8},{32,48},{40,56},{48,32},{56,40},{64,80... | collective-permute-start | bytes 86024 | tf_op jit(solution)/shard_map/ppermute | solution.py:123
  6.2 3.9 %collective-permute-start.2 = (f32[56,128]{1,0:T(8,128)S(1)}, f32[56,128]{1,0:T(8,128)S(1)}, u32[]{:S(2)}, u32[]{:S(2)}) collective-permute-start(f32[56,128]{1,0:T(8,128)S(1)} %get-tuple-element.18), channel_id=1, source_target_pairs={{0,24},{8,16},{16,8},{24,0},{32,56},{40,48},{48,40},{56,32},{64,88... | collective-permute-start | bytes 86024 | tf_op jit(solution)/shard_map/ppermute | solution.py:123
  10.2 7.2 %collective-permute-start.3 = (f32[40,128]{1,0:T(8,128)S(1)}, f32[40,128]{1,0:T(8,128)S(1)}, u32[]{:S(2)}, u32[]{:S(2)}) collective-permute-start(f32[40,128]{1,0:T(8,128)S(1)} %get-tuple-element.20), channel_id=1, source_target_pairs={{0,32},{8,40},{16,48},{24,56},{32,0},{40,8},{48,16},{56,24},{64,96... | collective-permute-start | bytes 61448 | tf_op jit(solution)/shard_map/ppermute | solution.py:123
  11.9 5.5 %collective-permute-start.4 = (f32[40,128]{1,0:T(8,128)S(1)}, f32[40,128]{1,0:T(8,128)S(1)}, u32[]{:S(2)}, u32[]{:S(2)}) collective-permute-start(f32[40,128]{1,0:T(8,128)S(1)} %get-tuple-element.21), channel_id=1, source_target_pairs={{0,64},{8,72},{16,80},{24,88},{32,96},{40,104},{48,112},{56,120},{... | collective-permute-start | bytes 61448 | tf_op jit(solution)/shard_map/ppermute | solution.py:123
  15.2 4.1 %collective-permute-start.5 = (f32[40,128]{1,0:T(8,128)S(1)}, f32[40,128]{1,0:T(8,128)S(1)}, u32[]{:S(2)}, u32[]{:S(2)}) collective-permute-start(f32[40,128]{1,0:T(8,128)S(1)} %get-tuple-element.22), channel_id=1, source_target_pairs={{0,96},{8,104},{16,112},{24,120},{32,64},{40,72},{48,80},{56,88},{... | collective-permute-start | bytes 61448 | tf_op jit(solution)/shard_map/ppermute | solution.py:123
  19.3 15.0 %copy-start = (bf16[256,256]{1,0:T(8,128)(2,1)S(1)}, bf16[256,256]{1,0:T(8,128)(2,1)}, u32[]{:S(2)}) copy-start(bf16[256,256]{1,0:T(8,128)(2,1)} %out_weight.1) | copy-start | bytes 393220
  19.3 15.0 %copy-start.1 = (f32[128]{0:T(128)S(1)}, f32[128]{0:T(128)}, u32[]{:S(2)}) copy-start(f32[128]{0:T(128)} %param.19) | copy-start | bytes 1540

commit v11 on v8

--- a/solution.py
+++ b/solution.py
@@ -15,7 +15,7 @@
 epsilon = 1e-05
 theta_base = 500000.0
 floor_value = -1e30
-EARLY = 5
+EARLY = 1
 
 VM = pl.BlockSpec(memory_space=pltpu.VMEM)
 SM = pl.BlockSpec(memory_space=pltpu.SMEM)
@@ -52,7 +52,7 @@
         )
     ]
     far = [
-        pltpu.make_async_copy(source, weights.at[n], large.at[n])
+        pltpu.make_async_copy(source, weights.at[:, 256 * n : 256 * n + 256], large.at[n])
         for n, source in enumerate((query_in, key_in, value_in))
     ]
     ahead = [
@@ -85,11 +85,10 @@
         ],
         axis=0,
     )
-    products = []
-    for n in range(3):
-        far[n].wait()
-        products.append(jnp.dot(normed, weights[n], preferred_element_type=F32))
-    query, key, value = products
+    for copy in far:
+        copy.wait()
+    products = jnp.dot(normed, weights[...], preferred_element_type=F32)
+    query, key, value = products[:, :256], products[:, 256:512], products[:, 512:]
     blank = jnp.zeros((3, LANES), F32)
     for dest in range(SEQS):
         out[dest, 0:16, :] = query[:, :LANES]
@@ -205,10 +204,19 @@
         sums[0] = sums[0] + jnp.where(place, highest, jnp.where(beside, total, 0.0))
 
     def value(pair):
-        both_values = jnp.concatenate([values[2 * pair], values[2 * pair + 1]], axis=1)
-        valued = jnp.dot(
-            weight_rows[pair * 8 : pair * 8 + 8, :], both_values, preferred_element_type=F32
-        )
+        return sides_of(weighed(pair, slice(0, 2048)))
+
+    def weighed(pair, part):
+        both_values = jnp.concatenate(
+            [values[2 * pair, part, :], values[2 * pair + 1, part, :]], axis=1
+        )
+        return jnp.dot(
+            weight_rows[pair * 8 : pair * 8 + 8, part],
+            both_values,
+            preferred_element_type=F32,
+        )
+
+    def sides_of(valued):
         return jnp.where(row[:8] < 4, valued[:, :LANES], valued[:, LANES:])
 
     def arrive(seqs):
@@ -256,10 +264,8 @@
     for group in range(1, 3):
         arrive(range(4 * group, 4 * group + 4))
         give(group, [value(2 * group), value(2 * group + 1)])
-    arrive((12, 13))
-    early = value(6)
-    arrive((14, 15))
-    give(3, [early, value(7)])
+    arrive(range(12, 16))
+    give(3, [value(6), value(7)])
 
 
 def thirds(x):
@@ -372,7 +378,7 @@
             pltpu.VMEM((1, SEQS), jnp.int32),
             pltpu.VMEM((1, HEADS), F32),
             pltpu.VMEM((1, LANES), F32),
-            pltpu.VMEM((3, 256, 256), BF16),
+            pltpu.VMEM((256, 768), BF16),
             pltpu.SemaphoreType.DMA((5,)),
             pltpu.SemaphoreType.DMA((3,)),
             pltpu.SemaphoreType.DMA((EARLY,)),

time: 49 us -> 48.6 us (level)
    pallas_call x1, Pallas kernels: 2.15 us -> 1.39 us  [local(): pl.pallas_call(project_kernel, in_specs=[ANY] * 9, out_specs=[VM] * 3, ou...]
where the time goes in v11:
time: 48.6 us; the launch traced here: 48.4 us
  blocking collectives  39.4 us (81%)
  Pallas kernels  8.35 us (17%)
  other arithmetic  0.61 us (1%)
    all_to_all x1, blocking collectives, local(): got = lax.all_to_all(sent, 'kv', split_axis=0, concat_axis=0, tiled=True)  16.9 us
    all_to_all x1, blocking collectives, local(): lax.all_to_all(partial_out, 'tp', split_axis=0, concat_axis=0, tiled=True)  11.8 us
    all_to_all x1, blocking collectives, local(): lax.all_to_all(shared, 'kv', split_axis=0, concat_axis=0, tiled=True)  10.7 us
    pallas_call x1, Pallas kernels, attend_call(): pl.pallas_call(attend_kernel, in_specs=[VM, VM, VM, ANY, ANY], out_specs=...  6.32 us
    pallas_call x1, Pallas kernels, local(): pl.pallas_call(project_kernel, in_specs=[ANY] * 9, out_specs=[VM] * 3, ou...  1.39 us

profile of v11, /device:TPU:1, one launch (start us, length us, event | category | flops | bytes accessed | tf_op | source)
XLA Modules:
  0.0 48.4 jit_solution(14962300382731011572)
XLA Ops:
  0.0 1.4 %project.1 = (f32[16,40,128]{2,1,0:T(8,128)S(1)}, f32[40,128]{1,0:T(8,128)S(1)}, bf16[1,2048,128]{2,1,0:T(8,128)(2,1)S(1)}) custom-call(bf16[16,256]{1,0:T(8,128)(2,1)} %tokens_in.1, f32[1,256]{1,0:T(1,128)} %bitcast.10, s32[1,16]{1,0:T(1,128)} %bitcast.11, f32[1,2]{1,0:T(1,128)} %bitcast.12, f32[1,128]{1,0:T(1,128)} %constant.9.rates_in, ...), custom_call_target="tpu_custom_call" | custom-call | tf_op jit(solution)/shard_map/project/pallas_call | solution.py:366
  1.4 16.9 %all_to_all.15.got = f32[16,40,128]{2,1,0:T(8,128)S(1)} all-to-all(f32[16,40,128]{2,1,0:T(8,128)S(1)} %get-tuple-element.9), channel_id=1, replica_groups=mesh['kv'=16,'tp'=8] {'kv'}, dimensions={0} | all-to-all | bytes 655360 | tf_op jit(solution)/shard_map/all_to_all | solution.py:399
  18.3 0.0 copy-start
  18.3 0.0 copy-start.1
  18.3 6.3 %attend.1 = bf16[16,72,128]{2,1,0:T(8,128)(2,1)S(1)} custom-call(f32[40,128]{1,0:T(8,128)S(1)} %get-tuple-element.8.tables, f32[16,40,128]{2,1,0:T(8,128)S(1)} %all_to_all.15.got, bf16[1,2048,128]{2,1,0:T(8,128)(2,1)S(1)} %get-tuple-element.10.early_keys, bf16[16,2048,128]{2,1,0:T(8,128)(2,1)} %bitcast.8, bf16[16,2048,128]{2,1,0:T(8,128)(2,1)} %bitcast.9), custom_call_target="tpu_custom_call" | custom-call | tf_op jit(solution)/shard_map/attend/pallas_call | solution.py:330
  24.6 10.7 %all_to_all.16.got = bf16[16,72,128]{2,1,0:T(8,128)(2,1)S(1)} all-to-all(bf16[16,72,128]{2,1,0:T(8,128)(2,1)S(1)} %attend.1), channel_id=1, replica_groups=mesh['kv'=16,'tp'=8] {'kv'}, dimensions={0} | all-to-all | bytes 589824 | tf_op jit(solution)/shard_map/all_to_all | solution.py:403
  35.3 0.0 copy-done
  35.3 0.0 copy-done.1
  35.3 0.6 %finish.1 = bf16[8,16,256]{2,1,0:T(8,128)(2,1)S(1)} custom-call(bf16[16,72,128]{2,1,0:T(8,128)(2,1)S(1)} %all_to_all.16.got, f32[40,128]{1,0:T(8,128)S(1)} %get-tuple-element.8.tables, f32[1,128]{1,0:T(1,128)S(1)} %bitcast.6, bf16[256,256]{1,0:T(8,128)(2,1)S(1)} %copy-done), custom_call_target="tpu_custom_call" | custom-call | tf_op jit(solution)/shard_map/finish/pallas_call | solution.py:404
  36.0 11.8 %all_to_all.17 = bf16[8,16,256]{2,1,0:T(8,128)(2,1)S(1)} all-to-all(bf16[8,16,256]{2,1,0:T(8,128)(2,1)S(1)} %finish.1), channel_id=1, replica_groups=mesh['kv'=16,'tp'=8] {'tp'}, dimensions={0} | all-to-all | bytes 131072 | tf_op jit(solution)/shard_map/all_to_all | solution.py:413
  47.8 0.6 %reduce_sum.12 = bf16[16,256]{1,0:T(8,128)(2,1)} reduce(bf16[8,16,256]{2,1,0:T(8,128)(2,1)S(1)} %all_to_all.17, bf16[]{:T(256)} %constant.4.clone.1), dimensions={0}, to_apply=%region_0.0 | reduce | flops 28672 | bytes 73730 | tf_op jit(solution)/shard_map/reduce_sum | solution.py:414
Async XLA Ops:
  18.3 17.0 %copy-start = (bf16[256,256]{1,0:T(8,128)(2,1)S(1)}, bf16[256,256]{1,0:T(8,128)(2,1)}, u32[]{:S(2)}) copy-start(bf16[256,256]{1,0:T(8,128)(2,1)} %out_weight.1) | copy-start | bytes 393220
  18.3 17.0 %copy-start.1 = (f32[128]{0:T(128)S(1)}, f32[128]{0:T(128)}, u32[]{:S(2)}) copy-start(f32[128]{0:T(128)} %param.19) | copy-start | bytes 1540
